TPU v7x, 512 devices: a whole 4x4x16 slice. The times are simulated.
512 devices in a mesh: sp: 64 (over z, y), tp: 8 (over x, core).
Axes of the slice: x: 4, y: 4, z: 16, core: 2. Of those that a mesh axis runs over, the one named last changes fastest.
Arguments:
- stream: bfloat16 [16384, 2048], P(('sp', 'tp')), may hold values from -6 to 6
- queries: bfloat16 [16384, 1024], P('sp', 'tp'), may hold values from -6 to 6
- keys_in: bfloat16 [16384, 1024], P('sp', 'tp'), may hold values from -6 to 6
- values_in: bfloat16 [16384, 1024], P('sp', 'tp'), may hold values from -6 to 6
- gate_in: bfloat16 [16384, 1024], P('sp', 'tp'), may hold values from -6 to 6
- log_decay: float32 [16384, 8], P('sp', 'tp'), may hold values from -0.8 to 0
- head_gain: bfloat16 [1024], P('tp'), may hold values from 0.099609375 to 1.8984375
- out_weight: bfloat16 [1024, 2048], P('tp'), may hold values from -0.1875 to 0.1875
- norm_gain: bfloat16 [2048], replicated, may hold values from 0.099609375 to 1.8984375
- gate_weight: bfloat16 [2048, 5632], P('sp', 'tp'), may hold values from -0.125 to 0.125
- up_weight: bfloat16 [2048, 5632], P('sp', 'tp'), may hold values from -0.125 to 0.125
- down_weight: bfloat16 [5632, 2048], P('tp', 'sp'), may hold values from -0.078125 to 0.078125
Outputs:
- result: bfloat16 [16384, 2048], P(('sp', 'tp'))
All inputs are finite; a program needn't handle non-finite values.
Results may differ from a plain program's by a relative error of at most 0.02.
Values may be sent and summed in bfloat16 or wider, within the bound.
No kernel may reach another device: no remote copies, remote signals or barrier semaphores. Data moves between devices by JAX's collectives and lax.ppermute only.
A program may use at most 64 MiB of HBM per device.

v0:
```python
import jax
import jax.numpy as jnp
from jax import lax
from jax.sharding import Mesh
from jax.sharding import PartitionSpec as P

BLOCK = 128
SP = ("sp_0", "sp_1")
SP_TP = ("sp_0", "sp_1", "tp")


epsilon = 1e-06


def in_one_piece(arrays, axis, dim, along):
    ends, at = ([], 0)
    for a in arrays[:-1]:
        at += a.shape[along]
        ends.append(at)
    both = jnp.concatenate(arrays, axis=along)
    return tuple(jnp.split(lax.all_gather(both, axis, axis=dim, tiled=True), ends, axis=along))


def whole_of(value, axes, dim):
    filled = value
    for number in range(len(axes) - 1, -1, -1):
        filled = lax.all_gather(filled, axes[number], axis=dim, tiled=True)
    return filled


def filled_with(value, identity):
    return jax.tree.map(
        lambda a, e: jnp.broadcast_to(jnp.asarray(e, a.dtype), a.shape), value, identity
    )


def all_in_one(value, axis):
    leaves = jax.tree.leaves(value)
    sequence = sorted(range(len(leaves)), key=lambda k: -leaves[k].size)
    width = (1, *leaves[sequence[0]].shape)[-1]
    lines = [
        jnp.pad(leaves[k].reshape(-1), (0, -leaves[k].size % width)).reshape(-1, width)
        for k in sequence
    ]
    both, at, found = (lax.all_gather(jnp.concatenate(lines), axis), 0, {})
    for k, line in zip(sequence, lines):
        piece = both[:, at : at + len(line)].reshape(len(both), -1)
        found[k] = piece[:, : leaves[k].size].reshape(-1, *leaves[k].shape)
        at += len(line)
    numbers = iter(range(len(leaves)))
    return jax.tree.map(lambda _: found[next(numbers)], value)


def prefix_by_axis(value, axes, combine, identity):
    before = start = filled_with(value, identity)
    so_far = value
    for axis in reversed(axes):
        length, here = (lax.axis_size(axis), lax.axis_index(axis))
        pieces = all_in_one(
            jax.tree.map(
                lambda part, kind: part.astype(kind), so_far, (jnp.bfloat16, jnp.bfloat16)
            ),
            axis,
        )
        inside, so_far = (start, start)
        for k in range(length):
            passed = k < here
            so_far = combine(
                so_far, jax.tree.map(lambda part, own: part[k].astype(own.dtype), pieces, value)
            )
            inside = jax.tree.map(lambda new, old: jnp.where(passed, new, old), so_far, inside)
        before = combine(inside, before)
    return before


def cut_along(value, dim, length):
    shape = value.shape
    tiles = value.reshape(*shape[:dim], length, shape[dim] // length, *shape[dim + 1 :])
    return jnp.moveaxis(tiles, dim, 0)


def summed_on_arrival(value, axis, dim):
    tiles = cut_along(value, dim, lax.axis_size(axis))
    arrived = lax.all_to_all(tiles, axis, split_axis=0, concat_axis=0, tiled=True)
    return arrived.astype(jnp.float32).sum(axis=0)


def sent_to_all(value, axis):
    copies = jnp.broadcast_to(value, (lax.axis_size(axis), *value.shape))
    return lax.all_to_all(copies, axis, split_axis=0, concat_axis=0, tiled=True)


def in_order(tiles, dim):
    tiles = jnp.moveaxis(tiles, 0, dim)
    shape = tiles.shape
    return tiles.reshape(*shape[:dim], shape[dim] * shape[dim + 1], *shape[dim + 2 :])


def gather_directly(value, axis, dim):
    tiles = sent_to_all(value, axis)
    return in_order(tiles, dim)


def block_pass(state, block_inputs):
    query_block, key_block, value_block, decay_block = block_inputs
    head_dim = query_block.shape[-1]
    key_scale = head_dim ** (-0.5)
    running = jnp.cumsum(decay_block, axis=0)
    scores = (
        jnp.einsum("ihd,jhd->hij", query_block, key_block, preferred_element_type=jnp.float32)
        * key_scale
    )
    offsets = jnp.arange(decay_block.shape[0])
    causal = offsets[:, None] >= offsets[None, :]
    log_gap = running.T[:, :, None] - running.T[:, None, :]
    decay_table = jnp.where(causal[None], jnp.exp(jnp.minimum(log_gap, 0.0)), 0.0)
    value_wide = value_block.astype(jnp.float32)
    within = jnp.einsum("hij,jhe->ihe", scores * decay_table, value_wide)
    query_wide = query_block.astype(jnp.float32) * jnp.exp(running)[:, :, None]
    carried = jnp.einsum("ihd,hde->ihe", query_wide, state)
    block_total = running[-1]
    key_wide = (
        key_block.astype(jnp.float32) * key_scale * jnp.exp(block_total[None] - running)[:, :, None]
    )
    state = jnp.exp(block_total)[:, None, None] * state + jnp.einsum(
        "jhd,jhe->hde", key_wide, value_wide
    )
    return (state, within + carried)


def chain_combine(earlier_pair, later_pair):
    return (
        earlier_pair[0] * later_pair[0],
        later_pair[0][:, None, None] * earlier_pair[1] + later_pair[1],
    )


def local(
    stream,
    queries,
    keys_in,
    values_in,
    gate_in,
    log_decay,
    head_gain,
    out_weight,
    norm_gain,
    gate_weight,
    up_weight,
    down_weight,
):
    gate_full, up_full = in_one_piece((gate_weight, up_weight), SP, 0, 1)
    down_full = whole_of(down_weight, SP, 1)
    row_count, heads_here = log_decay.shape
    head_dim = queries.shape[1] // heads_here
    block_count = row_count // BLOCK
    block_shape = (block_count, BLOCK, heads_here, head_dim)
    block_inputs = (
        queries.reshape(block_shape),
        keys_in.reshape(block_shape),
        values_in.reshape(block_shape),
        log_decay.reshape(block_count, BLOCK, heads_here),
    )
    start_state = jnp.zeros((heads_here, head_dim, head_dim), jnp.float32)
    final_state, within = lax.scan(block_pass, start_state, block_inputs)
    within = within.reshape(row_count, heads_here, head_dim)
    running = jnp.cumsum(log_decay, axis=0)
    device_total = running[-1]
    scanned = prefix_by_axis(
        (jnp.exp(device_total), final_state),
        SP,
        chain_combine,
        (jnp.ones_like(device_total), jnp.zeros_like(final_state)),
    )
    incoming = scanned[1]
    query_wide = (
        queries.reshape(row_count, heads_here, head_dim).astype(jnp.float32)
        * jnp.exp(running)[:, :, None]
    )
    retained = within + jnp.einsum("ihd,hde->ihe", query_wide, incoming)
    center = jnp.mean(retained, axis=-1, keepdims=True)
    spread = jnp.mean(jnp.square(retained - center), axis=-1, keepdims=True)
    normed_heads = (
        (retained - center)
        * lax.rsqrt(spread + epsilon)
        * head_gain.astype(jnp.float32).reshape(heads_here, head_dim)
    )
    mixed = (
        jax.nn.silu(gate_in.astype(jnp.float32))
        * normed_heads.reshape(row_count, heads_here * head_dim)
    ).astype(jnp.bfloat16)
    attended = summed_on_arrival(
        jnp.dot(mixed, out_weight, preferred_element_type=jnp.float32).astype(jnp.bfloat16), "tp", 0
    )
    residual = stream.astype(jnp.float32) + attended
    normed = (
        residual
        * lax.rsqrt(jnp.mean(residual * residual, axis=-1, keepdims=True) + epsilon)
        * norm_gain.astype(jnp.float32)
    ).astype(jnp.bfloat16)
    whole_rows = gather_directly(normed, "tp", 0)
    gate_sum = jnp.dot(whole_rows, gate_full, preferred_element_type=jnp.float32)
    up_sum = jnp.dot(whole_rows, up_full, preferred_element_type=jnp.float32)
    hidden = (jax.nn.silu(gate_sum) * up_sum).astype(jnp.bfloat16)
    down_terms = jnp.dot(hidden, down_full, preferred_element_type=jnp.float32)
    mixer_out = summed_on_arrival(down_terms.astype(jnp.bfloat16), "tp", 0)
    return (residual + mixer_out).astype(jnp.bfloat16)


def solution(mesh):
    finer = Mesh(mesh.devices.reshape(16, 4, mesh.shape["tp"]), ("sp_0", "sp_1", "tp"))
    return jax.shard_map(
        local,
        mesh=finer,
        in_specs=(
            P(SP_TP, None),
            P(SP, "tp"),
            P(SP, "tp"),
            P(SP, "tp"),
            P(SP, "tp"),
            P(SP, "tp"),
            P("tp"),
            P("tp", None),
            P(),
            P(SP, "tp"),
            P(SP, "tp"),
            P("tp", SP),
        ),
        out_specs=P(SP_TP, None),
        check_vma=False,
    )
```

profile of v0, /device:TPU:1, one launch (start us, length us, event | category | flops | bytes accessed | tf_op | source)
XLA Modules:
  0.0 272.7 jit_solution(10176328622319258803)
XLA Ops:
  6.5 1.6 pad_maximum_fusion
  8.2 12.5 %all_gather.26 = bf16[704,128]{0,1:T(8,128)(2,1)} all-gather(bf16[704,32]{0,1:T(8,128)(2,1)} %param.25), channel_id=1, replica_groups=mesh['sp_0'=16,'sp_1'=4,'tp'=8] {'sp_1'}, dimensions={1}, use_global_device_ids=true | all-gather | bytes 225280 | tf_op jit(solution)/shard_map/all_gather | solution.py:27
  20.8 1.0 reduce-window.6
  22.8 0.6 slice.251
  24.5 14.7 %while.13 = (s32[]{:T(128)}, f32[1,128,128]{2,1,0:T(8,128)S(1)}, f32[2,128,1,128]{1,0,3,2:T(2,128)S(1)}, f32[2,128,1]{1,2,0:T(1,128)}, bf16[2,128,1,128]{3,1,2,0...) while((s32[]{:T(128)}, f32[1,128,128]{2,1,0:T(8,128)S(1)}, ...), condition=%wide.region_2.3_spmd.clone, body=%wide.region_0.2_spmd.clone.sunk | while | flops 17039492 | bytes 732327 | solution.py:165
  24.5 0.7 fusion.243
  26.7 0.6 fusion.244
  27.2 1.1 fusion.246
  28.4 1.0 fusion.247
  29.4 1.0 fusion.245
  30.4 1.5 dynamic_update_slice.6
  31.9 0.7 fusion.243
  34.0 0.6 fusion.244
  34.6 1.1 fusion.246
  35.7 1.0 fusion.247
  36.7 1.0 fusion.245
  37.8 1.5 dynamic_update_slice.6
  39.3 9.9 %all-gather.2 = bf16[4,129,128]{2,1,0:T(8,128)(2,1)S(1)} all-gather(bf16[1,129,128]{2,1,0:T(8,128)(2,1)S(1)} %maximum_bitcast_fusion), channel_id=2, replica_groups=mesh['sp_0'=16,'sp_1'=4,'tp'=8] {'sp_1'}, dimensions={0}, use_global_device_ids=true | all-gather | bytes 165120 | tf_op jit(solution)/shard_map/all_gather | solution.py:45
  49.5 0.6 fusion.218
  53.3 32.4 %all-gather.3 = bf16[16,129,128]{2,1,0:T(8,128)(2,1)S(1)} all-gather(bf16[1,129,128]{2,1,0:T(8,128)(2,1)S(1)} %maximum_bitcast_fusion.1), channel_id=3, replica_groups=mesh['sp_0'=16,'sp_1'=4,'tp'=8] {'sp_0'}, dimensions={0}, use_global_device_ids=true | all-gather | bytes 561408 | tf_op jit(solution)/shard_map/all_gather | solution.py:45
  85.7 0.6 fusion.217
  97.0 1.3 fusion.219
  98.4 1.6 convolution_convert_fusion
  100.0 16.1 %all-to-all-start = ((bf16[8,32,2048]{2,1,0:T(8,128)(2,1)}), bf16[8,32,2048]{2,1,0:T(8,128)(2,1)S(1)}, u32[]{:S(2)}, u32[]{:S(2)}) async-start(bf16[8,32,2048]{2,1,0:T(8,128)(2,1)} %bitcast.55), calls=%async_computation | async-start | bytes 2097152 | tf_op jit(solution)/shard_map/all_to_all | solution.py:84
  116.0 15.0 %all-to-all-done = bf16[8,32,2048]{2,1,0:T(8,128)(2,1)S(1)} async-done(((bf16[8,32,2048]{2,1,0:T(8,128)(2,1)}), bf16[8,32,2048]{2,1,0:T(8,128)(2,1)S(1)}, u32[]{:S(2)}, u32[]{:S(2)}) %all-to-all-start) | async-done | bytes 1048608 | tf_op jit(solution)/shard_map/all_to_all | solution.py:84
  131.5 18.3 %all_to_all.15 = bf16[8,32,2048]{2,1,0:T(8,128)(2,1)S(1)} all-to-all(bf16[8,32,2048]{2,1,0:T(8,128)(2,1)S(1)} %broadcast_in_dim.17), channel_id=1, replica_groups=mesh['sp_0'=16,'sp_1'=4,'tp'=8] {'tp'}, dimensions={0} | all-to-all | bytes 2097152 | tf_op jit(solution)/shard_map/all_to_all | solution.py:90
  149.9 7.6 %all-gather.7.cloned.1.call-done = bf16[2048,1408]{1,0:T(8,128)(2,1)} async-done(((bf16[32,1408]{1,0:T(8,128)(2,1)}), bf16[2048,1408]{1,0:T(8,128)(2,1)}) %all-gather.7.cloned.1.call-update) | async-done | bytes 5767184 | tf_op jit(solution)/shard_map/all_gather | solution.py:21
  157.5 4.1 %fusion.48 = f32[256,704]{0,1:T(8,128)} fusion(bf16[256,2048]{1,0:T(8,128)(2,1)S(1)} %bitcast.195, bf16[2048,1408]{1,0:T(8,128)(2,1)} %all-gather.7.cloned.1.call-done), kind=kOutput, calls=%fused_computation.49 | convolution fusion | flops 738197504 | bytes 4915200 | tf_op jit(solution)/shard_map/dot_general | solution.py:202
  161.6 67.5 %all-gather.9.cloned.1.call-done = bf16[704,2048]{0,1:T(8,128)(2,1)} async-done(((bf16[704,128]{0,1:T(8,128)(2,1)}), bf16[704,2048]{0,1:T(8,128)(2,1)}) %all-gather.9.cloned.1.call-update) | async-done | bytes 2883600 | tf_op jit(solution)/shard_map/all_gather | solution.py:27
  229.1 7.4 %convolution_convert_fusion.1 = bf16[256,2048]{1,0:T(8,128)(2,1)S(1)} fusion(bf16[704,2048]{0,1:T(8,128)(2,1)} %all-gather.9.cloned.1.call-done, bf16[256,2048]{1,0:T(8,128)(2,1)S(1)} %bitcast.196, bf16[2048,1408]{1,0:T(8,128)(2,1)} %all-gather.7.cloned.1.call-done, f32[256,704]{0,1:T(8,128)} %fusion.48), kind=kOutput, calls=%fused_computation.52 | convolution fusion | flops 1478000640 | bytes 9109504 | tf_op jit(solution)/shard_map/dot_general | solution.py:205
  236.5 28.6 %all_to_all.16 = bf16[8,32,2048]{2,1,0:T(8,128)(2,1)S(1)} all-to-all(bf16[8,32,2048]{2,1,0:T(8,128)(2,1)S(1)} %bitcast.197), channel_id=1, replica_groups=mesh['sp_0'=16,'sp_1'=4,'tp'=8] {'tp'}, dimensions={0} | all-to-all | bytes 2097152 | tf_op jit(solution)/shard_map/all_to_all | solution.py:84
  265.2 0.7 add_convert_fusion
  (53 shorter events, 3.9 us)
Async XLA Ops:
  6.5 91.9 %copy-start = (bf16[128,2048]{1,0:T(8,128)(2,1)S(1)}, bf16[128,2048]{1,0:T(8,128)(2,1)}, u32[]{:S(2)}) copy-start(bf16[128,2048]{1,0:T(8,128)(2,1)} %param.21) | copy-start | bytes 1572868
  6.5 150.9 %all-gather.7.cloned.1.call-start = ((), (), s32[]{:S(2)}) async-start(), calls=%async_computation.3 | async-start | bytes 5857280 | tf_op jit(solution)/shard_map/all_gather | solution.py:21
  8.2 41.0 %copy-start.4 = (bf16[128]{0:T(256)(128)(2,1)S(1)}, bf16[128]{0:T(256)(128)(2,1)}, u32[]{:S(2)}) copy-start(bf16[128]{0:T(256)(128)(2,1)} %param.20) | copy-start | bytes 772
  8.2 41.0 %copy-start.2 = (bf16[256,128]{1,0:T(8,128)(2,1)S(1)}, bf16[256,128]{1,0:T(8,128)(2,1)}, u32[]{:S(2)}) copy-start(bf16[256,128]{1,0:T(8,128)(2,1)} %param.18) | copy-start | bytes 196612
  8.2 220.9 %all-gather.9.cloned.1.call-start = ((), (), s32[]{:S(2)}) async-start(), calls=%async_computation.4 | async-start | bytes 3342336 | tf_op jit(solution)/shard_map/all_gather | solution.py:27
  53.3 62.7 %copy-start.3 = (bf16[2048]{0:T(1024)(128)(2,1)S(1)}, bf16[2048]{0:T(1024)(128)(2,1)}, u32[]{:S(2)}) copy-start(bf16[2048]{0:T(1024)(128)(2,1)} %param.22) | copy-start | bytes 12292
  97.0 34.1 %copy-start.1 = (bf16[32,2048]{1,0:T(8,128)(2,1)S(1)}, bf16[32,2048]{1,0:T(8,128)(2,1)}, u32[]{:S(2)}) copy-start(bf16[32,2048]{1,0:T(8,128)(2,1)} %param.14) | copy-start | bytes 393220
  100.0 31.0 %all-to-all-start = ((bf16[8,32,2048]{2,1,0:T(8,128)(2,1)}), bf16[8,32,2048]{2,1,0:T(8,128)(2,1)S(1)}, u32[]{:S(2)}, u32[]{:S(2)}) async-start(bf16[8,32,2048]{2,1,0:T(8,128)(2,1)} %bitcast.55), calls=%async_computation | async-start | bytes 2097152 | tf_op jit(solution)/shard_map/all_to_all | solution.py:84
Sparse Core Ops, SparseCore 0:
  10.3 147.1 all-gather.6
  159.6 69.4 all-gather.8
where the time goes:
time: 274 us; the launch traced here: 273 us
  blocking collectives  102 us (37%)
  waiting for transfers between devices  90.1 us (33%)
  between operations  28.5 us (10%)
  matrix products  20.7 us (8%)
  starting transfers between devices  16.1 us (6%)
  local copies, waits for them, and re-layouts  8.47 us (3%)
  other arithmetic  5.84 us (2%)
    all_gather x1, waiting for transfers between devices, whole_of(): filled = lax.all_gather(filled, axes[number], axis=dim, tiled=True)  67.5 us
    all_gather x2, blocking collectives, all_in_one(): both, at, found = (lax.all_gather(jnp.concatenate(lines), axis), 0, {})  42.4 us
    all_to_all x1, blocking collectives, summed_on_arrival(): lax.all_to_all(tiles, axis, split_axis=0, concat_axis=0, tiled=True)  28.6 us
    all_to_all x1, blocking collectives, sent_to_all(): return lax.all_to_all(copies, axis, split_axis=0, concat_axis=0, tiled=True)  18.3 us
    all_to_all x1, starting transfers between devices, summed_on_arrival(): lax.all_to_all(tiles, axis, split_axis=0, concat_axis=0, tiled=True)  16.1 us
    all_to_all x1, waiting for transfers between devices, summed_on_arrival(): lax.all_to_all(tiles, axis, split_axis=0, concat_axis=0, tiled=True)  15 us
    all_gather x1, blocking collectives, whole_of(): filled = lax.all_gather(filled, axes[number], axis=dim, tiled=True)  12.5 us
    all_gather x1, waiting for transfers between devices, in_one_piece(): lax.all_gather(both, axis, axis=dim, tiled=True)  7.62 us
  transfers between devices with their start and end apart: 3, of which 3 were waited for; matrix products, arithmetic and copies ran while one was open for 9% of the time, Pallas kernels for 0%

commit v1 on v0

v1 whole, which is shorter than its diff:
```python
import functools

import jax
import jax.numpy as jnp
from jax import lax
from jax.experimental import pallas as pl
from jax.experimental.pallas import tpu as pltpu
from jax.sharding import Mesh
from jax.sharding import PartitionSpec as P

Z, Y = "z", ("y1", "y0")
SP = ("z", "y1", "y0")
TP = ("x", "c")
GROUP = ("y0", "x")
SIZES = {"z": 16, "y1": 2, "y0": 2, "x": 4, "c": 2}
EPS = 1e-6
F32, BF16 = jnp.float32, jnp.bfloat16


def vmem(count):
    return [pl.BlockSpec(memory_space=pltpu.VMEM)] * count


def kernel_cost(flops, moved, exps=0):
    return pl.CostEstimate(flops=flops, bytes_accessed=moved, transcendentals=exps)


def dot(a, b):
    return jnp.dot(a, b, preferred_element_type=F32)


def dot_nt(a, b):
    return lax.dot_general(a, b, (((1,), (1,)), ((), ())), preferred_element_type=F32)


def dot_tn(a, b):
    return lax.dot_general(a, b, (((0,), (0,)), ((), ())), preferred_element_type=F32)


def retention_kernel(q_ref, k_ref, v_ref, decay_ref, within_ref, carry_q_ref, state_ref):
    rows, head_dim = q_ref.shape
    scale = head_dim**-0.5
    at = lax.broadcasted_iota(jnp.int32, (rows, rows), 0)
    to = lax.broadcasted_iota(jnp.int32, (rows, rows), 1)
    causal = at >= to
    running = jnp.sum(jnp.where(causal, decay_ref[...], 0.0), axis=1, keepdims=True)
    across = jnp.sum(jnp.where(at == to, running, 0.0), axis=0, keepdims=True)
    total = running[rows - 1 : rows, :]
    q, k, v = q_ref[...], k_ref[...], v_ref[...]
    table = jnp.where(causal, jnp.exp(jnp.minimum(running - across, 0.0)), 0.0)
    scores = dot_nt(q, k) * scale
    within_ref[...] = dot((scores * table).astype(BF16), v)
    carry_q_ref[...] = (q.astype(F32) * jnp.exp(running)).astype(BF16)
    key_wide = (k.astype(F32) * scale * jnp.exp(total - running)).astype(BF16)
    state = dot_tn(key_wide, v)
    fill = jnp.broadcast_to(total, (8, head_dim))
    slices = state_ref.shape[0]
    part = head_dim // slices
    for n in range(slices):
        state_ref[n, :part, :] = state[n * part : (n + 1) * part]
        state_ref[n, part:, :] = fill


def retention(q, k, v, decay):
    rows, head_dim = q.shape
    part = head_dim // 4
    return pl.pallas_call(
        retention_kernel,
        out_shape=(
            jax.ShapeDtypeStruct((rows, head_dim), F32),
            jax.ShapeDtypeStruct((rows, head_dim), BF16),
            jax.ShapeDtypeStruct((4, part + 8, head_dim), F32),
        ),
        in_specs=vmem(4),
        out_specs=vmem(3),
        cost_estimate=kernel_cost(6 * rows * rows * head_dim, 2**20, rows * rows),
        name="retention",
    )(q, k, v, decay)


def plane_kernel(states_ref, out_ref):
    part = states_ref.shape[1] - 8
    state = states_ref[0, :part, :]
    total = states_ref[0, part : part + 1, :]
    for n in range(1, states_ref.shape[0]):
        own = states_ref[n, part : part + 1, :]
        state = jnp.exp(own) * state + states_ref[n, :part, :]
        total = total + own
    high = total.astype(BF16)
    rest = total - high.astype(F32)
    mid = rest.astype(BF16)
    low = (rest - mid.astype(F32)).astype(BF16)
    line = lax.broadcasted_iota(jnp.int32, (16, total.shape[1]), 0)
    spread = jnp.where(
        line == 0,
        high.astype(F32),
        jnp.where(line == 1, mid.astype(F32), jnp.where(line == 2, low.astype(F32), 0.0)),
    ).astype(BF16)
    packed = state.astype(BF16)
    for n in range(out_ref.shape[0]):
        out_ref[n, :part, :] = packed
        out_ref[n, part:, :] = spread


def plane_state(states):
    count, lines, width = states.shape
    return pl.pallas_call(
        plane_kernel,
        out_shape=jax.ShapeDtypeStruct((16, lines - 8 + 16, width), BF16),
        in_specs=vmem(1),
        out_specs=pl.BlockSpec(memory_space=pltpu.VMEM),
        cost_estimate=kernel_cost(2**18, 2**18, 2**10),
        name="plane_state",
    )(states)


def incoming_kernel(here_ref, planes_ref, states_ref, out_ref):
    part = out_ref.shape[1]
    here = here_ref[0]
    carried = jnp.zeros(out_ref.shape[1:], F32)
    for n in range(planes_ref.shape[0]):
        tail = planes_ref[n, part:, :].astype(F32)
        total = tail[0:1] + tail[1:2] + tail[2:3]
        after = jnp.exp(total) * carried + planes_ref[n, :part, :].astype(F32)
        carried = jnp.where(n < here, after, carried)
    for n in range(out_ref.shape[0]):
        out_ref[n] = carried
        own = states_ref[n, part : part + 1, :]
        carried = jnp.exp(own) * carried + states_ref[n, :part, :]


def incoming_state(here, planes, states):
    count, lines, width = states.shape
    return pl.pallas_call(
        incoming_kernel,
        out_shape=jax.ShapeDtypeStruct((count, lines - 8, width), F32),
        in_specs=[pl.BlockSpec(memory_space=pltpu.SMEM)] + vmem(2),
        out_specs=pl.BlockSpec(memory_space=pltpu.VMEM),
        cost_estimate=kernel_cost(2**19, 2**19, 2**12),
        name="incoming_state",
    )(here, planes, states)


def project_kernel(within_ref, carry_q_ref, state_ref, gate_ref, gain_ref, weight_ref, out_ref):
    retained = within_ref[...] + dot(carry_q_ref[...], state_ref[...].astype(BF16))
    center = jnp.mean(retained, axis=-1, keepdims=True)
    off = retained - center
    spread = jnp.mean(off * off, axis=-1, keepdims=True)
    normed = off * lax.rsqrt(spread + EPS) * gain_ref[...].astype(F32)
    gate = gate_ref[...].astype(F32)
    mixed = (gate * jax.nn.sigmoid(gate) * normed).astype(BF16)
    out_ref[...] = dot(mixed, weight_ref[...]).astype(BF16)


def project(within, carry_q, state, gate, gain, weight):
    rows, width = within.shape[0], weight.shape[1]
    return pl.pallas_call(
        project_kernel,
        out_shape=jax.ShapeDtypeStruct((rows, width), BF16),
        in_specs=vmem(6),
        out_specs=pl.BlockSpec(memory_space=pltpu.VMEM),
        cost_estimate=kernel_cost(2 * rows * 128 * (width + 128), 2**21, rows * 128),
        name="project",
    )(within, carry_q, state, gate, gain, weight)


CHUNKS = 4


def ffn_kernel(rows_ref, weight_ref, out_ref, held, sems):
    z, _, _, kinds, lines, hidden_width = weight_ref.shape
    each = z // CHUNKS
    depth = each * 4 * lines

    def copies(kind, n):
        span = pl.ds(n * each, each)
        return [
            pltpu.make_async_copy(
                weight_ref.at[span, y0, y1, kind],
                held.at[kind, span, y1, y0],
                sems.at[kind, n, 2 * y1 + y0],
            )
            for y1 in range(2)
            for y0 in range(2)
        ]

    for n in range(CHUNKS):
        for kind in (0, 1):
            for copy in copies(kind, n):
                copy.start()
    for n in range(CHUNKS):
        for copy in copies(2, n):
            copy.start()

    def block(kind, n):
        return held[kind, n * each : (n + 1) * each].reshape(depth, hidden_width)

    gate_sum = up_sum = None
    for n in range(CHUNKS):
        for kind in (0, 1):
            for copy in copies(kind, n):
                copy.wait()
        rows = rows_ref[:, n * depth : (n + 1) * depth]
        gate_part, up_part = dot(rows, block(0, n)), dot(rows, block(1, n))
        gate_sum = gate_part if gate_sum is None else gate_sum + gate_part
        up_sum = up_part if up_sum is None else up_sum + up_part
    hidden = (gate_sum * jax.nn.sigmoid(gate_sum) * up_sum).astype(BF16)
    for n in range(CHUNKS):
        for copy in copies(2, n):
            copy.wait()
        out_ref[:, n * depth : (n + 1) * depth] = dot_nt(hidden, block(2, n)).astype(BF16)


def feed_forward(rows, weights):
    count, width = rows.shape
    z, y0, y1, kinds, lines, hidden_width = weights.shape
    return pl.pallas_call(
        ffn_kernel,
        out_shape=jax.ShapeDtypeStruct((count, width), BF16),
        in_specs=[
            pl.BlockSpec(memory_space=pltpu.VMEM),
            pl.BlockSpec(memory_space=pl.ANY),
        ],
        out_specs=pl.BlockSpec(memory_space=pltpu.VMEM),
        scratch_shapes=[
            pltpu.VMEM((kinds, z, y1, y0, lines, hidden_width), BF16),
            pltpu.SemaphoreType.DMA((kinds, CHUNKS, 4)),
        ],
        cost_estimate=kernel_cost(6 * count * width * hidden_width, 2**23, count * hidden_width),
        name="feed_forward",
    )(rows, weights)


def moved(value, axes, place):
    lengths = [SIZES[a] for a in axes]
    pairs = []
    for y1 in range(lengths[0]):
        for y0 in range(lengths[1]):
            for c in range(lengths[2]):
                a, b, d = place(y1, y0, c)
                pairs.append(((y1 * 2 + y0) * 2 + c, (a * 2 + b) * 2 + d))
    return lax.ppermute(value, axes, pairs)


def exchange(tiles, axes):
    return lax.all_to_all(tiles, axes, split_axis=0, concat_axis=0, tiled=True)


def copies_to(value, axes, count):
    return exchange(jnp.broadcast_to(value, (count, *value.shape)), axes)


def gathered_weights(gate_weight, up_weight, down_weight):
    mine = jnp.concatenate([gate_weight, up_weight, down_weight.T], axis=0)
    lines, width = mine.shape
    axes = ("y1", "y0", "c")
    near = moved(mine, axes, lambda y1, y0, c: (y1, c, y0))
    far = moved(mine, axes, lambda y1, y0, c: (1 - y1, c, y0))
    upper = lax.axis_index("y1") == 1
    pair = jnp.stack([jnp.where(upper, far, near), jnp.where(upper, near, far)])
    whole = lax.all_gather(pair, (Z, "c"), axis=0)
    return whole.reshape(16, 2, 2, 3, lines // 3, width)


def local(
    stream,
    queries,
    keys_in,
    values_in,
    gate_in,
    log_decay,
    head_gain,
    out_weight,
    norm_gain,
    gate_weight,
    up_weight,
    down_weight,
):
    weights = gathered_weights(gate_weight, up_weight, down_weight)
    rows = queries.shape[0]
    within, carry_q, state = retention(
        queries, keys_in, values_in, log_decay.reshape(1, rows)
    )
    states = exchange(state, Y)
    planes = exchange(plane_state(states), Z)
    here = lax.axis_index(Z).astype(jnp.int32).reshape(1)
    entering = exchange(incoming_state(here, planes, states), Y)
    entering = entering.reshape(queries.shape[1], queries.shape[1])
    terms = project(within, carry_q, entering, gate_in, head_gain.reshape(1, -1), out_weight)
    width = terms.shape[1]
    attended = exchange(terms.reshape(8, rows // 8, width), TP).astype(F32).sum(axis=0)
    residual = stream.astype(F32) + attended
    normed = (
        residual
        * lax.rsqrt(jnp.mean(residual * residual, axis=-1, keepdims=True) + EPS)
        * norm_gain.astype(F32)
    ).astype(BF16)
    group_rows = copies_to(normed, GROUP, 8).reshape(rows, width)
    down_terms = feed_forward(group_rows, weights)
    mixer_out = exchange(down_terms.reshape(8, rows // 8, width), GROUP).astype(F32).sum(axis=0)
    return (residual + mixer_out).astype(BF16)


def solution(mesh):
    finer = Mesh(mesh.devices.reshape(*SIZES.values()), tuple(SIZES))
    return jax.shard_map(
        local,
        mesh=finer,
        in_specs=(
            P(SP + TP, None),
            P(SP, TP),
            P(SP, TP),
            P(SP, TP),
            P(SP, TP),
            P(SP, TP),
            P(TP),
            P(TP, None),
            P(),
            P(SP, TP),
            P(SP, TP),
            P(TP, SP),
        ),
        out_specs=P(SP + TP, None),
        check_vma=False,
    )
```

time: 274 us -> 154 us (0.56)
  waiting for transfers between devices: 90.1 us -> 36.7 us
  blocking collectives: 102 us -> 53.1 us
  matrix products: 20.7 us -> 0 us
  Pallas kernels: 0 us -> 16.3 us
  between operations: 28.5 us -> 13.5 us
  starting transfers between devices: 16.1 us -> 30.1 us
  local copies, waits for them, and re-layouts: 8.47 us -> 0.79 us
  other arithmetic: 5.84 us -> 2.86 us
    all_gather x2 -> x1, waiting for transfers between devices: 75.1 us -> 0.01 us  [gathered_weights(): whole = lax.all_gather(pair, (Z, 'c'), axis=0)]
    all_gather x3 -> x0, blocking collectives: 54.9 us -> none  [the longest x2 42.4 us: all_in_one(): both, at, found = (lax.all_gather(jnp.concatenate(lines), axis), 0, {})]
    dot_general x10 -> x0, matrix products: 20.7 us -> none  [the longest x1 7.39 us: local(): down_terms = jnp.dot(hidden, down_full, preferred_element_type=jnp.float32)]
    all_to_all x1 -> x2, waiting for transfers between devices: 15 us -> 32.2 us  [exchange(): return lax.all_to_all(tiles, axes, split_axis=0, concat_axis=0, tiled=True)]
    pallas_call x0 -> x5, Pallas kernels: none -> 16.3 us  [the longest x1 8.11 us: feed_forward(): pl.pallas_call(ffn_kernel, out_shape=jax.ShapeDtypeStruct((count, width),...]
    ppermute x0 -> x2, starting transfers between devices: none -> 7.94 us  [moved(): return lax.ppermute(value, axes, pairs)]
    all_to_all x2 -> x4, blocking collectives: 46.9 us -> 53.1 us  [exchange(): return lax.all_to_all(tiles, axes, split_axis=0, concat_axis=0, tiled=True)]
    all_to_all x1 -> x2, starting transfers between devices: 16.1 us -> 22.1 us  [exchange(): return lax.all_to_all(tiles, axes, split_axis=0, concat_axis=0, tiled=True)]
  transfers between devices with their start and end apart: 3 -> 5, of which waited for: 3 -> 4; matrix products, arithmetic and copies ran while one was open for 9% -> 0% of each run, Pallas kernels for 0% -> 5%
where the time goes in v1:
time: 154 us; the launch traced here: 153 us
  blocking collectives  53.1 us (34%)
  waiting for transfers between devices  36.7 us (24%)
  starting transfers between devices  30.1 us (20%)
  Pallas kernels  16.3 us (11%)
  between operations  13.5 us (9%)
  other arithmetic  2.86 us (2%)
    all_to_all x4, blocking collectives, exchange(): return lax.all_to_all(tiles, axes, split_axis=0, concat_axis=0, tiled=True)  53.1 us
    all_to_all x2, waiting for transfers between devices, exchange(): return lax.all_to_all(tiles, axes, split_axis=0, concat_axis=0, tiled=True)  32.2 us
    all_to_all x2, starting transfers between devices, exchange(): return lax.all_to_all(tiles, axes, split_axis=0, concat_axis=0, tiled=True)  22.1 us
    pallas_call x1, Pallas kernels, feed_forward(): pl.pallas_call(ffn_kernel, out_shape=jax.ShapeDtypeStruct((count, width),...  8.11 us
    ppermute x2, starting transfers between devices, moved(): return lax.ppermute(value, axes, pairs)  7.94 us
    ppermute x2, waiting for transfers between devices, moved(): return lax.ppermute(value, axes, pairs)  4.53 us
  transfers between devices with their start and end apart: 5, of which 4 were waited for; matrix products, arithmetic and copies ran while one was open for 0% of the time, Pallas kernels for 5%

profile of v1, /device:TPU:1, one launch (start us, length us, event | category | flops | bytes accessed | tf_op | source)
XLA Modules:
  0.0 153.3 jit_solution(3274136103168143189)
XLA Ops:
  6.5 0.0 all-gather.3.cloned.1.call-start
  6.5 0.9 pad_maximum_fusion.1
  7.4 6.0 %collective-permute-start = (bf16[96,704]{1,0:T(8,128)(2,1)S(1)}, bf16[96,704]{1,0:T(8,128)(2,1)S(1)}, u32[]{:S(2)}, u32[]{:S(2)}) collective-permute-start(bf16[96,704]{1,0:T(8,128)(2,1)S(1)} %pad_maximum_fusion.1), channel_id=1, source_target_pairs={{0,16},{1,24},{8,17},{9,25},{16,0},{17,8},{24,1},{25,9},{2,18},{3,... | collective-permute-start | bytes 405512 | tf_op jit(solution)/shard_map/ppermute | solution.py:242
  13.4 1.9 %collective-permute-start.1 = (bf16[96,704]{1,0:T(8,128)(2,1)S(1)}, bf16[96,704]{1,0:T(8,128)(2,1)S(1)}, u32[]{:S(2)}, u32[]{:S(2)}) collective-permute-start(bf16[96,704]{1,0:T(8,128)(2,1)S(1)} %pad_maximum_fusion.1), channel_id=1, source_target_pairs={{0,0},{1,8},{8,1},{9,9},{16,16},{17,24},{24,17},{25,25},{2,2},{3,1... | collective-permute-start | bytes 405512 | tf_op jit(solution)/shard_map/ppermute | solution.py:242
  15.4 1.4 collective-permute-done
  16.8 3.1 %collective-permute-done.1 = bf16[96,704]{1,0:T(8,128)(2,1)S(1)} collective-permute-done((bf16[96,704]{1,0:T(8,128)(2,1)S(1)}, bf16[96,704]{1,0:T(8,128)(2,1)S(1)}, u32[]{:S(2)}, u32[]{:S(2)}) %collective-permute-start.1) | collective-permute-done | bytes 135200 | tf_op jit(solution)/shard_map/ppermute | solution.py:242
  19.9 0.7 pad_maximum_fusion
  20.7 0.0 all-gather.3.cloned.1.call-update
  20.7 1.9 %retention.1 = (f32[256,128]{1,0:T(8,128)}, bf16[256,128]{1,0:T(8,128)(2,1)}, f32[4,40,128]{2,1,0:T(8,128)}) custom-call(bf16[256,128]{1,0:T(8,128)(2,1)} %q_ref.1, bf16[256,128]{1,0:T(8,128)(2,1)} %k_ref.1, bf16[256,128]{1,0:T(8,128)(2,1)} %v_ref.1, f32[1,256]{1,0:T(1,128)} %bitcast.19), custom_call_target="tpu_custom_call" | custom-call | flops 50331648 | bytes 1048576 | tf_op jit(solution)/shard_map/retention/pallas_call | solution.py:67
  22.6 8.5 %all_to_all.30.states_ref = f32[4,40,128]{2,1,0:T(8,128)} all-to-all(f32[4,40,128]{2,1,0:T(8,128)} %get-tuple-element.10), channel_id=1, replica_groups=mesh['z'=16,'y1'=2,'y0'=2,'x'=4,'c'=2] {'y1','y0'}, dimensions={0} | all-to-all | bytes 163840 | tf_op jit(solution)/shard_map/all_to_all | solution.py:246
  31.2 1.6 %plane_state.1 = bf16[16,48,128]{2,1,0:T(8,128)(2,1)} custom-call(f32[4,40,128]{2,1,0:T(8,128)} %all_to_all.30.states_ref), custom_call_target="tpu_custom_call" | custom-call | flops 262144 | bytes 262144 | tf_op jit(solution)/shard_map/plane_state/pallas_call | solution.py:107
  32.8 14.9 %all-to-all-start.1 = ((bf16[16,48,128]{2,1,0:T(8,128)(2,1)}), bf16[16,48,128]{2,1,0:T(8,128)(2,1)S(1)}, u32[]{:S(2)}, u32[]{:S(2)}) async-start(bf16[16,48,128]{2,1,0:T(8,128)(2,1)} %plane_state.1), calls=%async_computation.1 | async-start | bytes 393216 | tf_op jit(solution)/shard_map/all_to_all | solution.py:246
  47.7 17.2 %all-to-all-done.1.planes_ref = bf16[16,48,128]{2,1,0:T(8,128)(2,1)S(1)} async-done(((bf16[16,48,128]{2,1,0:T(8,128)(2,1)}), bf16[16,48,128]{2,1,0:T(8,128)(2,1)S(1)}, u32[]{:S(2)}, u32[]{:S(2)}) %all-to-all-start.1) | async-done | bytes 196640 | tf_op jit(solution)/shard_map/all_to_all | solution.py:246
  64.9 0.0 copy-start.1
  64.9 0.7 copy-done.1
  65.6 1.7 %incoming_state.1 = f32[4,32,128]{2,1,0:T(8,128)} custom-call(s32[1]{0:T(128)} %bitcast.1.here_ref, bf16[16,48,128]{2,1,0:T(8,128)(2,1)} %copy-done.1, f32[4,40,128]{2,1,0:T(8,128)} %all_to_all.30.states_ref), custom_call_target="tpu_custom_call" | custom-call | flops 524288 | bytes 524288 | tf_op jit(solution)/shard_map/incoming_state/pallas_call | solution.py:134
  67.3 0.0 copy-start.2
  67.3 8.6 %all_to_all.31 = f32[4,32,128]{2,1,0:T(8,128)} all-to-all(f32[4,32,128]{2,1,0:T(8,128)} %incoming_state.1), channel_id=1, replica_groups=mesh['z'=16,'y1'=2,'y0'=2,'x'=4,'c'=2] {'y1','y0'}, dimensions={0} | all-to-all | bytes 131072 | tf_op jit(solution)/shard_map/all_to_all | solution.py:246
  75.9 3.0 %project.1 = bf16[256,2048]{1,0:T(8,128)(2,1)} custom-call(f32[256,128]{1,0:T(8,128)} %get-tuple-element.8.within_ref, bf16[256,128]{1,0:T(8,128)(2,1)} %get-tuple-element.9.carry_q_ref, f32[128,128]{1,0:T(8,128)} %bitcast.17, bf16[256,128]{1,0:T(8,128)(2,1)} %gate_ref.1, bf16[1,128]{1,0:T(2,128)(2,1)} %bitcast.20, bf16[128,2048]{1,0:T(8,128)(2,1)} %weight_ref.1), custom_call_target="tpu_custom_call" | custom-call | flops 142606336 | bytes 2097152 | tf_op jit(solution)/shard_map/project/pallas_call | solution.py:157
  78.8 7.2 %all-to-all-start.3 = ((bf16[8,32,2048]{2,1,0:T(8,128)(2,1)}), bf16[8,32,2048]{2,1,0:T(8,128)(2,1)S(1)}, u32[]{:S(2)}, u32[]{:S(2)}) async-start(bf16[8,32,2048]{2,1,0:T(8,128)(2,1)} %bitcast.14), calls=%async_computation.3 | async-start | bytes 2097152 | tf_op jit(solution)/shard_map/all_to_all | solution.py:246
  86.0 0.0 copy-done.2
  86.1 15.0 %all-to-all-done.3 = bf16[8,32,2048]{2,1,0:T(8,128)(2,1)S(1)} async-done(((bf16[8,32,2048]{2,1,0:T(8,128)(2,1)}), bf16[8,32,2048]{2,1,0:T(8,128)(2,1)S(1)}, u32[]{:S(2)}, u32[]{:S(2)}) %all-to-all-start.3) | async-done | bytes 1048608 | tf_op jit(solution)/shard_map/all_to_all | solution.py:246
  101.0 0.1 convert_reduce_fusion.1
  101.2 0.0 copy-done
  101.2 0.1 multiply_reduce_fusion
  101.3 0.1 multiply_convert_fusion
  101.4 0.1 broadcast_in_dim.2
  101.6 17.9 %all_to_all.32 = bf16[8,32,2048]{2,1,0:T(8,128)(2,1)} all-to-all(bf16[8,32,2048]{2,1,0:T(8,128)(2,1)S(1)} %broadcast_in_dim.2), channel_id=1, replica_groups=mesh['z'=16,'y1'=2,'y0'=2,'x'=4,'c'=2] {'y0','x'}, dimensions={0} | all-to-all | bytes 2097152 | tf_op jit(solution)/shard_map/all_to_all | solution.py:246
  119.5 8.1 %feed_forward.1 = bf16[256,2048]{1,0:T(8,128)(2,1)} custom-call(bf16[256,2048]{1,0:T(8,128)(2,1)} %bitcast.15, bf16[16,2,2,3,32,704]{5,4,3,2,1,0:T(8,128)(2,1)} %bitcast.13), custom_call_target="tpu_custom_call" | custom-call | flops 2214592512 | bytes 8388608 | tf_op jit(solution)/shard_map/feed_forward/pallas_call | solution.py:217
  127.6 18.0 %all_to_all.33 = bf16[8,32,2048]{2,1,0:T(8,128)(2,1)S(1)} all-to-all(bf16[8,32,2048]{2,1,0:T(8,128)(2,1)} %bitcast.16), channel_id=1, replica_groups=mesh['z'=16,'y1'=2,'y0'=2,'x'=4,'c'=2] {'y0','x'}, dimensions={0} | all-to-all | bytes 2097152 | tf_op jit(solution)/shard_map/all_to_all | solution.py:246
  145.7 0.1 convert_reduce_fusion
  145.8 0.7 add_convert_fusion
  (5 shorter events, 0.0 us)
Async XLA Ops:
  6.5 113.0 %all-gather.3.cloned.1.call-start = ((), (), s32[]{:S(2)}) async-start(), calls=%async_computation.6 | async-start | bytes 9732096 | tf_op jit(solution)/shard_map/all_gather | solution.py:261
  7.4 9.4 %collective-permute-start = (bf16[96,704]{1,0:T(8,128)(2,1)S(1)}, bf16[96,704]{1,0:T(8,128)(2,1)S(1)}, u32[]{:S(2)}, u32[]{:S(2)}) collective-permute-start(bf16[96,704]{1,0:T(8,128)(2,1)S(1)} %pad_maximum_fusion.1), channel_id=1, source_target_pairs={{0,16},{1,24},{8,17},{9,25},{16,0},{17,8},{24,1},{25,9},{2,18},{3,... | collective-permute-start | bytes 405512 | tf_op jit(solution)/shard_map/ppermute | solution.py:242
  13.4 6.5 %collective-permute-start.1 = (bf16[96,704]{1,0:T(8,128)(2,1)S(1)}, bf16[96,704]{1,0:T(8,128)(2,1)S(1)}, u32[]{:S(2)}, u32[]{:S(2)}) collective-permute-start(bf16[96,704]{1,0:T(8,128)(2,1)S(1)} %pad_maximum_fusion.1), channel_id=1, source_target_pairs={{0,0},{1,8},{8,1},{9,9},{16,16},{17,24},{24,17},{25,25},{2,2},{3,1... | collective-permute-start | bytes 405512 | tf_op jit(solution)/shard_map/ppermute | solution.py:242
  32.8 32.2 %all-to-all-start.1 = ((bf16[16,48,128]{2,1,0:T(8,128)(2,1)}), bf16[16,48,128]{2,1,0:T(8,128)(2,1)S(1)}, u32[]{:S(2)}, u32[]{:S(2)}) async-start(bf16[16,48,128]{2,1,0:T(8,128)(2,1)} %plane_state.1), calls=%async_computation.1 | async-start | bytes 393216 | tf_op jit(solution)/shard_map/all_to_all | solution.py:246
  64.9 0.7 copy-start.1
  67.3 18.8 %copy-start.2 = (bf16[2048]{0:T(1024)(128)(2,1)S(1)}, bf16[2048]{0:T(1024)(128)(2,1)}, u32[]{:S(2)}) copy-start(bf16[2048]{0:T(1024)(128)(2,1)} %param.20) | copy-start | bytes 12292
  78.8 22.3 %copy-start = (bf16[32,2048]{1,0:T(8,128)(2,1)S(1)}, bf16[32,2048]{1,0:T(8,128)(2,1)}, u32[]{:S(2)}) copy-start(bf16[32,2048]{1,0:T(8,128)(2,1)} %param.12) | copy-start | bytes 393220
  78.8 22.2 %all-to-all-start.3 = ((bf16[8,32,2048]{2,1,0:T(8,128)(2,1)}), bf16[8,32,2048]{2,1,0:T(8,128)(2,1)S(1)}, u32[]{:S(2)}, u32[]{:S(2)}) async-start(bf16[8,32,2048]{2,1,0:T(8,128)(2,1)} %bitcast.14), calls=%async_computation.3 | async-start | bytes 2097152 | tf_op jit(solution)/shard_map/all_to_all | solution.py:246
Sparse Core Ops, SparseCore 0:
  20.8 89.8 all-gather.2

commit v2 on v1

--- a/solution.py
+++ b/solution.py
@@ -1,5 +1,3 @@
-import functools
-
 import jax
 import jax.numpy as jnp
 from jax import lax
@@ -7,6 +5,7 @@
 from jax.experimental.pallas import tpu as pltpu
 from jax.sharding import Mesh
 from jax.sharding import PartitionSpec as P
+
 
 Z, Y = "z", ("y1", "y0")
 SP = ("z", "y1", "y0")
@@ -103,7 +102,7 @@
 
 
 def plane_state(states):
-    count, lines, width = states.shape
+    _, lines, width = states.shape
     return pl.pallas_call(
         plane_kernel,
         out_shape=jax.ShapeDtypeStruct((16, lines - 8 + 16, width), BF16),
@@ -141,7 +140,7 @@
     )(here, planes, states)
 
 
-def project_kernel(within_ref, carry_q_ref, state_ref, gate_ref, gain_ref, weight_ref, out_ref):
+def mix_kernel(within_ref, carry_q_ref, state_ref, gate_ref, gain_ref, out_ref):
     retained = within_ref[...] + dot(carry_q_ref[...], state_ref[...].astype(BF16))
     center = jnp.mean(retained, axis=-1, keepdims=True)
     off = retained - center
@@ -149,26 +148,93 @@
     normed = off * lax.rsqrt(spread + EPS) * gain_ref[...].astype(F32)
     gate = gate_ref[...].astype(F32)
     mixed = (gate * jax.nn.sigmoid(gate) * normed).astype(BF16)
-    out_ref[...] = dot(mixed, weight_ref[...]).astype(BF16)
-
-
-def project(within, carry_q, state, gate, gain, weight):
-    rows, width = within.shape[0], weight.shape[1]
-    return pl.pallas_call(
-        project_kernel,
-        out_shape=jax.ShapeDtypeStruct((rows, width), BF16),
-        in_specs=vmem(6),
+    places, cores, blocks, lines, _ = out_ref.shape
+    for core in range(cores):
+        for n in range(blocks):
+            first = (n * cores + core) * lines
+            piece = mixed[first : first + lines]
+            for place in range(places):
+                out_ref[place, core, n] = piece
+
+
+def mix(within, carry_q, state, gate, gain):
+    rows, width = within.shape
+    return pl.pallas_call(
+        mix_kernel,
+        out_shape=jax.ShapeDtypeStruct((8, 2, 4, rows // 8, width), BF16),
+        in_specs=vmem(5),
         out_specs=pl.BlockSpec(memory_space=pltpu.VMEM),
-        cost_estimate=kernel_cost(2 * rows * 128 * (width + 128), 2**21, rows * 128),
-        name="project",
-    )(within, carry_q, state, gate, gain, weight)
+        cost_estimate=kernel_cost(2 * rows * width * width, 2**20, rows * width),
+        name="mix",
+    )(within, carry_q, state, gate, gain)
+
+
+def rows_kernel(
+    here_ref, mixed_ref, near_w_ref, far_w_ref, near_s_ref, far_s_ref, gain_ref, normed_ref, own_ref, residual
+):
+    halves, _, blocks, lines, head_dim = mixed_ref.shape
+    count, width = normed_ref.shape
+    x, c, y0 = here_ref[0], here_ref[1], here_ref[2]
+
+    def heads_of(core):
+        return jnp.concatenate(
+            [
+                jnp.concatenate(
+                    [mixed_ref[n, ((x + 4 - r) % 4) * 2 + core].reshape(count // halves, head_dim) for r in range(4)],
+                    axis=1,
+                )
+                for n in range(halves)
+            ],
+            axis=0,
+        )
+
+    near, far = heads_of(c), heads_of(1 - c)
+    step = width // 4
+    squares = jnp.zeros((count, 1), F32)
+    for n in range(4):
+        span = slice(n * step, (n + 1) * step)
+        rows = []
+        for half in range(halves):
+            for block in range(blocks):
+                at = (x + 4 - block) % 4
+                rows.append(jnp.where(y0 == half, near_s_ref[at, :, span], far_s_ref[at, :, span]))
+        part = (
+            jnp.concatenate(rows, axis=0).astype(F32)
+            + dot(near, near_w_ref[:, span])
+            + dot(far, far_w_ref[:, span])
+        )
+        residual[:, span] = part
+        squares += jnp.sum(part * part, axis=-1, keepdims=True)
+    factor = lax.rsqrt(squares / width + EPS)
+    for n in range(4):
+        span = slice(n * step, (n + 1) * step)
+        normed_ref[:, span] = (residual[:, span] * factor * gain_ref[:, span].astype(F32)).astype(BF16)
+    first = pl.multiple_of((y0 * blocks + x) * lines, lines)
+    own_ref[...] = residual[pl.ds(first, lines), :]
+
+
+def group_rows(here, mixed, near_w, far_w, near_s, far_s, gain):
+    lines, width = near_s.shape[1:]
+    count = 8 * lines
+    return pl.pallas_call(
+        rows_kernel,
+        out_shape=(
+            jax.ShapeDtypeStruct((count, width), BF16),
+            jax.ShapeDtypeStruct((lines, width), F32),
+        ),
+        in_specs=[pl.BlockSpec(memory_space=pltpu.SMEM)] + vmem(6),
+        out_specs=vmem(2),
+        scratch_shapes=[pltpu.VMEM((count, width), F32)],
+        cost_estimate=kernel_cost(2 * count * width * 1024, 2**23),
+        name="group_rows",
+    )(here, mixed, near_w, far_w, near_s, far_s, gain)
 
 
 CHUNKS = 4
 
 
 def ffn_kernel(rows_ref, weight_ref, out_ref, held, sems):
-    z, _, _, kinds, lines, hidden_width = weight_ref.shape
+    z, _, _, _, lines, hidden_width = weight_ref.shape
     each = z // CHUNKS
     depth = each * 4 * lines
 
@@ -242,12 +308,13 @@
     return lax.ppermute(value, axes, pairs)
 
 
+def shifted(value, axis, by):
+    length = SIZES[axis]
+    return lax.ppermute(value, axis, [(i, (i + by) % length) for i in range(length)])
+
+
 def exchange(tiles, axes):
     return lax.all_to_all(tiles, axes, split_axis=0, concat_axis=0, tiled=True)
-
-
-def copies_to(value, axes, count):
-    return exchange(jnp.broadcast_to(value, (count, *value.shape)), axes)
 
 
 def gathered_weights(gate_weight, up_weight, down_weight):
@@ -259,10 +326,10 @@
     upper = lax.axis_index("y1") == 1
     pair = jnp.stack([jnp.where(upper, far, near), jnp.where(upper, near, far)])
     whole = lax.all_gather(pair, (Z, "c"), axis=0)
-    return whole.reshape(16, 2, 2, 3, lines // 3, width)
-
-
-def local(
+    return whole.reshape(16, 2, 2, 3, lines // 3, width), pair
+
+
+def layer(
     stream,
     queries,
     keys_in,
@@ -276,27 +343,33 @@
     up_weight,
     down_weight,
 ):
-    weights = gathered_weights(gate_weight, up_weight, down_weight)
-    rows = queries.shape[0]
+    weights, tied = gathered_weights(gate_weight, up_weight, down_weight)
+    rows, width = queries.shape[0], stream.shape[1]
+    head_dim = queries.shape[1]
+    block = jnp.concatenate([out_weight, stream], axis=0)
+    block, _ = lax.optimization_barrier((block, tied))
+    found = [block] + [shifted(block, "x", r) for r in (1, 2, 3)]
+    near_w = jnp.concatenate([b[:head_dim] for b in found], axis=0)
+    near_s = jnp.stack([b[head_dim:] for b in found])
+    far_w = shifted(near_w, "c", 1)
+    far_s = shifted(near_s, "y0", 1)
     within, carry_q, state = retention(
         queries, keys_in, values_in, log_decay.reshape(1, rows)
     )
     states = exchange(state, Y)
-    planes = exchange(plane_state(states), Z)
+    packed = plane_state(states)
+    planes = exchange(packed, Z)
     here = lax.axis_index(Z).astype(jnp.int32).reshape(1)
-    entering = exchange(incoming_state(here, planes, states), Y)
+    entering = incoming_state(here, planes, states)
+    entering = exchange(entering, Y)
     entering = entering.reshape(queries.shape[1], queries.shape[1])
-    terms = project(within, carry_q, entering, gate_in, head_gain.reshape(1, -1), out_weight)
-    width = terms.shape[1]
-    attended = exchange(terms.reshape(8, rows // 8, width), TP).astype(F32).sum(axis=0)
-    residual = stream.astype(F32) + attended
-    normed = (
-        residual
-        * lax.rsqrt(jnp.mean(residual * residual, axis=-1, keepdims=True) + EPS)
-        * norm_gain.astype(F32)
-    ).astype(BF16)
-    group_rows = copies_to(normed, GROUP, 8).reshape(rows, width)
-    down_terms = feed_forward(group_rows, weights)
+    sent = mix(within, carry_q, entering, gate_in, head_gain.reshape(1, -1))
+    mixed = exchange(sent.reshape(16, *sent.shape[2:]), GROUP + ("c",))
+    here = jnp.stack([lax.axis_index(a).astype(jnp.int32) for a in ("x", "c", "y0")])
+    normed, residual = group_rows(
+        here, mixed.reshape(2, 8, *mixed.shape[1:]), near_w, far_w, near_s, far_s, norm_gain.reshape(1, -1)
+    )
+    down_terms = feed_forward(normed, weights)
     mixer_out = exchange(down_terms.reshape(8, rows // 8, width), GROUP).astype(F32).sum(axis=0)
     return (residual + mixer_out).astype(BF16)
 
@@ -304,7 +377,7 @@
 def solution(mesh):
     finer = Mesh(mesh.devices.reshape(*SIZES.values()), tuple(SIZES))
     return jax.shard_map(
-        local,
+        layer,
         mesh=finer,
         in_specs=(
             P(SP + TP, None),

time: 154 us -> 147 us (0.955)
  blocking collectives: 53.1 us -> 19 us
  starting transfers between devices: 30.1 us -> 54.1 us
  waiting for transfers between devices: 36.7 us -> 28.6 us
  local copies, waits for them, and re-layouts: 0.79 us -> 6.18 us
  Pallas kernels: 16.3 us -> 20.6 us
    all_to_all x4 -> x1, blocking collectives: 53.1 us -> 19 us  [exchange(): return lax.all_to_all(tiles, axes, split_axis=0, concat_axis=0, tiled=True)]
    ppermute x0 -> x5, starting transfers between devices: none -> 15.2 us  [shifted(): lax.ppermute(value, axis, [(i, (i + by) % length) for i in range(length)])]
    all_to_all x2 -> x4, waiting for transfers between devices: 32.2 us -> 22.3 us  [exchange(): return lax.all_to_all(tiles, axes, split_axis=0, concat_axis=0, tiled=True)]
    all_to_all x2 -> x4, starting transfers between devices: 22.1 us -> 30.9 us  [exchange(): return lax.all_to_all(tiles, axes, split_axis=0, concat_axis=0, tiled=True)]
    pallas_call x1 -> x2, Pallas kernels: 2.97 us -> 7.25 us  [the longest x1 5.09 us: group_rows(): pl.pallas_call(rows_kernel, out_shape=(jax.ShapeDtypeStruct((count, width...]
    unnamed x6 -> x22, local copies, waits for them, and re-layouts: 0.68 us -> 3.58 us
    another operation x0 -> x4, local copies, waits for them, and re-layouts: none -> 1.85 us  [layer(): near_s = jnp.stack([b[head_dim:] for b in found])]
    ppermute x0 -> x5, waiting for transfers between devices: none -> 1.78 us  [shifted(): lax.ppermute(value, axis, [(i, (i + by) % length) for i in range(length)])]
  transfers between devices with their start and end apart: 5 -> 12, of which waited for: 4 -> 7; matrix products, arithmetic and copies ran while one was open for 0% -> 3% of each run, Pallas kernels for 5% -> 8%
where the time goes in v2:
time: 147 us; the launch traced here: 146 us
  starting transfers between devices  54.1 us (37%)
  waiting for transfers between devices  28.6 us (19%)
  Pallas kernels  20.6 us (14%)
  blocking collectives  19 us (13%)
  between operations  13.7 us (9%)
  local copies, waits for them, and re-layouts  6.18 us (4%)
  other arithmetic  4.24 us (3%)
    all_to_all x4, starting transfers between devices, exchange(): return lax.all_to_all(tiles, axes, split_axis=0, concat_axis=0, tiled=True)  30.9 us
    all_to_all x4, waiting for transfers between devices, exchange(): return lax.all_to_all(tiles, axes, split_axis=0, concat_axis=0, tiled=True)  22.3 us
    all_to_all x1, blocking collectives, exchange(): return lax.all_to_all(tiles, axes, split_axis=0, concat_axis=0, tiled=True)  19 us
    ppermute x5, starting transfers between devices, shifted(): lax.ppermute(value, axis, [(i, (i + by) % length) for i in range(length)])  15.2 us
    pallas_call x1, Pallas kernels, feed_forward(): pl.pallas_call(ffn_kernel, out_shape=jax.ShapeDtypeStruct((count, width),...  8.13 us
    ppermute x2, starting transfers between devices, moved(): return lax.ppermute(value, axes, pairs)  7.94 us
    pallas_call x1, Pallas kernels, group_rows(): pl.pallas_call(rows_kernel, out_shape=(jax.ShapeDtypeStruct((count, width...  5.09 us
    ppermute x2, waiting for transfers between devices, moved(): return lax.ppermute(value, axes, pairs)  4.53 us
  transfers between devices with their start and end apart: 12, of which 7 were waited for; matrix products, arithmetic and copies ran while one was open for 3% of the time, Pallas kernels for 8%

profile of v2, /device:TPU:1, one launch (start us, length us, event | category | flops | bytes accessed | tf_op | source)
XLA Modules:
  0.0 146.3 jit_solution(6048646927807997841)
XLA Ops:
  6.5 0.9 pad_maximum_fusion.4
  7.5 6.0 %collective-permute-start = (bf16[96,704]{1,0:T(8,128)(2,1)S(1)}, bf16[96,704]{1,0:T(8,128)(2,1)S(1)}, u32[]{:S(2)}, u32[]{:S(2)}) collective-permute-start(bf16[96,704]{1,0:T(8,128)(2,1)S(1)} %pad_maximum_fusion.4), channel_id=1, source_target_pairs={{0,16},{1,24},{8,17},{9,25},{16,0},{17,8},{24,1},{25,9},{2,18},{3,... | collective-permute-start | bytes 405512 | tf_op jit(solution)/shard_map/ppermute | solution.py:308
  13.5 1.9 %collective-permute-start.1 = (bf16[96,704]{1,0:T(8,128)(2,1)S(1)}, bf16[96,704]{1,0:T(8,128)(2,1)S(1)}, u32[]{:S(2)}, u32[]{:S(2)}) collective-permute-start(bf16[96,704]{1,0:T(8,128)(2,1)S(1)} %pad_maximum_fusion.4), channel_id=1, source_target_pairs={{0,0},{1,8},{8,1},{9,9},{16,16},{17,24},{24,17},{25,25},{2,2},{3,1... | collective-permute-start | bytes 405512 | tf_op jit(solution)/shard_map/ppermute | solution.py:308
  15.4 1.4 collective-permute-done
  16.9 3.1 %collective-permute-done.1 = bf16[96,704]{1,0:T(8,128)(2,1)S(1)} collective-permute-done((bf16[96,704]{1,0:T(8,128)(2,1)S(1)}, bf16[96,704]{1,0:T(8,128)(2,1)S(1)}, u32[]{:S(2)}, u32[]{:S(2)}) %collective-permute-start.1) | collective-permute-done | bytes 135200 | tf_op jit(solution)/shard_map/ppermute | solution.py:308
  20.0 0.7 pad_maximum_fusion.3
  20.8 1.0 pad_maximum_fusion.1
  21.7 4.4 %collective-permute-start.4 = (bf16[160,2048]{1,0:T(8,128)(2,1)S(1)}, bf16[160,2048]{1,0:T(8,128)(2,1)S(1)}, u32[]{:S(2)}, u32[]{:S(2)}) collective-permute-start(bf16[160,2048]{1,0:T(8,128)(2,1)S(1)} %pad_maximum_fusion.1), channel_id=1, source_target_pairs={{0,6},{2,0},{4,2},{6,4},{1,7},{3,1},{5,3},{7,5},{8,14},{10,8},{12,... | collective-permute-start | bytes 1966088 | tf_op jit(solution)/shard_map/ppermute | solution.py:313
  26.1 2.4 %collective-permute-start.3 = (bf16[160,2048]{1,0:T(8,128)(2,1)S(1)}, bf16[160,2048]{1,0:T(8,128)(2,1)S(1)}, u32[]{:S(2)}, u32[]{:S(2)}) collective-permute-start(bf16[160,2048]{1,0:T(8,128)(2,1)S(1)} %pad_maximum_fusion.1), channel_id=1, source_target_pairs={{0,4},{2,6},{4,0},{6,2},{1,5},{3,7},{5,1},{7,3},{8,12},{10,14},{12... | collective-permute-start | bytes 1966088 | tf_op jit(solution)/shard_map/ppermute | solution.py:313
  28.5 2.5 %collective-permute-start.2 = (bf16[160,2048]{1,0:T(8,128)(2,1)S(1)}, bf16[160,2048]{1,0:T(8,128)(2,1)S(1)}, u32[]{:S(2)}, u32[]{:S(2)}) collective-permute-start(bf16[160,2048]{1,0:T(8,128)(2,1)S(1)} %pad_maximum_fusion.1), channel_id=1, source_target_pairs={{0,2},{2,4},{4,6},{6,0},{1,3},{3,5},{5,7},{7,1},{8,10},{10,12},{12... | collective-permute-start | bytes 1966088 | tf_op jit(solution)/shard_map/ppermute | solution.py:313
  31.1 1.9 %retention.1 = (f32[256,128]{1,0:T(8,128)}, bf16[256,128]{1,0:T(8,128)(2,1)}, f32[4,40,128]{2,1,0:T(8,128)}) custom-call(bf16[256,128]{1,0:T(8,128)(2,1)} %q_ref.1, bf16[256,128]{1,0:T(8,128)(2,1)} %k_ref.1, bf16[256,128]{1,0:T(8,128)(2,1)} %v_ref.1, f32[1,256]{1,0:T(1,128)} %bitcast.30), custom_call_target="tpu_custom_call" | custom-call | flops 50331648 | bytes 1048576 | tf_op jit(solution)/shard_map/retention/pallas_call | solution.py:66
  33.0 3.3 %all-to-all-start = ((f32[4,40,128]{2,1,0:T(8,128)}), f32[4,40,128]{2,1,0:T(8,128)S(1)}, u32[]{:S(2)}, u32[]{:S(2)}) async-start(f32[4,40,128]{2,1,0:T(8,128)} %get-tuple-element.13), calls=%async_computation | async-start | bytes 163840 | tf_op jit(solution)/shard_map/all_to_all | solution.py:317
  36.3 4.8 %all-to-all-done.states_ref = f32[4,40,128]{2,1,0:T(8,128)S(1)} async-done(((f32[4,40,128]{2,1,0:T(8,128)}), f32[4,40,128]{2,1,0:T(8,128)S(1)}, u32[]{:S(2)}, u32[]{:S(2)}) %all-to-all-start) | async-done | bytes 81952 | tf_op jit(solution)/shard_map/all_to_all | solution.py:317
  41.7 1.6 %plane_state.1 = bf16[16,48,128]{2,1,0:T(8,128)(2,1)} custom-call(f32[4,40,128]{2,1,0:T(8,128)} %copy-done.4), custom_call_target="tpu_custom_call" | custom-call | flops 262144 | bytes 262144 | tf_op jit(solution)/shard_map/plane_state/pallas_call | solution.py:106
  43.3 14.9 %all-to-all-start.1 = ((bf16[16,48,128]{2,1,0:T(8,128)(2,1)}), bf16[16,48,128]{2,1,0:T(8,128)(2,1)S(1)}, u32[]{:S(2)}, u32[]{:S(2)}) async-start(bf16[16,48,128]{2,1,0:T(8,128)(2,1)} %plane_state.1), calls=%async_computation.1 | async-start | bytes 393216 | tf_op jit(solution)/shard_map/all_to_all | solution.py:317
  58.4 1.8 %collective-permute-done.2 = bf16[160,2048]{1,0:T(8,128)(2,1)S(1)} collective-permute-done((bf16[160,2048]{1,0:T(8,128)(2,1)S(1)}, bf16[160,2048]{1,0:T(8,128)(2,1)S(1)}, u32[]{:S(2)}, u32[]{:S(2)}) %collective-permute-start.2) | collective-permute-done | bytes 655392 | tf_op jit(solution)/shard_map/ppermute | solution.py:313
  60.2 0.8 copy-done.6
  61.2 2.5 %collective-permute-start.5 = (bf16[512,2048]{1,0:T(8,128)(2,1)S(1)}, bf16[512,2048]{1,0:T(8,128)(2,1)}, u32[]{:S(2)}, u32[]{:S(2)}) collective-permute-start(bf16[512,2048]{1,0:T(8,128)(2,1)S(1)} %pad_maximum_fusion.near_w_ref), channel_id=1, source_target_pairs={{0,1},{1,0},{2,3},{3,2},{4,5},{5,4},{6,7},{7,6},{8,9},{9,8},{10,11... | collective-permute-start | bytes 6291464 | tf_op jit(solution)/shard_map/ppermute | solution.py:313
  63.8 0.9 slice_bitcast_fusion.1
  64.7 0.9 slice_bitcast_fusion.2
  65.6 8.0 %all-to-all-done.1.planes_ref = bf16[16,48,128]{2,1,0:T(8,128)(2,1)S(1)} async-done(((bf16[16,48,128]{2,1,0:T(8,128)(2,1)}), bf16[16,48,128]{2,1,0:T(8,128)(2,1)S(1)}, u32[]{:S(2)}, u32[]{:S(2)}) %all-to-all-start.1) | async-done | bytes 196640 | tf_op jit(solution)/shard_map/all_to_all | solution.py:317
  74.3 1.7 %incoming_state.1 = f32[4,32,128]{2,1,0:T(8,128)} custom-call(s32[1]{0:T(128)} %bitcast.4.here_ref, bf16[16,48,128]{2,1,0:T(8,128)(2,1)} %copy-done.3, f32[4,40,128]{2,1,0:T(8,128)} %copy-done.4), custom_call_target="tpu_custom_call" | custom-call | flops 524288 | bytes 524288 | tf_op jit(solution)/shard_map/incoming_state/pallas_call | solution.py:133
  76.0 3.3 %all-to-all-start.2 = ((f32[4,32,128]{2,1,0:T(8,128)}), f32[4,32,128]{2,1,0:T(8,128)S(1)}, u32[]{:S(2)}, u32[]{:S(2)}) async-start(f32[4,32,128]{2,1,0:T(8,128)} %incoming_state.1), calls=%async_computation.2 | async-start | bytes 131072 | tf_op jit(solution)/shard_map/all_to_all | solution.py:317
  79.4 3.3 %collective-permute-start.6 = (bf16[4,32,2048]{2,1,0:T(8,128)(2,1)S(1)}, bf16[4,32,2048]{2,1,0:T(8,128)(2,1)}, u32[]{:S(2)}, u32[]{:S(2)}) collective-permute-start(bf16[4,32,2048]{2,1,0:T(8,128)(2,1)S(1)} %pad_maximum_fusion.2.near_s_ref), channel_id=1, source_target_pairs={{0,8},{8,0},{1,9},{9,1},{2,10},{10,2},{3,11},{11,3},{4,12},{12,4},... | collective-permute-start | bytes 1572872 | tf_op jit(solution)/shard_map/ppermute | solution.py:313
  82.7 1.1 all-to-all-done.2
  84.4 2.2 %mix.1 = bf16[8,2,4,32,128]{4,3,2,1,0:T(8,128)(2,1)} custom-call(f32[256,128]{1,0:T(8,128)} %get-tuple-element.11.within_ref, bf16[256,128]{1,0:T(8,128)(2,1)} %get-tuple-element.12.carry_q_ref, f32[128,128]{1,0:T(8,128)} %bitcast.28, bf16[256,128]{1,0:T(8,128)(2,1)} %gate_ref.1, bf16[1,128]{1,0:T(2,128)(2,1)} %bitcast.31), custom_call_target="tpu_custom_call" | custom-call | flops 8388608 | bytes 1048576 | tf_op jit(solution)/shard_map/mix/pallas_call | solution.py:162
  86.6 9.4 %all-to-all-start.3 = ((bf16[16,4,32,128]{3,2,1,0:T(8,128)(2,1)}), bf16[16,4,32,128]{3,2,1,0:T(8,128)(2,1)S(1)}, u32[]{:S(2)}, u32[]{:S(2)}) async-start(bf16[16,4,32,128]{3,2,1,0:T(8,128)(2,1)} %bitcast.27), calls=%async_computation.3 | async-start | bytes 1048576 | tf_op jit(solution)/shard_map/all_to_all | solution.py:317
  97.2 8.4 %all-to-all-done.3 = bf16[16,4,32,128]{3,2,1,0:T(8,128)(2,1)S(1)} async-done(((bf16[16,4,32,128]{3,2,1,0:T(8,128)(2,1)}), bf16[16,4,32,128]{3,2,1,0:T(8,128)(2,1)S(1)}, u32[]{:S(2)}, u32[]{:S(2)}) %all-to-all-start.3) | async-done | bytes 524320 | tf_op jit(solution)/shard_map/all_to_all | solution.py:317
  105.6 0.8 copy-done.2
  106.4 5.1 %group_rows.1 = (bf16[256,2048]{1,0:T(8,128)(2,1)}, f32[32,2048]{1,0:T(8,128)}) custom-call(s32[3]{0:T(128)} %pad_add_fusion.here_ref, bf16[2,8,4,32,128]{4,3,2,1,0:T(8,128)(2,1)} %bitcast.26, bf16[512,2048]{1,0:T(8,128)(2,1)} %copy-done, bf16[512,2048]{1,0:T(8,128)(2,1)} %collective-permute-done.5.far_w_ref, bf16[4,32,2048]{2,1,0:T(8,128)(2,1)} %copy-done.1, ...), custom_call_target="tpu_custom_call" | custom-call | flops 1073741824 | bytes 8388608 | tf_op jit(solution)/shard_map/group_rows/pallas_call | solution.py:219
  111.5 8.1 %feed_forward.1 = bf16[256,2048]{1,0:T(8,128)(2,1)} custom-call(bf16[256,2048]{1,0:T(8,128)(2,1)} %get-tuple-element.16.rows_ref, bf16[16,2,2,3,32,704]{5,4,3,2,1,0:T(8,128)(2,1)} %bitcast.24), custom_call_target="tpu_custom_call" | custom-call | flops 2214592512 | bytes 8388608 | tf_op jit(solution)/shard_map/feed_forward/pallas_call | solution.py:283
  119.6 19.0 %all_to_all.25 = bf16[8,32,2048]{2,1,0:T(8,128)(2,1)S(1)} all-to-all(bf16[8,32,2048]{2,1,0:T(8,128)(2,1)} %bitcast.25), channel_id=1, replica_groups=mesh['z'=16,'y1'=2,'y0'=2,'x'=4,'c'=2] {'y0','x'}, dimensions={0} | all-to-all | bytes 2097152 | tf_op jit(solution)/shard_map/all_to_all | solution.py:317
  (40 shorter events, 4.4 us)
Async XLA Ops:
  6.5 14.2 %copy-start.7 = (bf16[128,2048]{1,0:T(8,128)(2,1)S(1)}, bf16[128,2048]{1,0:T(8,128)(2,1)}, u32[]{:S(2)}) copy-start(bf16[128,2048]{1,0:T(8,128)(2,1)} %param.19) | copy-start | bytes 1572868
  6.5 105.0 %all-gather.3.cloned.1.call-start = ((), (), s32[]{:S(2)}) async-start(), calls=%async_computation.5 | async-start | bytes 9732096 | tf_op jit(solution)/shard_map/all_gather | solution.py:328
  7.5 9.4 %collective-permute-start = (bf16[96,704]{1,0:T(8,128)(2,1)S(1)}, bf16[96,704]{1,0:T(8,128)(2,1)S(1)}, u32[]{:S(2)}, u32[]{:S(2)}) collective-permute-start(bf16[96,704]{1,0:T(8,128)(2,1)S(1)} %pad_maximum_fusion.4), channel_id=1, source_target_pairs={{0,16},{1,24},{8,17},{9,25},{16,0},{17,8},{24,1},{25,9},{2,18},{3,... | collective-permute-start | bytes 405512 | tf_op jit(solution)/shard_map/ppermute | solution.py:308
  13.5 6.5 %collective-permute-start.1 = (bf16[96,704]{1,0:T(8,128)(2,1)S(1)}, bf16[96,704]{1,0:T(8,128)(2,1)S(1)}, u32[]{:S(2)}, u32[]{:S(2)}) collective-permute-start(bf16[96,704]{1,0:T(8,128)(2,1)S(1)} %pad_maximum_fusion.4), channel_id=1, source_target_pairs={{0,0},{1,8},{8,1},{9,9},{16,16},{17,24},{24,17},{25,25},{2,2},{3,1... | collective-permute-start | bytes 405512 | tf_op jit(solution)/shard_map/ppermute | solution.py:308
  21.7 36.6 %collective-permute-start.4 = (bf16[160,2048]{1,0:T(8,128)(2,1)S(1)}, bf16[160,2048]{1,0:T(8,128)(2,1)S(1)}, u32[]{:S(2)}, u32[]{:S(2)}) collective-permute-start(bf16[160,2048]{1,0:T(8,128)(2,1)S(1)} %pad_maximum_fusion.1), channel_id=1, source_target_pairs={{0,6},{2,0},{4,2},{6,4},{1,7},{3,1},{5,3},{7,5},{8,14},{10,8},{12,... | collective-permute-start | bytes 1966088 | tf_op jit(solution)/shard_map/ppermute | solution.py:313
  26.1 32.3 %collective-permute-start.3 = (bf16[160,2048]{1,0:T(8,128)(2,1)S(1)}, bf16[160,2048]{1,0:T(8,128)(2,1)S(1)}, u32[]{:S(2)}, u32[]{:S(2)}) collective-permute-start(bf16[160,2048]{1,0:T(8,128)(2,1)S(1)} %pad_maximum_fusion.1), channel_id=1, source_target_pairs={{0,4},{2,6},{4,0},{6,2},{1,5},{3,7},{5,1},{7,3},{8,12},{10,14},{12... | collective-permute-start | bytes 1966088 | tf_op jit(solution)/shard_map/ppermute | solution.py:313
  28.5 31.7 %collective-permute-start.2 = (bf16[160,2048]{1,0:T(8,128)(2,1)S(1)}, bf16[160,2048]{1,0:T(8,128)(2,1)S(1)}, u32[]{:S(2)}, u32[]{:S(2)}) collective-permute-start(bf16[160,2048]{1,0:T(8,128)(2,1)S(1)} %pad_maximum_fusion.1), channel_id=1, source_target_pairs={{0,2},{2,4},{4,6},{6,0},{1,3},{3,5},{5,7},{7,1},{8,10},{10,12},{12... | collective-permute-start | bytes 1966088 | tf_op jit(solution)/shard_map/ppermute | solution.py:313
  33.0 8.1 %all-to-all-start = ((f32[4,40,128]{2,1,0:T(8,128)}), f32[4,40,128]{2,1,0:T(8,128)S(1)}, u32[]{:S(2)}, u32[]{:S(2)}) async-start(f32[4,40,128]{2,1,0:T(8,128)} %get-tuple-element.13), calls=%async_computation | async-start | bytes 163840 | tf_op jit(solution)/shard_map/all_to_all | solution.py:317
  41.1 0.6 copy-start.4
  43.3 30.3 %all-to-all-start.1 = ((bf16[16,48,128]{2,1,0:T(8,128)(2,1)}), bf16[16,48,128]{2,1,0:T(8,128)(2,1)S(1)}, u32[]{:S(2)}, u32[]{:S(2)}) async-start(bf16[16,48,128]{2,1,0:T(8,128)(2,1)} %plane_state.1), calls=%async_computation.1 | async-start | bytes 393216 | tf_op jit(solution)/shard_map/all_to_all | solution.py:317
  58.4 1.8 %copy-start.5 = (bf16[160,2048]{1,0:T(8,128)(2,1)}, bf16[160,2048]{1,0:T(8,128)(2,1)S(1)}, u32[]{:S(2)}) copy-start(bf16[160,2048]{1,0:T(8,128)(2,1)S(1)} %collective-permute-done.3) | copy-start | bytes 1966084
  60.2 0.8 copy-start.6
  61.2 25.4 %copy-start = (bf16[512,2048]{1,0:T(8,128)(2,1)}, bf16[512,2048]{1,0:T(8,128)(2,1)S(1)}, u32[]{:S(2)}) copy-start(bf16[512,2048]{1,0:T(8,128)(2,1)S(1)} %pad_maximum_fusion.near_w_ref) | copy-start | bytes 6291460
  61.2 34.8 %copy-start.10 = (bf16[2048]{0:T(1024)(128)(2,1)S(1)}, bf16[2048]{0:T(1024)(128)(2,1)}, u32[]{:S(2)}) copy-start(bf16[2048]{0:T(1024)(128)(2,1)} %param.20) | copy-start | bytes 12292
  61.2 44.4 %collective-permute-start.5 = (bf16[512,2048]{1,0:T(8,128)(2,1)S(1)}, bf16[512,2048]{1,0:T(8,128)(2,1)}, u32[]{:S(2)}, u32[]{:S(2)}) collective-permute-start(bf16[512,2048]{1,0:T(8,128)(2,1)S(1)} %pad_maximum_fusion.near_w_ref), channel_id=1, source_target_pairs={{0,1},{1,0},{2,3},{3,2},{4,5},{5,4},{6,7},{7,6},{8,9},{9,8},{10,11... | collective-permute-start | bytes 6291464 | tf_op jit(solution)/shard_map/ppermute | solution.py:313
  73.7 0.7 copy-start.3
  76.0 7.8 %all-to-all-start.2 = ((f32[4,32,128]{2,1,0:T(8,128)}), f32[4,32,128]{2,1,0:T(8,128)S(1)}, u32[]{:S(2)}, u32[]{:S(2)}) async-start(f32[4,32,128]{2,1,0:T(8,128)} %incoming_state.1), calls=%async_computation.2 | async-start | bytes 131072 | tf_op jit(solution)/shard_map/all_to_all | solution.py:317
  79.4 26.2 %copy-start.1 = (bf16[4,32,2048]{2,1,0:T(8,128)(2,1)}, bf16[4,32,2048]{2,1,0:T(8,128)(2,1)S(1)}, u32[]{:S(2)}) copy-start(bf16[4,32,2048]{2,1,0:T(8,128)(2,1)S(1)} %pad_maximum_fusion.2.near_s_ref) | copy-start | bytes 1572868
  79.4 17.8 %collective-permute-start.6 = (bf16[4,32,2048]{2,1,0:T(8,128)(2,1)S(1)}, bf16[4,32,2048]{2,1,0:T(8,128)(2,1)}, u32[]{:S(2)}, u32[]{:S(2)}) collective-permute-start(bf16[4,32,2048]{2,1,0:T(8,128)(2,1)S(1)} %pad_maximum_fusion.2.near_s_ref), channel_id=1, source_target_pairs={{0,8},{8,0},{1,9},{9,1},{2,10},{10,2},{3,11},{11,3},{4,12},{12,4},... | collective-permute-start | bytes 1572872 | tf_op jit(solution)/shard_map/ppermute | solution.py:313
  83.8 0.6 copy-start.8
  86.6 19.0 %all-to-all-start.3 = ((bf16[16,4,32,128]{3,2,1,0:T(8,128)(2,1)}), bf16[16,4,32,128]{3,2,1,0:T(8,128)(2,1)S(1)}, u32[]{:S(2)}, u32[]{:S(2)}) async-start(bf16[16,4,32,128]{3,2,1,0:T(8,128)(2,1)} %bitcast.27), calls=%async_computation.3 | async-start | bytes 1048576 | tf_op jit(solution)/shard_map/all_to_all | solution.py:317
  105.6 0.8 copy-start.2
  119.6 19.2 %copy-start.9 = (f32[32,2048]{1,0:T(8,128)S(1)}, f32[32,2048]{1,0:T(8,128)}, u32[]{:S(2)}) copy-start(f32[32,2048]{1,0:T(8,128)} %get-tuple-element.15) | copy-start | bytes 786436
Sparse Core Ops, SparseCore 0:
  20.9 89.6 all-gather.2

commit v3 on v2

--- a/solution.py
+++ b/solution.py
@@ -7,11 +7,12 @@
 from jax.sharding import PartitionSpec as P
 
 
-Z, Y = "z", ("y1", "y0")
-SP = ("z", "y1", "y0")
+Z, Y = ("zh", "zl"), ("y1", "y0")
+NEAR = ("zl",) + Y
+SP = Z + Y
 TP = ("x", "c")
 GROUP = ("y0", "x")
-SIZES = {"z": 16, "y1": 2, "y0": 2, "x": 4, "c": 2}
+SIZES = {"zh": 4, "zl": 4, "y1": 2, "y0": 2, "x": 4, "c": 2}
 EPS = 1e-6
 F32, BF16 = jnp.float32, jnp.bfloat16
 
@@ -62,13 +63,13 @@
 
 def retention(q, k, v, decay):
     rows, head_dim = q.shape
-    part = head_dim // 4
+    part = head_dim // 16
     return pl.pallas_call(
         retention_kernel,
         out_shape=(
             jax.ShapeDtypeStruct((rows, head_dim), F32),
             jax.ShapeDtypeStruct((rows, head_dim), BF16),
-            jax.ShapeDtypeStruct((4, part + 8, head_dim), F32),
+            jax.ShapeDtypeStruct((16, part + 8, head_dim), F32),
         ),
         in_specs=vmem(4),
         out_specs=vmem(3),
@@ -77,58 +78,44 @@
     )(q, k, v, decay)
 
 
-def plane_kernel(states_ref, out_ref):
+def joined_kernel(states_ref, out_ref):
     part = states_ref.shape[1] - 8
     state = states_ref[0, :part, :]
-    total = states_ref[0, part : part + 1, :]
+    total = states_ref[0, part:, :]
     for n in range(1, states_ref.shape[0]):
-        own = states_ref[n, part : part + 1, :]
+        own = states_ref[n, part:, :]
         state = jnp.exp(own) * state + states_ref[n, :part, :]
         total = total + own
-    high = total.astype(BF16)
-    rest = total - high.astype(F32)
-    mid = rest.astype(BF16)
-    low = (rest - mid.astype(F32)).astype(BF16)
-    line = lax.broadcasted_iota(jnp.int32, (16, total.shape[1]), 0)
-    spread = jnp.where(
-        line == 0,
-        high.astype(F32),
-        jnp.where(line == 1, mid.astype(F32), jnp.where(line == 2, low.astype(F32), 0.0)),
-    ).astype(BF16)
-    packed = state.astype(BF16)
     for n in range(out_ref.shape[0]):
-        out_ref[n, :part, :] = packed
-        out_ref[n, part:, :] = spread
-
-
-def plane_state(states):
+        out_ref[n, :part, :] = state
+        out_ref[n, part:, :] = total
+
+
+def joined_state(states):
     _, lines, width = states.shape
     return pl.pallas_call(
-        plane_kernel,
-        out_shape=jax.ShapeDtypeStruct((16, lines - 8 + 16, width), BF16),
+        joined_kernel,
+        out_shape=jax.ShapeDtypeStruct((4, lines, width), F32),
         in_specs=vmem(1),
         out_specs=pl.BlockSpec(memory_space=pltpu.VMEM),
         cost_estimate=kernel_cost(2**18, 2**18, 2**10),
-        name="plane_state",
+        name="joined_state",
     )(states)
 
 
-def incoming_kernel(here_ref, planes_ref, states_ref, out_ref):
+def incoming_kernel(here_ref, joined_ref, states_ref, out_ref):
     part = out_ref.shape[1]
     here = here_ref[0]
     carried = jnp.zeros(out_ref.shape[1:], F32)
-    for n in range(planes_ref.shape[0]):
-        tail = planes_ref[n, part:, :].astype(F32)
-        total = tail[0:1] + tail[1:2] + tail[2:3]
-        after = jnp.exp(total) * carried + planes_ref[n, :part, :].astype(F32)
+    for n in range(joined_ref.shape[0]):
+        after = jnp.exp(joined_ref[n, part:, :]) * carried + joined_ref[n, :part, :]
         carried = jnp.where(n < here, after, carried)
     for n in range(out_ref.shape[0]):
         out_ref[n] = carried
-        own = states_ref[n, part : part + 1, :]
-        carried = jnp.exp(own) * carried + states_ref[n, :part, :]
-
-
-def incoming_state(here, planes, states):
+        carried = jnp.exp(states_ref[n, part:, :]) * carried + states_ref[n, :part, :]
+
+
+def incoming_state(here, joined, states):
     count, lines, width = states.shape
     return pl.pallas_call(
         incoming_kernel,
@@ -137,7 +124,7 @@
         out_specs=pl.BlockSpec(memory_space=pltpu.VMEM),
         cost_estimate=kernel_cost(2**19, 2**19, 2**12),
         name="incoming_state",
-    )(here, planes, states)
+    )(here, joined, states)
 
 
 def mix_kernel(within_ref, carry_q_ref, state_ref, gate_ref, gain_ref, out_ref):
@@ -325,7 +312,7 @@
     far = moved(mine, axes, lambda y1, y0, c: (1 - y1, c, y0))
     upper = lax.axis_index("y1") == 1
     pair = jnp.stack([jnp.where(upper, far, near), jnp.where(upper, near, far)])
-    whole = lax.all_gather(pair, (Z, "c"), axis=0)
+    whole = lax.all_gather(pair, Z + ("c",), axis=0)
     return whole.reshape(16, 2, 2, 3, lines // 3, width), pair
 
 
@@ -356,13 +343,13 @@
     within, carry_q, state = retention(
         queries, keys_in, values_in, log_decay.reshape(1, rows)
     )
-    states = exchange(state, Y)
-    packed = plane_state(states)
-    planes = exchange(packed, Z)
-    here = lax.axis_index(Z).astype(jnp.int32).reshape(1)
-    entering = incoming_state(here, planes, states)
-    entering = exchange(entering, Y)
-    entering = entering.reshape(queries.shape[1], queries.shape[1])
+    states = exchange(state, NEAR)
+    joined = joined_state(states)
+    joined = exchange(joined, "zh")
+    zh = lax.axis_index("zh").astype(jnp.int32).reshape(1)
+    entering = incoming_state(zh, joined, states)
+    entering = exchange(entering, NEAR)
+    entering = entering.reshape(head_dim, head_dim)
     sent = mix(within, carry_q, entering, gate_in, head_gain.reshape(1, -1))
     mixed = exchange(sent.reshape(16, *sent.shape[2:]), GROUP + ("c",))
     here = jnp.stack([lax.axis_index(a).astype(jnp.int32) for a in ("x", "c", "y0")])

time: 147 us -> 148 us (level)
  waiting for transfers between devices: 28.6 us -> 26.6 us
  blocking collectives: 19 us -> 20.5 us
    all_to_all x4, waiting for transfers between devices: 22.3 us -> 14.3 us  [exchange(): return lax.all_to_all(tiles, axes, split_axis=0, concat_axis=0, tiled=True)]
    ppermute x5, waiting for transfers between devices: 1.78 us -> 7.78 us  [shifted(): lax.ppermute(value, axis, [(i, (i + by) % length) for i in range(length)])]
    ppermute x5, starting transfers between devices: 15.2 us -> 18.1 us  [shifted(): lax.ppermute(value, axis, [(i, (i + by) % length) for i in range(length)])]
    all_to_all x4, starting transfers between devices: 30.9 us -> 29 us  [exchange(): return lax.all_to_all(tiles, axes, split_axis=0, concat_axis=0, tiled=True)]
    all_to_all x1, blocking collectives: 19 us -> 20.5 us  [exchange(): return lax.all_to_all(tiles, axes, split_axis=0, concat_axis=0, tiled=True)]
    unnamed x22 -> x24, local copies, waits for them, and re-layouts: 3.58 us -> 4.29 us
  transfers between devices with their start and end apart: 12 -> 12, of which waited for: 7 -> 5; matrix products, arithmetic and copies ran while one was open for 3% -> 2% of each run, Pallas kernels for 8% -> 8%
where the time goes in v3:
time: 148 us; the launch traced here: 147 us
  starting transfers between devices  55 us (37%)
  waiting for transfers between devices  26.6 us (18%)
  blocking collectives  20.5 us (14%)
  Pallas kernels  20.4 us (14%)
  between operations  13.7 us (9%)
  local copies, waits for them, and re-layouts  6.9 us (5%)
  other arithmetic  3.46 us (2%)
    all_to_all x4, starting transfers between devices, exchange(): return lax.all_to_all(tiles, axes, split_axis=0, concat_axis=0, tiled=True)  29 us
    all_to_all x1, blocking collectives, exchange(): return lax.all_to_all(tiles, axes, split_axis=0, concat_axis=0, tiled=True)  20.5 us
    ppermute x5, starting transfers between devices, shifted(): lax.ppermute(value, axis, [(i, (i + by) % length) for i in range(length)])  18.1 us
    all_to_all x4, waiting for transfers between devices, exchange(): return lax.all_to_all(tiles, axes, split_axis=0, concat_axis=0, tiled=True)  14.3 us
    pallas_call x1, Pallas kernels, feed_forward(): pl.pallas_call(ffn_kernel, out_shape=jax.ShapeDtypeStruct((count, width),...  8.12 us
    ppermute x2, starting transfers between devices, moved(): return lax.ppermute(value, axes, pairs)  7.94 us
    ppermute x5, waiting for transfers between devices, shifted(): lax.ppermute(value, axis, [(i, (i + by) % length) for i in range(length)])  7.78 us
    pallas_call x1, Pallas kernels, group_rows(): pl.pallas_call(rows_kernel, out_shape=(jax.ShapeDtypeStruct((count, width...  5.1 us
  transfers between devices with their start and end apart: 12, of which 5 were waited for; matrix products, arithmetic and copies ran while one was open for 2% of the time, Pallas kernels for 8%

profile of v3, /device:TPU:1, one launch (start us, length us, event | category | flops | bytes accessed | tf_op | source)
XLA Modules:
  0.0 146.6 jit_solution(13453476984004032519)
XLA Ops:
  6.5 0.9 pad_maximum_fusion.4
  7.5 6.0 %collective-permute-start = (bf16[96,704]{1,0:T(8,128)(2,1)S(1)}, bf16[96,704]{1,0:T(8,128)(2,1)S(1)}, u32[]{:S(2)}, u32[]{:S(2)}) collective-permute-start(bf16[96,704]{1,0:T(8,128)(2,1)S(1)} %pad_maximum_fusion.4), channel_id=1, source_target_pairs={{0,16},{1,24},{8,17},{9,25},{16,0},{17,8},{24,1},{25,9},{2,18},{3,... | collective-permute-start | bytes 405512 | tf_op jit(solution)/shard_map/ppermute | solution.py:295
  13.5 1.9 %collective-permute-start.1 = (bf16[96,704]{1,0:T(8,128)(2,1)S(1)}, bf16[96,704]{1,0:T(8,128)(2,1)S(1)}, u32[]{:S(2)}, u32[]{:S(2)}) collective-permute-start(bf16[96,704]{1,0:T(8,128)(2,1)S(1)} %pad_maximum_fusion.4), channel_id=1, source_target_pairs={{0,0},{1,8},{8,1},{9,9},{16,16},{17,24},{24,17},{25,25},{2,2},{3,1... | collective-permute-start | bytes 405512 | tf_op jit(solution)/shard_map/ppermute | solution.py:295
  15.4 1.4 collective-permute-done
  16.9 3.1 %collective-permute-done.1 = bf16[96,704]{1,0:T(8,128)(2,1)S(1)} collective-permute-done((bf16[96,704]{1,0:T(8,128)(2,1)S(1)}, bf16[96,704]{1,0:T(8,128)(2,1)S(1)}, u32[]{:S(2)}, u32[]{:S(2)}) %collective-permute-start.1) | collective-permute-done | bytes 135200 | tf_op jit(solution)/shard_map/ppermute | solution.py:295
  20.0 0.7 pad_maximum_fusion.3
  20.8 1.9 %retention.1 = (f32[256,128]{1,0:T(8,128)}, bf16[256,128]{1,0:T(8,128)(2,1)}, f32[16,16,128]{2,1,0:T(8,128)}) custom-call(bf16[256,128]{1,0:T(8,128)(2,1)} %q_ref.1, bf16[256,128]{1,0:T(8,128)(2,1)} %k_ref.1, bf16[256,128]{1,0:T(8,128)(2,1)} %v_ref.1, f32[1,256]{1,0:T(1,128)} %bitcast.30), custom_call_target="tpu_custom_call" | custom-call | flops 50331648 | bytes 1048576 | tf_op jit(solution)/shard_map/retention/pallas_call | solution.py:67
  22.7 5.9 %all-to-all-start = ((f32[16,16,128]{2,1,0:T(8,128)}), f32[16,16,128]{2,1,0:T(8,128)S(1)}, u32[]{:S(2)}, u32[]{:S(2)}) async-start(f32[16,16,128]{2,1,0:T(8,128)} %get-tuple-element.13), calls=%async_computation | async-start | bytes 262144 | tf_op jit(solution)/shard_map/all_to_all | solution.py:304
  28.7 4.4 %collective-permute-start.4 = (bf16[160,2048]{1,0:T(8,128)(2,1)S(1)}, bf16[160,2048]{1,0:T(8,128)(2,1)S(1)}, u32[]{:S(2)}, u32[]{:S(2)}) collective-permute-start(bf16[160,2048]{1,0:T(8,128)(2,1)S(1)} %pad_maximum_fusion.1), channel_id=1, source_target_pairs={{0,6},{2,0},{4,2},{6,4},{1,7},{3,1},{5,3},{7,5},{8,14},{10,8},{12,... | collective-permute-start | bytes 1966088 | tf_op jit(solution)/shard_map/ppermute | solution.py:300
  33.1 2.4 %collective-permute-start.3 = (bf16[160,2048]{1,0:T(8,128)(2,1)S(1)}, bf16[160,2048]{1,0:T(8,128)(2,1)S(1)}, u32[]{:S(2)}, u32[]{:S(2)}) collective-permute-start(bf16[160,2048]{1,0:T(8,128)(2,1)S(1)} %pad_maximum_fusion.1), channel_id=1, source_target_pairs={{0,4},{2,6},{4,0},{6,2},{1,5},{3,7},{5,1},{7,3},{8,12},{10,14},{12... | collective-permute-start | bytes 1966088 | tf_op jit(solution)/shard_map/ppermute | solution.py:300
  35.5 2.5 %collective-permute-start.2 = (bf16[160,2048]{1,0:T(8,128)(2,1)S(1)}, bf16[160,2048]{1,0:T(8,128)(2,1)S(1)}, u32[]{:S(2)}, u32[]{:S(2)}) collective-permute-start(bf16[160,2048]{1,0:T(8,128)(2,1)S(1)} %pad_maximum_fusion.1), channel_id=1, source_target_pairs={{0,2},{2,4},{4,6},{6,0},{1,3},{3,5},{5,7},{7,1},{8,10},{10,12},{12... | collective-permute-start | bytes 1966088 | tf_op jit(solution)/shard_map/ppermute | solution.py:300
  38.7 1.6 %joined_state.1 = f32[4,16,128]{2,1,0:T(8,128)} custom-call(f32[16,16,128]{2,1,0:T(8,128)} %copy-done.3), custom_call_target="tpu_custom_call" | custom-call | flops 262144 | bytes 262144 | tf_op jit(solution)/shard_map/joined_state/pallas_call | solution.py:96
  40.3 12.4 %all-to-all-start.1 = ((f32[4,16,128]{2,1,0:T(8,128)}), f32[4,16,128]{2,1,0:T(8,128)S(1)}, u32[]{:S(2)}, u32[]{:S(2)}) async-start(f32[4,16,128]{2,1,0:T(8,128)} %joined_state.1), calls=%async_computation.1 | async-start | bytes 65536 | tf_op jit(solution)/shard_map/all_to_all | solution.py:304
  52.7 12.2 %all-to-all-done.1.joined_ref = f32[4,16,128]{2,1,0:T(8,128)S(1)} async-done(((f32[4,16,128]{2,1,0:T(8,128)}), f32[4,16,128]{2,1,0:T(8,128)S(1)}, u32[]{:S(2)}, u32[]{:S(2)}) %all-to-all-start.1) | async-done | bytes 32800 | tf_op jit(solution)/shard_map/all_to_all | solution.py:304
  65.6 1.6 %incoming_state.1 = f32[16,8,128]{2,1,0:T(8,128)} custom-call(s32[1]{0:T(128)} %bitcast.4.here_ref, f32[4,16,128]{2,1,0:T(8,128)} %copy-done.10, f32[16,16,128]{2,1,0:T(8,128)} %copy-done.3), custom_call_target="tpu_custom_call" | custom-call | flops 524288 | bytes 524288 | tf_op jit(solution)/shard_map/incoming_state/pallas_call | solution.py:120
  67.2 6.7 %all-to-all-start.2 = ((f32[16,8,128]{2,1,0:T(8,128)}), f32[16,8,128]{2,1,0:T(8,128)S(1)}, u32[]{:S(2)}, u32[]{:S(2)}) async-start(f32[16,8,128]{2,1,0:T(8,128)} %incoming_state.1), calls=%async_computation.2 | async-start | bytes 131072 | tf_op jit(solution)/shard_map/all_to_all | solution.py:304
  74.0 0.8 copy-done.4
  74.8 0.8 copy-done.5
  75.8 5.2 %collective-permute-start.5 = (bf16[512,2048]{1,0:T(8,128)(2,1)S(1)}, bf16[512,2048]{1,0:T(8,128)(2,1)}, u32[]{:S(2)}, u32[]{:S(2)}) collective-permute-start(bf16[512,2048]{1,0:T(8,128)(2,1)S(1)} %pad_maximum_fusion.near_w_ref), channel_id=1, source_target_pairs={{0,1},{1,0},{2,3},{3,2},{4,5},{5,4},{6,7},{7,6},{8,9},{9,8},{10,11... | collective-permute-start | bytes 6291464 | tf_op jit(solution)/shard_map/ppermute | solution.py:300
  81.0 0.9 slice_bitcast_fusion.1
  82.0 0.9 slice_bitcast_fusion.2
  83.0 3.6 %collective-permute-start.6 = (bf16[4,32,2048]{2,1,0:T(8,128)(2,1)S(1)}, bf16[4,32,2048]{2,1,0:T(8,128)(2,1)}, u32[]{:S(2)}, u32[]{:S(2)}) collective-permute-start(bf16[4,32,2048]{2,1,0:T(8,128)(2,1)S(1)} %pad_maximum_fusion.2.near_s_ref), channel_id=1, source_target_pairs={{0,8},{8,0},{1,9},{9,1},{2,10},{10,2},{3,11},{11,3},{4,12},{12,4},... | collective-permute-start | bytes 1572872 | tf_op jit(solution)/shard_map/ppermute | solution.py:300
  87.2 2.1 %mix.1 = bf16[8,2,4,32,128]{4,3,2,1,0:T(8,128)(2,1)} custom-call(f32[256,128]{1,0:T(8,128)} %get-tuple-element.11.within_ref, bf16[256,128]{1,0:T(8,128)(2,1)} %get-tuple-element.12.carry_q_ref, f32[128,128]{1,0:T(8,128)} %bitcast.28, bf16[256,128]{1,0:T(8,128)(2,1)} %gate_ref.1, bf16[1,128]{1,0:T(2,128)(2,1)} %bitcast.31), custom_call_target="tpu_custom_call" | custom-call | flops 8388608 | bytes 1048576 | tf_op jit(solution)/shard_map/mix/pallas_call | solution.py:149
  89.3 4.0 %all-to-all-start.3 = ((bf16[16,4,32,128]{3,2,1,0:T(8,128)(2,1)}), bf16[16,4,32,128]{3,2,1,0:T(8,128)(2,1)S(1)}, u32[]{:S(2)}, u32[]{:S(2)}) async-start(bf16[16,4,32,128]{3,2,1,0:T(8,128)(2,1)} %bitcast.27), calls=%async_computation.3 | async-start | bytes 1048576 | tf_op jit(solution)/shard_map/all_to_all | solution.py:304
  93.9 0.7 pad_add_fusion.here_ref
  94.6 7.8 %collective-permute-done.6.far_s_ref = bf16[4,32,2048]{2,1,0:T(8,128)(2,1)} collective-permute-done((bf16[4,32,2048]{2,1,0:T(8,128)(2,1)S(1)}, bf16[4,32,2048]{2,1,0:T(8,128)(2,1)}, u32[]{:S(2)}, u32[]{:S(2)}) %collective-permute-start.6) | collective-permute-done | bytes 524320 | tf_op jit(solution)/shard_map/ppermute | solution.py:300
  102.3 2.0 %all-to-all-done.3 = bf16[16,4,32,128]{3,2,1,0:T(8,128)(2,1)S(1)} async-done(((bf16[16,4,32,128]{3,2,1,0:T(8,128)(2,1)}), bf16[16,4,32,128]{3,2,1,0:T(8,128)(2,1)S(1)}, u32[]{:S(2)}, u32[]{:S(2)}) %all-to-all-start.3) | async-done | bytes 524320 | tf_op jit(solution)/shard_map/all_to_all | solution.py:304
  104.4 0.8 copy-done.2
  105.2 5.1 %group_rows.1 = (bf16[256,2048]{1,0:T(8,128)(2,1)}, f32[32,2048]{1,0:T(8,128)}) custom-call(s32[3]{0:T(128)} %pad_add_fusion.here_ref, bf16[2,8,4,32,128]{4,3,2,1,0:T(8,128)(2,1)} %bitcast.26, bf16[512,2048]{1,0:T(8,128)(2,1)} %copy-done, bf16[512,2048]{1,0:T(8,128)(2,1)} %collective-permute-done.5.far_w_ref, bf16[4,32,2048]{2,1,0:T(8,128)(2,1)} %copy-done.1, ...), custom_call_target="tpu_custom_call" | custom-call | flops 1073741824 | bytes 8388608 | tf_op jit(solution)/shard_map/group_rows/pallas_call | solution.py:206
  110.3 8.1 %feed_forward.1 = bf16[256,2048]{1,0:T(8,128)(2,1)} custom-call(bf16[256,2048]{1,0:T(8,128)(2,1)} %get-tuple-element.16.rows_ref, bf16[16,2,2,3,32,704]{5,4,3,2,1,0:T(8,128)(2,1)} %bitcast.24), custom_call_target="tpu_custom_call" | custom-call | flops 2214592512 | bytes 8388608 | tf_op jit(solution)/shard_map/feed_forward/pallas_call | solution.py:270
  118.4 20.5 %all_to_all.25 = bf16[8,32,2048]{2,1,0:T(8,128)(2,1)S(1)} all-to-all(bf16[8,32,2048]{2,1,0:T(8,128)(2,1)} %bitcast.25), channel_id=1, replica_groups=mesh['zh'=4,'zl'=4,'y1'=2,'y0'=2,'x'=4,'c'=2] {'y0','x'}, dimensions={0} | all-to-all | bytes 2097152 | tf_op jit(solution)/shard_map/all_to_all | solution.py:304
  139.1 0.7 add_convert_fusion
  (42 shorter events, 3.1 us)
Async XLA Ops:
  6.5 22.1 %copy-start.9 = (bf16[32,2048]{1,0:T(8,128)(2,1)S(1)}, bf16[32,2048]{1,0:T(8,128)(2,1)}, u32[]{:S(2)}) copy-start(bf16[32,2048]{1,0:T(8,128)(2,1)} %param.12) | copy-start | bytes 393220
  6.5 22.1 %copy-start.6 = (bf16[128,2048]{1,0:T(8,128)(2,1)S(1)}, bf16[128,2048]{1,0:T(8,128)(2,1)}, u32[]{:S(2)}) copy-start(bf16[128,2048]{1,0:T(8,128)(2,1)} %param.19) | copy-start | bytes 1572868
  6.5 103.7 %all-gather.3.cloned.1.call-start = ((), (), s32[]{:S(2)}) async-start(), calls=%async_computation.5 | async-start | bytes 9732096 | tf_op jit(solution)/shard_map/all_gather | solution.py:315
  7.5 9.4 %collective-permute-start = (bf16[96,704]{1,0:T(8,128)(2,1)S(1)}, bf16[96,704]{1,0:T(8,128)(2,1)S(1)}, u32[]{:S(2)}, u32[]{:S(2)}) collective-permute-start(bf16[96,704]{1,0:T(8,128)(2,1)S(1)} %pad_maximum_fusion.4), channel_id=1, source_target_pairs={{0,16},{1,24},{8,17},{9,25},{16,0},{17,8},{24,1},{25,9},{2,18},{3,... | collective-permute-start | bytes 405512 | tf_op jit(solution)/shard_map/ppermute | solution.py:295
  13.5 6.5 %collective-permute-start.1 = (bf16[96,704]{1,0:T(8,128)(2,1)S(1)}, bf16[96,704]{1,0:T(8,128)(2,1)S(1)}, u32[]{:S(2)}, u32[]{:S(2)}) collective-permute-start(bf16[96,704]{1,0:T(8,128)(2,1)S(1)} %pad_maximum_fusion.4), channel_id=1, source_target_pairs={{0,0},{1,8},{8,1},{9,9},{16,16},{17,24},{24,17},{25,25},{2,2},{3,1... | collective-permute-start | bytes 405512 | tf_op jit(solution)/shard_map/ppermute | solution.py:295
  22.7 15.4 %all-to-all-start = ((f32[16,16,128]{2,1,0:T(8,128)}), f32[16,16,128]{2,1,0:T(8,128)S(1)}, u32[]{:S(2)}, u32[]{:S(2)}) async-start(f32[16,16,128]{2,1,0:T(8,128)} %get-tuple-element.13), calls=%async_computation | async-start | bytes 262144 | tf_op jit(solution)/shard_map/all_to_all | solution.py:304
  28.7 45.2 %collective-permute-start.4 = (bf16[160,2048]{1,0:T(8,128)(2,1)S(1)}, bf16[160,2048]{1,0:T(8,128)(2,1)S(1)}, u32[]{:S(2)}, u32[]{:S(2)}) collective-permute-start(bf16[160,2048]{1,0:T(8,128)(2,1)S(1)} %pad_maximum_fusion.1), channel_id=1, source_target_pairs={{0,6},{2,0},{4,2},{6,4},{1,7},{3,1},{5,3},{7,5},{8,14},{10,8},{12,... | collective-permute-start | bytes 1966088 | tf_op jit(solution)/shard_map/ppermute | solution.py:300
  33.1 40.8 %collective-permute-start.3 = (bf16[160,2048]{1,0:T(8,128)(2,1)S(1)}, bf16[160,2048]{1,0:T(8,128)(2,1)S(1)}, u32[]{:S(2)}, u32[]{:S(2)}) collective-permute-start(bf16[160,2048]{1,0:T(8,128)(2,1)S(1)} %pad_maximum_fusion.1), channel_id=1, source_target_pairs={{0,4},{2,6},{4,0},{6,2},{1,5},{3,7},{5,1},{7,3},{8,12},{10,14},{12... | collective-permute-start | bytes 1966088 | tf_op jit(solution)/shard_map/ppermute | solution.py:300
  35.5 38.4 %collective-permute-start.2 = (bf16[160,2048]{1,0:T(8,128)(2,1)S(1)}, bf16[160,2048]{1,0:T(8,128)(2,1)S(1)}, u32[]{:S(2)}, u32[]{:S(2)}) collective-permute-start(bf16[160,2048]{1,0:T(8,128)(2,1)S(1)} %pad_maximum_fusion.1), channel_id=1, source_target_pairs={{0,2},{2,4},{4,6},{6,0},{1,3},{3,5},{5,7},{7,1},{8,10},{10,12},{12... | collective-permute-start | bytes 1966088 | tf_op jit(solution)/shard_map/ppermute | solution.py:300
  38.1 0.7 copy-start.3
  40.3 24.7 %all-to-all-start.1 = ((f32[4,16,128]{2,1,0:T(8,128)}), f32[4,16,128]{2,1,0:T(8,128)S(1)}, u32[]{:S(2)}, u32[]{:S(2)}) async-start(f32[4,16,128]{2,1,0:T(8,128)} %joined_state.1), calls=%async_computation.1 | async-start | bytes 65536 | tf_op jit(solution)/shard_map/all_to_all | solution.py:304
  65.0 0.6 copy-start.10
  67.2 19.4 %all-to-all-start.2 = ((f32[16,8,128]{2,1,0:T(8,128)}), f32[16,8,128]{2,1,0:T(8,128)S(1)}, u32[]{:S(2)}, u32[]{:S(2)}) async-start(f32[16,8,128]{2,1,0:T(8,128)} %incoming_state.1), calls=%async_computation.2 | async-start | bytes 131072 | tf_op jit(solution)/shard_map/all_to_all | solution.py:304
  73.9 0.8 copy-start.4
  74.8 0.8 copy-start.5
  75.8 28.6 %copy-start = (bf16[512,2048]{1,0:T(8,128)(2,1)}, bf16[512,2048]{1,0:T(8,128)(2,1)S(1)}, u32[]{:S(2)}) copy-start(bf16[512,2048]{1,0:T(8,128)(2,1)S(1)} %pad_maximum_fusion.near_w_ref) | copy-start | bytes 6291460
  75.8 17.5 %copy-start.11 = (bf16[2048]{0:T(1024)(128)(2,1)S(1)}, bf16[2048]{0:T(1024)(128)(2,1)}, u32[]{:S(2)}) copy-start(bf16[2048]{0:T(1024)(128)(2,1)} %param.20) | copy-start | bytes 12292
  75.8 28.6 %collective-permute-start.5 = (bf16[512,2048]{1,0:T(8,128)(2,1)S(1)}, bf16[512,2048]{1,0:T(8,128)(2,1)}, u32[]{:S(2)}, u32[]{:S(2)}) collective-permute-start(bf16[512,2048]{1,0:T(8,128)(2,1)S(1)} %pad_maximum_fusion.near_w_ref), channel_id=1, source_target_pairs={{0,1},{1,0},{2,3},{3,2},{4,5},{5,4},{6,7},{7,6},{8,9},{9,8},{10,11... | collective-permute-start | bytes 6291464 | tf_op jit(solution)/shard_map/ppermute | solution.py:300
  83.0 21.4 %copy-start.1 = (bf16[4,32,2048]{2,1,0:T(8,128)(2,1)}, bf16[4,32,2048]{2,1,0:T(8,128)(2,1)S(1)}, u32[]{:S(2)}) copy-start(bf16[4,32,2048]{2,1,0:T(8,128)(2,1)S(1)} %pad_maximum_fusion.2.near_s_ref) | copy-start | bytes 1572868
  83.0 19.4 %collective-permute-start.6 = (bf16[4,32,2048]{2,1,0:T(8,128)(2,1)S(1)}, bf16[4,32,2048]{2,1,0:T(8,128)(2,1)}, u32[]{:S(2)}, u32[]{:S(2)}) collective-permute-start(bf16[4,32,2048]{2,1,0:T(8,128)(2,1)S(1)} %pad_maximum_fusion.2.near_s_ref), channel_id=1, source_target_pairs={{0,8},{8,0},{1,9},{9,1},{2,10},{10,2},{3,11},{11,3},{4,12},{12,4},... | collective-permute-start | bytes 1572872 | tf_op jit(solution)/shard_map/ppermute | solution.py:300
  86.5 0.6 copy-start.7
  89.3 15.1 %all-to-all-start.3 = ((bf16[16,4,32,128]{3,2,1,0:T(8,128)(2,1)}), bf16[16,4,32,128]{3,2,1,0:T(8,128)(2,1)S(1)}, u32[]{:S(2)}, u32[]{:S(2)}) async-start(bf16[16,4,32,128]{3,2,1,0:T(8,128)(2,1)} %bitcast.27), calls=%async_computation.3 | async-start | bytes 1048576 | tf_op jit(solution)/shard_map/all_to_all | solution.py:304
  104.4 0.8 copy-start.2
  118.4 20.7 %copy-start.8 = (f32[32,2048]{1,0:T(8,128)S(1)}, f32[32,2048]{1,0:T(8,128)}, u32[]{:S(2)}) copy-start(f32[32,2048]{1,0:T(8,128)} %get-tuple-element.15) | copy-start | bytes 786436
Sparse Core Ops, SparseCore 0:
  20.9 83.4 all-gather.2

commit v4 on v3

--- a/solution.py
+++ b/solution.py
@@ -313,7 +313,7 @@
     upper = lax.axis_index("y1") == 1
     pair = jnp.stack([jnp.where(upper, far, near), jnp.where(upper, near, far)])
     whole = lax.all_gather(pair, Z + ("c",), axis=0)
-    return whole.reshape(16, 2, 2, 3, lines // 3, width), pair
+    return whole.reshape(16, 2, 2, 3, lines // 3, width)
 
 
 def layer(
@@ -330,11 +330,10 @@
     up_weight,
     down_weight,
 ):
-    weights, tied = gathered_weights(gate_weight, up_weight, down_weight)
+    weights = gathered_weights(gate_weight, up_weight, down_weight)
     rows, width = queries.shape[0], stream.shape[1]
     head_dim = queries.shape[1]
     block = jnp.concatenate([out_weight, stream], axis=0)
-    block, _ = lax.optimization_barrier((block, tied))
     found = [block] + [shifted(block, "x", r) for r in (1, 2, 3)]
     near_w = jnp.concatenate([b[:head_dim] for b in found], axis=0)
     near_s = jnp.stack([b[head_dim:] for b in found])

time: 148 us -> 156 us (1.054)
  blocking collectives: 20.5 us -> 36.2 us
  starting transfers between devices: 55 us -> 46.5 us
    all_to_all x1 -> x2, blocking collectives: 20.5 us -> 36.2 us  [exchange(): return lax.all_to_all(tiles, axes, split_axis=0, concat_axis=0, tiled=True)]
    all_to_all x4 -> x3, starting transfers between devices: 29 us -> 20.6 us  [exchange(): return lax.all_to_all(tiles, axes, split_axis=0, concat_axis=0, tiled=True)]
    unnamed x24 -> x23, local copies, waits for them, and re-layouts: 4.29 us -> 4.73 us
    all_to_all x4 -> x3, waiting for transfers between devices: 14.3 us -> 14 us  [exchange(): return lax.all_to_all(tiles, axes, split_axis=0, concat_axis=0, tiled=True)]
  transfers between devices with their start and end apart: 12 -> 11, of which waited for: 5 -> 5; matrix products, arithmetic and copies ran while one was open for 2% -> 3% of each run, Pallas kernels for 8% -> 8%
where the time goes in v4:
time: 156 us; the launch traced here: 155 us
  starting transfers between devices  46.5 us (30%)
  blocking collectives  36.2 us (23%)
  waiting for transfers between devices  26.6 us (17%)
  Pallas kernels  20.5 us (13%)
  between operations  13.7 us (9%)
  local copies, waits for them, and re-layouts  8.2 us (5%)
  other arithmetic  3.33 us (2%)
    all_to_all x2, blocking collectives, exchange(): return lax.all_to_all(tiles, axes, split_axis=0, concat_axis=0, tiled=True)  36.2 us
    all_to_all x3, starting transfers between devices, exchange(): return lax.all_to_all(tiles, axes, split_axis=0, concat_axis=0, tiled=True)  20.6 us
    ppermute x5, starting transfers between devices, shifted(): lax.ppermute(value, axis, [(i, (i + by) % length) for i in range(length)])  17.9 us
    all_to_all x3, waiting for transfers between devices, exchange(): return lax.all_to_all(tiles, axes, split_axis=0, concat_axis=0, tiled=True)  14 us
    pallas_call x1, Pallas kernels, feed_forward(): pl.pallas_call(ffn_kernel, out_shape=jax.ShapeDtypeStruct((count, width),...  8.17 us
    ppermute x5, waiting for transfers between devices, shifted(): lax.ppermute(value, axis, [(i, (i + by) % length) for i in range(length)])  8.05 us
    ppermute x2, starting transfers between devices, moved(): return lax.ppermute(value, axes, pairs)  7.94 us
    pallas_call x1, Pallas kernels, group_rows(): pl.pallas_call(rows_kernel, out_shape=(jax.ShapeDtypeStruct((count, width...  5.09 us
  transfers between devices with their start and end apart: 11, of which 5 were waited for; matrix products, arithmetic and copies ran while one was open for 3% of the time, Pallas kernels for 8%

profile of v4, /device:TPU:1, one launch (start us, length us, event | category | flops | bytes accessed | tf_op | source)
XLA Modules:
  0.0 154.9 jit_solution(9633140582351404327)
XLA Ops:
  6.5 0.9 pad_maximum_fusion.3
  7.5 6.0 %collective-permute-start.5 = (bf16[96,704]{1,0:T(8,128)(2,1)S(1)}, bf16[96,704]{1,0:T(8,128)(2,1)S(1)}, u32[]{:S(2)}, u32[]{:S(2)}) collective-permute-start(bf16[96,704]{1,0:T(8,128)(2,1)S(1)} %pad_maximum_fusion.3), channel_id=1, source_target_pairs={{0,16},{1,24},{8,17},{9,25},{16,0},{17,8},{24,1},{25,9},{2,18},{3,... | collective-permute-start | bytes 405512 | tf_op jit(solution)/shard_map/ppermute | solution.py:295
  13.5 1.9 %collective-permute-start.6 = (bf16[96,704]{1,0:T(8,128)(2,1)S(1)}, bf16[96,704]{1,0:T(8,128)(2,1)S(1)}, u32[]{:S(2)}, u32[]{:S(2)}) collective-permute-start(bf16[96,704]{1,0:T(8,128)(2,1)S(1)} %pad_maximum_fusion.3), channel_id=1, source_target_pairs={{0,0},{1,8},{8,1},{9,9},{16,16},{17,24},{24,17},{25,25},{2,2},{3,1... | collective-permute-start | bytes 405512 | tf_op jit(solution)/shard_map/ppermute | solution.py:295
  15.4 1.4 collective-permute-done.5
  16.9 3.1 %collective-permute-done.6 = bf16[96,704]{1,0:T(8,128)(2,1)S(1)} collective-permute-done((bf16[96,704]{1,0:T(8,128)(2,1)S(1)}, bf16[96,704]{1,0:T(8,128)(2,1)S(1)}, u32[]{:S(2)}, u32[]{:S(2)}) %collective-permute-start.6) | collective-permute-done | bytes 135200 | tf_op jit(solution)/shard_map/ppermute | solution.py:295
  20.0 0.7 pad_maximum_fusion.2
  20.7 1.1 constant_dynamic-update-slice_fusion.1
  21.8 0.9 constant_dynamic-update-slice_fusion
  22.7 4.4 %collective-permute-start.2 = (bf16[160,2048]{1,0:T(8,128)(2,1)S(1)}, bf16[160,2048]{1,0:T(8,128)(2,1)S(1)}, u32[]{:S(2)}, u32[]{:S(2)}) collective-permute-start(bf16[160,2048]{1,0:T(8,128)(2,1)S(1)} %constant_dynamic-update-slice_fusion), channel_id=1, source_target_pairs={{0,6},{2,0},{4,2},{6,4},{1,7},{3,1},{5,3},{7,5},{8,14},{10,8},{12,... | collective-permute-start | bytes 1966088 | tf_op jit(solution)/shard_map/ppermute | solution.py:300
  27.1 2.4 %collective-permute-start.1 = (bf16[160,2048]{1,0:T(8,128)(2,1)S(1)}, bf16[160,2048]{1,0:T(8,128)(2,1)S(1)}, u32[]{:S(2)}, u32[]{:S(2)}) collective-permute-start(bf16[160,2048]{1,0:T(8,128)(2,1)S(1)} %constant_dynamic-update-slice_fusion), channel_id=1, source_target_pairs={{0,4},{2,6},{4,0},{6,2},{1,5},{3,7},{5,1},{7,3},{8,12},{10,14},{12... | collective-permute-start | bytes 1966088 | tf_op jit(solution)/shard_map/ppermute | solution.py:300
  29.6 2.5 %collective-permute-start = (bf16[160,2048]{1,0:T(8,128)(2,1)S(1)}, bf16[160,2048]{1,0:T(8,128)(2,1)S(1)}, u32[]{:S(2)}, u32[]{:S(2)}) collective-permute-start(bf16[160,2048]{1,0:T(8,128)(2,1)S(1)} %constant_dynamic-update-slice_fusion), channel_id=1, source_target_pairs={{0,2},{2,4},{4,6},{6,0},{1,3},{3,5},{5,7},{7,1},{8,10},{10,12},{12... | collective-permute-start | bytes 1966088 | tf_op jit(solution)/shard_map/ppermute | solution.py:300
  32.1 1.9 %retention.1 = (f32[256,128]{1,0:T(8,128)}, bf16[256,128]{1,0:T(8,128)(2,1)}, f32[16,16,128]{2,1,0:T(8,128)}) custom-call(bf16[256,128]{1,0:T(8,128)(2,1)} %q_ref.1, bf16[256,128]{1,0:T(8,128)(2,1)} %k_ref.1, bf16[256,128]{1,0:T(8,128)(2,1)} %v_ref.1, f32[1,256]{1,0:T(1,128)} %bitcast.30), custom_call_target="tpu_custom_call" | custom-call | flops 50331648 | bytes 1048576 | tf_op jit(solution)/shard_map/retention/pallas_call | solution.py:67
  34.0 16.0 %all_to_all.25.states_ref = f32[16,16,128]{2,1,0:T(8,128)} all-to-all(f32[16,16,128]{2,1,0:T(8,128)} %get-tuple-element.12), channel_id=1, replica_groups=mesh['zh'=4,'zl'=4,'y1'=2,'y0'=2,'x'=4,'c'=2] {'zl','y1','y0'}, dimensions={0} | all-to-all | bytes 262144 | tf_op jit(solution)/shard_map/all_to_all | solution.py:304
  50.1 1.5 joined_state.1
  51.6 13.5 %all-to-all-start.1 = ((f32[4,16,128]{2,1,0:T(8,128)}), f32[4,16,128]{2,1,0:T(8,128)S(1)}, u32[]{:S(2)}, u32[]{:S(2)}) async-start(f32[4,16,128]{2,1,0:T(8,128)} %joined_state.1), calls=%async_computation.1 | async-start | bytes 65536 | tf_op jit(solution)/shard_map/all_to_all | solution.py:304
  65.1 11.9 %all-to-all-done.1.joined_ref = f32[4,16,128]{2,1,0:T(8,128)S(1)} async-done(((f32[4,16,128]{2,1,0:T(8,128)}), f32[4,16,128]{2,1,0:T(8,128)S(1)}, u32[]{:S(2)}, u32[]{:S(2)}) %all-to-all-start.1) | async-done | bytes 32800 | tf_op jit(solution)/shard_map/all_to_all | solution.py:304
  77.6 1.6 %incoming_state.1 = f32[16,8,128]{2,1,0:T(8,128)} custom-call(s32[1]{0:T(128)} %bitcast.4.here_ref, f32[4,16,128]{2,1,0:T(8,128)} %copy-done.9, f32[16,16,128]{2,1,0:T(8,128)} %all_to_all.25.states_ref), custom_call_target="tpu_custom_call" | custom-call | flops 524288 | bytes 524288 | tf_op jit(solution)/shard_map/incoming_state/pallas_call | solution.py:120
  79.2 3.5 %all-to-all-start.2 = ((f32[16,8,128]{2,1,0:T(8,128)}), f32[16,8,128]{2,1,0:T(8,128)S(1)}, u32[]{:S(2)}, u32[]{:S(2)}) async-start(f32[16,8,128]{2,1,0:T(8,128)} %incoming_state.1), calls=%async_computation.2 | async-start | bytes 131072 | tf_op jit(solution)/shard_map/all_to_all | solution.py:304
  82.9 0.8 copy-done.4
  83.6 0.8 copy-done.5
  84.7 5.1 %collective-permute-start.3 = (bf16[512,2048]{1,0:T(8,128)(2,1)S(1)}, bf16[512,2048]{1,0:T(8,128)(2,1)}, u32[]{:S(2)}, u32[]{:S(2)}) collective-permute-start(bf16[512,2048]{1,0:T(8,128)(2,1)S(1)} %pad_maximum_fusion.near_w_ref), channel_id=1, source_target_pairs={{0,1},{1,0},{2,3},{3,2},{4,5},{5,4},{6,7},{7,6},{8,9},{9,8},{10,11... | collective-permute-start | bytes 6291464 | tf_op jit(solution)/shard_map/ppermute | solution.py:300
  89.9 0.9 slice_bitcast_fusion.1
  90.8 0.9 slice_bitcast_fusion.2
  91.8 3.4 %collective-permute-start.4 = (bf16[4,32,2048]{2,1,0:T(8,128)(2,1)S(1)}, bf16[4,32,2048]{2,1,0:T(8,128)(2,1)}, u32[]{:S(2)}, u32[]{:S(2)}) collective-permute-start(bf16[4,32,2048]{2,1,0:T(8,128)(2,1)S(1)} %pad_maximum_fusion.1.near_s_ref), channel_id=1, source_target_pairs={{0,8},{8,0},{1,9},{9,1},{2,10},{10,2},{3,11},{11,3},{4,12},{12,4},... | collective-permute-start | bytes 1572872 | tf_op jit(solution)/shard_map/ppermute | solution.py:300
  95.9 2.1 %mix.1 = bf16[8,2,4,32,128]{4,3,2,1,0:T(8,128)(2,1)} custom-call(f32[256,128]{1,0:T(8,128)} %get-tuple-element.10.within_ref, bf16[256,128]{1,0:T(8,128)(2,1)} %get-tuple-element.11.carry_q_ref, f32[128,128]{1,0:T(8,128)} %bitcast.28, bf16[256,128]{1,0:T(8,128)(2,1)} %gate_ref.1, bf16[1,128]{1,0:T(2,128)(2,1)} %bitcast.31), custom_call_target="tpu_custom_call" | custom-call | flops 8388608 | bytes 1048576 | tf_op jit(solution)/shard_map/mix/pallas_call | solution.py:149
  98.0 3.7 %all-to-all-start.3 = ((bf16[16,4,32,128]{3,2,1,0:T(8,128)(2,1)}), bf16[16,4,32,128]{3,2,1,0:T(8,128)(2,1)S(1)}, u32[]{:S(2)}, u32[]{:S(2)}) async-start(bf16[16,4,32,128]{3,2,1,0:T(8,128)(2,1)} %bitcast.26), calls=%async_computation.3 | async-start | bytes 1048576 | tf_op jit(solution)/shard_map/all_to_all | solution.py:304
  102.9 8.0 %collective-permute-done.4.far_s_ref = bf16[4,32,2048]{2,1,0:T(8,128)(2,1)} collective-permute-done((bf16[4,32,2048]{2,1,0:T(8,128)(2,1)S(1)}, bf16[4,32,2048]{2,1,0:T(8,128)(2,1)}, u32[]{:S(2)}, u32[]{:S(2)}) %collective-permute-start.4) | collective-permute-done | bytes 524320 | tf_op jit(solution)/shard_map/ppermute | solution.py:300
  111.0 2.1 %all-to-all-done.3 = bf16[16,4,32,128]{3,2,1,0:T(8,128)(2,1)S(1)} async-done(((bf16[16,4,32,128]{3,2,1,0:T(8,128)(2,1)}), bf16[16,4,32,128]{3,2,1,0:T(8,128)(2,1)S(1)}, u32[]{:S(2)}, u32[]{:S(2)}) %all-to-all-start.3) | async-done | bytes 524320 | tf_op jit(solution)/shard_map/all_to_all | solution.py:304
  113.0 0.8 copy-done.2
  113.8 5.1 %group_rows.1 = (bf16[256,2048]{1,0:T(8,128)(2,1)}, f32[32,2048]{1,0:T(8,128)}) custom-call(s32[3]{0:T(128)} %pad_add_fusion.here_ref, bf16[2,8,4,32,128]{4,3,2,1,0:T(8,128)(2,1)} %bitcast.25, bf16[512,2048]{1,0:T(8,128)(2,1)} %copy-done, bf16[512,2048]{1,0:T(8,128)(2,1)} %collective-permute-done.3.far_w_ref, bf16[4,32,2048]{2,1,0:T(8,128)(2,1)} %copy-done.1, ...), custom_call_target="tpu_custom_call" | custom-call | flops 1073741824 | bytes 8388608 | tf_op jit(solution)/shard_map/group_rows/pallas_call | solution.py:206
  118.9 8.2 %feed_forward.1 = bf16[256,2048]{1,0:T(8,128)(2,1)} custom-call(bf16[256,2048]{1,0:T(8,128)(2,1)} %get-tuple-element.14.rows_ref, bf16[16,2,2,3,32,704]{5,4,3,2,1,0:T(8,128)(2,1)} %bitcast.23), custom_call_target="tpu_custom_call" | custom-call | flops 2214592512 | bytes 8388608 | tf_op jit(solution)/shard_map/feed_forward/pallas_call | solution.py:270
  127.1 20.1 %all_to_all.26 = bf16[8,32,2048]{2,1,0:T(8,128)(2,1)S(1)} all-to-all(bf16[8,32,2048]{2,1,0:T(8,128)(2,1)} %bitcast.24), channel_id=1, replica_groups=mesh['zh'=4,'zl'=4,'y1'=2,'y0'=2,'x'=4,'c'=2] {'y0','x'}, dimensions={0} | all-to-all | bytes 2097152 | tf_op jit(solution)/shard_map/all_to_all | solution.py:304
  (38 shorter events, 3.7 us)
Async XLA Ops:
  6.5 78.0 %copy-start.3 = (bf16[128,2048]{1,0:T(8,128)(2,1)S(1)}, bf16[128,2048]{1,0:T(8,128)(2,1)}, u32[]{:S(2)}) copy-start(bf16[128,2048]{1,0:T(8,128)(2,1)} %param.19) | copy-start | bytes 1572868
  6.5 112.4 %all-gather.3.cloned.1.call-start = ((), (), s32[]{:S(2)}) async-start(), calls=%async_computation.5 | async-start | bytes 9732096 | tf_op jit(solution)/shard_map/all_gather | solution.py:315
  7.5 9.4 %collective-permute-start.5 = (bf16[96,704]{1,0:T(8,128)(2,1)S(1)}, bf16[96,704]{1,0:T(8,128)(2,1)S(1)}, u32[]{:S(2)}, u32[]{:S(2)}) collective-permute-start(bf16[96,704]{1,0:T(8,128)(2,1)S(1)} %pad_maximum_fusion.3), channel_id=1, source_target_pairs={{0,16},{1,24},{8,17},{9,25},{16,0},{17,8},{24,1},{25,9},{2,18},{3,... | collective-permute-start | bytes 405512 | tf_op jit(solution)/shard_map/ppermute | solution.py:295
  13.5 6.5 %collective-permute-start.6 = (bf16[96,704]{1,0:T(8,128)(2,1)S(1)}, bf16[96,704]{1,0:T(8,128)(2,1)S(1)}, u32[]{:S(2)}, u32[]{:S(2)}) collective-permute-start(bf16[96,704]{1,0:T(8,128)(2,1)S(1)} %pad_maximum_fusion.3), channel_id=1, source_target_pairs={{0,0},{1,8},{8,1},{9,9},{16,16},{17,24},{24,17},{25,25},{2,2},{3,1... | collective-permute-start | bytes 405512 | tf_op jit(solution)/shard_map/ppermute | solution.py:295
  22.7 60.0 %collective-permute-start.2 = (bf16[160,2048]{1,0:T(8,128)(2,1)S(1)}, bf16[160,2048]{1,0:T(8,128)(2,1)S(1)}, u32[]{:S(2)}, u32[]{:S(2)}) collective-permute-start(bf16[160,2048]{1,0:T(8,128)(2,1)S(1)} %constant_dynamic-update-slice_fusion), channel_id=1, source_target_pairs={{0,6},{2,0},{4,2},{6,4},{1,7},{3,1},{5,3},{7,5},{8,14},{10,8},{12,... | collective-permute-start | bytes 1966088 | tf_op jit(solution)/shard_map/ppermute | solution.py:300
  27.1 55.7 %collective-permute-start.1 = (bf16[160,2048]{1,0:T(8,128)(2,1)S(1)}, bf16[160,2048]{1,0:T(8,128)(2,1)S(1)}, u32[]{:S(2)}, u32[]{:S(2)}) collective-permute-start(bf16[160,2048]{1,0:T(8,128)(2,1)S(1)} %constant_dynamic-update-slice_fusion), channel_id=1, source_target_pairs={{0,4},{2,6},{4,0},{6,2},{1,5},{3,7},{5,1},{7,3},{8,12},{10,14},{12... | collective-permute-start | bytes 1966088 | tf_op jit(solution)/shard_map/ppermute | solution.py:300
  29.6 53.3 %collective-permute-start = (bf16[160,2048]{1,0:T(8,128)(2,1)S(1)}, bf16[160,2048]{1,0:T(8,128)(2,1)S(1)}, u32[]{:S(2)}, u32[]{:S(2)}) collective-permute-start(bf16[160,2048]{1,0:T(8,128)(2,1)S(1)} %constant_dynamic-update-slice_fusion), channel_id=1, source_target_pairs={{0,2},{2,4},{4,6},{6,0},{1,3},{3,5},{5,7},{7,1},{8,10},{10,12},{12... | collective-permute-start | bytes 1966088 | tf_op jit(solution)/shard_map/ppermute | solution.py:300
  51.6 25.4 %all-to-all-start.1 = ((f32[4,16,128]{2,1,0:T(8,128)}), f32[4,16,128]{2,1,0:T(8,128)S(1)}, u32[]{:S(2)}, u32[]{:S(2)}) async-start(f32[4,16,128]{2,1,0:T(8,128)} %joined_state.1), calls=%async_computation.1 | async-start | bytes 65536 | tf_op jit(solution)/shard_map/all_to_all | solution.py:304
  77.0 0.6 copy-start.9
  77.6 14.1 %copy-start.6 = (bf16[32,2048]{1,0:T(8,128)(2,1)S(1)}, bf16[32,2048]{1,0:T(8,128)(2,1)}, u32[]{:S(2)}) copy-start(bf16[32,2048]{1,0:T(8,128)(2,1)} %param.12) | copy-start | bytes 393220
  79.2 16.0 %all-to-all-start.2 = ((f32[16,8,128]{2,1,0:T(8,128)}), f32[16,8,128]{2,1,0:T(8,128)S(1)}, u32[]{:S(2)}, u32[]{:S(2)}) async-start(f32[16,8,128]{2,1,0:T(8,128)} %incoming_state.1), calls=%async_computation.2 | async-start | bytes 131072 | tf_op jit(solution)/shard_map/all_to_all | solution.py:304
  82.8 0.8 copy-start.4
  83.6 0.8 copy-start.5
  84.5 17.1 %copy-start.10 = (bf16[2048]{0:T(1024)(128)(2,1)S(1)}, bf16[2048]{0:T(1024)(128)(2,1)}, u32[]{:S(2)}) copy-start(bf16[2048]{0:T(1024)(128)(2,1)} %param.20) | copy-start | bytes 12292
  84.7 28.3 %copy-start = (bf16[512,2048]{1,0:T(8,128)(2,1)}, bf16[512,2048]{1,0:T(8,128)(2,1)S(1)}, u32[]{:S(2)}) copy-start(bf16[512,2048]{1,0:T(8,128)(2,1)S(1)} %pad_maximum_fusion.near_w_ref) | copy-start | bytes 6291460
  84.7 28.3 %collective-permute-start.3 = (bf16[512,2048]{1,0:T(8,128)(2,1)S(1)}, bf16[512,2048]{1,0:T(8,128)(2,1)}, u32[]{:S(2)}, u32[]{:S(2)}) collective-permute-start(bf16[512,2048]{1,0:T(8,128)(2,1)S(1)} %pad_maximum_fusion.near_w_ref), channel_id=1, source_target_pairs={{0,1},{1,0},{2,3},{3,2},{4,5},{5,4},{6,7},{7,6},{8,9},{9,8},{10,11... | collective-permute-start | bytes 6291464 | tf_op jit(solution)/shard_map/ppermute | solution.py:300
  91.8 21.2 %copy-start.1 = (bf16[4,32,2048]{2,1,0:T(8,128)(2,1)}, bf16[4,32,2048]{2,1,0:T(8,128)(2,1)S(1)}, u32[]{:S(2)}) copy-start(bf16[4,32,2048]{2,1,0:T(8,128)(2,1)S(1)} %pad_maximum_fusion.1.near_s_ref) | copy-start | bytes 1572868
  91.8 19.2 %collective-permute-start.4 = (bf16[4,32,2048]{2,1,0:T(8,128)(2,1)S(1)}, bf16[4,32,2048]{2,1,0:T(8,128)(2,1)}, u32[]{:S(2)}, u32[]{:S(2)}) collective-permute-start(bf16[4,32,2048]{2,1,0:T(8,128)(2,1)S(1)} %pad_maximum_fusion.1.near_s_ref), channel_id=1, source_target_pairs={{0,8},{8,0},{1,9},{9,1},{2,10},{10,2},{3,11},{11,3},{4,12},{12,4},... | collective-permute-start | bytes 1572872 | tf_op jit(solution)/shard_map/ppermute | solution.py:300
  95.2 0.6 copy-start.7
  98.0 15.0 %all-to-all-start.3 = ((bf16[16,4,32,128]{3,2,1,0:T(8,128)(2,1)}), bf16[16,4,32,128]{3,2,1,0:T(8,128)(2,1)S(1)}, u32[]{:S(2)}, u32[]{:S(2)}) async-start(bf16[16,4,32,128]{3,2,1,0:T(8,128)(2,1)} %bitcast.26), calls=%async_computation.3 | async-start | bytes 1048576 | tf_op jit(solution)/shard_map/all_to_all | solution.py:304
  113.0 0.8 copy-start.2
  118.9 28.5 %copy-start.8 = (f32[32,2048]{1,0:T(8,128)S(1)}, f32[32,2048]{1,0:T(8,128)}, u32[]{:S(2)}) copy-start(f32[32,2048]{1,0:T(8,128)} %get-tuple-element.13) | copy-start | bytes 786436
Sparse Core Ops, SparseCore 0:
  20.9 85.6 all-gather.2

commit v5 on v4

--- a/solution.py
+++ b/solution.py
@@ -99,6 +99,7 @@
         in_specs=vmem(1),
         out_specs=pl.BlockSpec(memory_space=pltpu.VMEM),
         cost_estimate=kernel_cost(2**18, 2**18, 2**10),
+        compiler_params=pltpu.CompilerParams(vmem_limit_bytes=2 * 2**20),
         name="joined_state",
     )(states)
 
@@ -123,6 +124,7 @@
         in_specs=[pl.BlockSpec(memory_space=pltpu.SMEM)] + vmem(2),
         out_specs=pl.BlockSpec(memory_space=pltpu.VMEM),
         cost_estimate=kernel_cost(2**19, 2**19, 2**12),
+        compiler_params=pltpu.CompilerParams(vmem_limit_bytes=2 * 2**20),
         name="incoming_state",
     )(here, joined, states)
 
@@ -213,6 +215,7 @@
         out_specs=vmem(2),
         scratch_shapes=[pltpu.VMEM((count, width), F32)],
         cost_estimate=kernel_cost(2 * count * width * 1024, 2**23),
+        compiler_params=pltpu.CompilerParams(vmem_limit_bytes=20 * 2**20),
         name="group_rows",
     )(here, mixed, near_w, far_w, near_s, far_s, gain)
 
@@ -280,6 +283,7 @@
             pltpu.SemaphoreType.DMA((kinds, CHUNKS, 4)),
         ],
         cost_estimate=kernel_cost(6 * count * width * hidden_width, 2**23, count * hidden_width),
+        compiler_params=pltpu.CompilerParams(vmem_limit_bytes=56 * 2**20),
         name="feed_forward",
     )(rows, weights)
 
@@ -333,10 +337,11 @@
     weights = gathered_weights(gate_weight, up_weight, down_weight)
     rows, width = queries.shape[0], stream.shape[1]
     head_dim = queries.shape[1]
-    block = jnp.concatenate([out_weight, stream], axis=0)
-    found = [block] + [shifted(block, "x", r) for r in (1, 2, 3)]
-    near_w = jnp.concatenate([b[:head_dim] for b in found], axis=0)
-    near_s = jnp.stack([b[head_dim:] for b in found])
+    sides = [shifted(out_weight, "x", 1), shifted(out_weight, "x", 3)]
+    across = shifted(out_weight, "x", 2)
+    others = [shifted(stream, "x", r) for r in (1, 2, 3)]
+    near_w = jnp.concatenate([out_weight, sides[0], across, sides[1]], axis=0)
+    near_s = jnp.stack([stream, *others])
     far_w = shifted(near_w, "c", 1)
     far_s = shifted(near_s, "y0", 1)
     within, carry_q, state = retention(

time: 156 us -> 171 us (1.096)
  waiting for transfers between devices: 26.6 us -> 49.8 us
  starting transfers between devices: 46.5 us -> 67.9 us
  blocking collectives: 36.2 us -> 18 us
  local copies, waits for them, and re-layouts: 8.2 us -> 1.79 us
  Pallas kernels: 20.5 us -> 16.7 us
    all_to_all x2 -> x1, blocking collectives: 36.2 us -> 18 us  [exchange(): return lax.all_to_all(tiles, axes, split_axis=0, concat_axis=0, tiled=True)]
    all_to_all x3 -> x4, starting transfers between devices: 20.6 us -> 32.9 us  [exchange(): return lax.all_to_all(tiles, axes, split_axis=0, concat_axis=0, tiled=True)]
    all_to_all x3 -> x4, waiting for transfers between devices: 14 us -> 25.9 us  [exchange(): return lax.all_to_all(tiles, axes, split_axis=0, concat_axis=0, tiled=True)]
    ppermute x5 -> x8, waiting for transfers between devices: 8.05 us -> 19.3 us  [shifted(): lax.ppermute(value, axis, [(i, (i + by) % length) for i in range(length)])]
    ppermute x5 -> x8, starting transfers between devices: 17.9 us -> 27.1 us  [shifted(): lax.ppermute(value, axis, [(i, (i + by) % length) for i in range(length)])]
    unnamed x23 -> x13, local copies, waits for them, and re-layouts: 4.73 us -> 1.75 us
    pallas_call x1, Pallas kernels: 5.09 us -> 3.17 us  [group_rows(): pl.pallas_call(rows_kernel, out_shape=(jax.ShapeDtypeStruct((count, width...]
    another operation x3 -> x0, local copies, waits for them, and re-layouts: 1.84 us -> none  [layer(): near_s = jnp.stack([b[head_dim:] for b in found])]
  transfers between devices with their start and end apart: 11 -> 15, of which waited for: 5 -> 9; matrix products, arithmetic and copies ran while one was open for 3% -> 0% of each run, Pallas kernels for 8% -> 5%
where the time goes in v5:
time: 171 us; the launch traced here: 170 us
  starting transfers between devices  67.9 us (40%)
  waiting for transfers between devices  49.8 us (29%)
  blocking collectives  18 us (11%)
  Pallas kernels  16.7 us (10%)
  between operations  13.6 us (8%)
  other arithmetic  2.67 us (2%)
  local copies, waits for them, and re-layouts  1.79 us (1%)
    all_to_all x4, starting transfers between devices, exchange(): return lax.all_to_all(tiles, axes, split_axis=0, concat_axis=0, tiled=True)  32.9 us
    ppermute x8, starting transfers between devices, shifted(): lax.ppermute(value, axis, [(i, (i + by) % length) for i in range(length)])  27.1 us
    all_to_all x4, waiting for transfers between devices, exchange(): return lax.all_to_all(tiles, axes, split_axis=0, concat_axis=0, tiled=True)  25.9 us
    ppermute x8, waiting for transfers between devices, shifted(): lax.ppermute(value, axis, [(i, (i + by) % length) for i in range(length)])  19.3 us
    all_to_all x1, blocking collectives, exchange(): return lax.all_to_all(tiles, axes, split_axis=0, concat_axis=0, tiled=True)  18 us
    pallas_call x1, Pallas kernels, feed_forward(): pl.pallas_call(ffn_kernel, out_shape=jax.ShapeDtypeStruct((count, width),...  8.11 us
    ppermute x2, starting transfers between devices, moved(): return lax.ppermute(value, axes, pairs)  7.94 us
    ppermute x2, waiting for transfers between devices, moved(): return lax.ppermute(value, axes, pairs)  4.53 us
  transfers between devices with their start and end apart: 15, of which 9 were waited for; matrix products, arithmetic and copies ran while one was open for 0% of the time, Pallas kernels for 5%

profile of v5, /device:TPU:1, one launch (start us, length us, event | category | flops | bytes accessed | tf_op | source)
XLA Modules:
  0.0 170.5 jit_solution(10968246949022706483)
XLA Ops:
  6.5 0.9 pad_maximum_fusion.2
  7.5 6.0 %collective-permute-start.8 = (bf16[96,704]{1,0:T(8,128)(2,1)S(1)}, bf16[96,704]{1,0:T(8,128)(2,1)S(1)}, u32[]{:S(2)}, u32[]{:S(2)}) collective-permute-start(bf16[96,704]{1,0:T(8,128)(2,1)S(1)} %pad_maximum_fusion.2), channel_id=1, source_target_pairs={{0,16},{1,24},{8,17},{9,25},{16,0},{17,8},{24,1},{25,9},{2,18},{3,... | collective-permute-start | bytes 405512 | tf_op jit(solution)/shard_map/ppermute | solution.py:299
  13.5 1.9 %collective-permute-start.9 = (bf16[96,704]{1,0:T(8,128)(2,1)S(1)}, bf16[96,704]{1,0:T(8,128)(2,1)S(1)}, u32[]{:S(2)}, u32[]{:S(2)}) collective-permute-start(bf16[96,704]{1,0:T(8,128)(2,1)S(1)} %pad_maximum_fusion.2), channel_id=1, source_target_pairs={{0,0},{1,8},{8,1},{9,9},{16,16},{17,24},{24,17},{25,25},{2,2},{3,1... | collective-permute-start | bytes 405512 | tf_op jit(solution)/shard_map/ppermute | solution.py:299
  15.4 1.4 collective-permute-done.8
  16.9 3.1 %collective-permute-done.9 = bf16[96,704]{1,0:T(8,128)(2,1)S(1)} collective-permute-done((bf16[96,704]{1,0:T(8,128)(2,1)S(1)}, bf16[96,704]{1,0:T(8,128)(2,1)S(1)}, u32[]{:S(2)}, u32[]{:S(2)}) %collective-permute-start.9) | collective-permute-done | bytes 135200 | tf_op jit(solution)/shard_map/ppermute | solution.py:299
  20.0 0.8 pad_maximum_fusion.1
  20.8 3.3 %collective-permute-start = (bf16[128,2048]{1,0:T(8,128)(2,1)}, bf16[128,2048]{1,0:T(8,128)(2,1)S(1)}, u32[]{:S(2)}, u32[]{:S(2)}) collective-permute-start(bf16[128,2048]{1,0:T(8,128)(2,1)} %param.19), channel_id=1, source_target_pairs={{0,2},{2,4},{4,6},{6,0},{1,3},{3,5},{5,7},{7,1},{8,10},{10,12},{12... | collective-permute-start | bytes 1572872 | tf_op jit(solution)/shard_map/ppermute | solution.py:304
  24.0 4.4 %collective-permute-start.1 = (bf16[128,2048]{1,0:T(8,128)(2,1)}, bf16[128,2048]{1,0:T(8,128)(2,1)S(1)}, u32[]{:S(2)}, u32[]{:S(2)}) collective-permute-start(bf16[128,2048]{1,0:T(8,128)(2,1)} %param.19), channel_id=1, source_target_pairs={{0,4},{2,6},{4,0},{6,2},{1,5},{3,7},{5,1},{7,3},{8,12},{10,14},{12... | collective-permute-start | bytes 1572872 | tf_op jit(solution)/shard_map/ppermute | solution.py:304
  28.4 3.1 %collective-permute-start.2 = (bf16[128,2048]{1,0:T(8,128)(2,1)}, bf16[128,2048]{1,0:T(8,128)(2,1)S(1)}, u32[]{:S(2)}, u32[]{:S(2)}) collective-permute-start(bf16[128,2048]{1,0:T(8,128)(2,1)} %param.19), channel_id=1, source_target_pairs={{0,6},{2,0},{4,2},{6,4},{1,7},{3,1},{5,3},{7,5},{8,14},{10,8},{12,... | collective-permute-start | bytes 1572872 | tf_op jit(solution)/shard_map/ppermute | solution.py:304
  31.5 3.3 %collective-permute-done = bf16[128,2048]{1,0:T(8,128)(2,1)S(1)} collective-permute-done((bf16[128,2048]{1,0:T(8,128)(2,1)}, bf16[128,2048]{1,0:T(8,128)(2,1)S(1)}, u32[]{:S(2)}, u32[]{:S(2)}) %collective-permute-start) | collective-permute-done | bytes 524320 | tf_op jit(solution)/shard_map/ppermute | solution.py:304
  34.9 13.5 %collective-permute-done.1 = bf16[128,2048]{1,0:T(8,128)(2,1)S(1)} collective-permute-done((bf16[128,2048]{1,0:T(8,128)(2,1)}, bf16[128,2048]{1,0:T(8,128)(2,1)S(1)}, u32[]{:S(2)}, u32[]{:S(2)}) %collective-permute-start.1) | collective-permute-done | bytes 524320 | tf_op jit(solution)/shard_map/ppermute | solution.py:304
  48.3 2.5 %collective-permute-done.2 = bf16[128,2048]{1,0:T(8,128)(2,1)S(1)} collective-permute-done((bf16[128,2048]{1,0:T(8,128)(2,1)}, bf16[128,2048]{1,0:T(8,128)(2,1)S(1)}, u32[]{:S(2)}, u32[]{:S(2)}) %collective-permute-start.2) | collective-permute-done | bytes 524320 | tf_op jit(solution)/shard_map/ppermute | solution.py:304
  50.9 3.4 %collective-permute-start.3 = (bf16[512,2048]{1,0:T(8,128)(2,1)S(1)}, bf16[512,2048]{1,0:T(8,128)(2,1)}, u32[]{:S(2)}, u32[]{:S(2)}) collective-permute-start(bf16[512,2048]{1,0:T(8,128)(2,1)S(1)} %constant_dynamic-update-slice_fusion.near_w_ref), channel_id=1, source_target_pairs={{0,1},{1,0},{2,3},{3,2},{4,5},{5,4},{6,7},{7,6},{8,9},{9,8},{10,11... | collective-permute-start | bytes 6291464 | tf_op jit(solution)/shard_map/ppermute | solution.py:304
  54.3 1.9 %retention.1 = (f32[256,128]{1,0:T(8,128)}, bf16[256,128]{1,0:T(8,128)(2,1)}, f32[16,16,128]{2,1,0:T(8,128)}) custom-call(bf16[256,128]{1,0:T(8,128)(2,1)} %q_ref.1, bf16[256,128]{1,0:T(8,128)(2,1)} %k_ref.1, bf16[256,128]{1,0:T(8,128)(2,1)} %v_ref.1, f32[1,256]{1,0:T(1,128)} %bitcast.30), custom_call_target="tpu_custom_call" | custom-call | flops 50331648 | bytes 1048576 | tf_op jit(solution)/shard_map/retention/pallas_call | solution.py:67
  56.2 5.9 %all-to-all-start = ((f32[16,16,128]{2,1,0:T(8,128)}), f32[16,16,128]{2,1,0:T(8,128)S(1)}, u32[]{:S(2)}, u32[]{:S(2)}) async-start(f32[16,16,128]{2,1,0:T(8,128)} %get-tuple-element.12), calls=%async_computation | async-start | bytes 262144 | tf_op jit(solution)/shard_map/all_to_all | solution.py:308
  62.2 4.3 %collective-permute-start.6 = (bf16[32,2048]{1,0:T(8,128)(2,1)S(1)}, bf16[32,2048]{1,0:T(8,128)(2,1)S(1)}, u32[]{:S(2)}, u32[]{:S(2)}) collective-permute-start(bf16[32,2048]{1,0:T(8,128)(2,1)S(1)} %copy-done.3), channel_id=1, source_target_pairs={{0,6},{2,0},{4,2},{6,4},{1,7},{3,1},{5,3},{7,5},{8,14},{10,8},{12,... | collective-permute-start | bytes 393224 | tf_op jit(solution)/shard_map/ppermute | solution.py:304
  66.5 3.6 %collective-permute-start.5 = (bf16[32,2048]{1,0:T(8,128)(2,1)S(1)}, bf16[32,2048]{1,0:T(8,128)(2,1)S(1)}, u32[]{:S(2)}, u32[]{:S(2)}) collective-permute-start(bf16[32,2048]{1,0:T(8,128)(2,1)S(1)} %copy-done.3), channel_id=1, source_target_pairs={{0,4},{2,6},{4,0},{6,2},{1,5},{3,7},{5,1},{7,3},{8,12},{10,14},{12... | collective-permute-start | bytes 393224 | tf_op jit(solution)/shard_map/ppermute | solution.py:304
  70.0 1.9 %collective-permute-start.4 = (bf16[32,2048]{1,0:T(8,128)(2,1)S(1)}, bf16[32,2048]{1,0:T(8,128)(2,1)S(1)}, u32[]{:S(2)}, u32[]{:S(2)}) collective-permute-start(bf16[32,2048]{1,0:T(8,128)(2,1)S(1)} %copy-done.3), channel_id=1, source_target_pairs={{0,2},{2,4},{4,6},{6,0},{1,3},{3,5},{5,7},{7,1},{8,10},{10,12},{12... | collective-permute-start | bytes 393224 | tf_op jit(solution)/shard_map/ppermute | solution.py:304
  72.0 0.8 all-to-all-done.states_ref
  73.4 12.2 %all-to-all-start.1 = ((f32[4,16,128]{2,1,0:T(8,128)}), f32[4,16,128]{2,1,0:T(8,128)S(1)}, u32[]{:S(2)}, u32[]{:S(2)}) async-start(f32[4,16,128]{2,1,0:T(8,128)} %joined_state.1), calls=%async_computation.1 | async-start | bytes 65536 | tf_op jit(solution)/shard_map/all_to_all | solution.py:308
  85.6 11.9 %all-to-all-done.1.joined_ref = f32[4,16,128]{2,1,0:T(8,128)S(1)} async-done(((f32[4,16,128]{2,1,0:T(8,128)}), f32[4,16,128]{2,1,0:T(8,128)S(1)}, u32[]{:S(2)}, u32[]{:S(2)}) %all-to-all-start.1) | async-done | bytes 32800 | tf_op jit(solution)/shard_map/all_to_all | solution.py:308
  97.5 0.7 incoming_state.1
  98.2 6.1 %all-to-all-start.2 = ((f32[16,8,128]{2,1,0:T(8,128)}), f32[16,8,128]{2,1,0:T(8,128)S(1)}, u32[]{:S(2)}, u32[]{:S(2)}) async-start(f32[16,8,128]{2,1,0:T(8,128)} %incoming_state.1), calls=%async_computation.2 | async-start | bytes 131072 | tf_op jit(solution)/shard_map/all_to_all | solution.py:308
  104.5 3.3 %collective-permute-start.7 = (bf16[4,32,2048]{2,1,0:T(8,128)(2,1)S(1)}, bf16[4,32,2048]{2,1,0:T(8,128)(2,1)}, u32[]{:S(2)}, u32[]{:S(2)}) collective-permute-start(bf16[4,32,2048]{2,1,0:T(8,128)(2,1)S(1)} %pad_maximum_fusion.near_s_ref), channel_id=1, source_target_pairs={{0,8},{8,0},{1,9},{9,1},{2,10},{10,2},{3,11},{11,3},{4,12},{12,4},... | collective-permute-start | bytes 1572872 | tf_op jit(solution)/shard_map/ppermute | solution.py:304
  107.8 3.9 %all-to-all-done.2 = f32[16,8,128]{2,1,0:T(8,128)S(1)} async-done(((f32[16,8,128]{2,1,0:T(8,128)}), f32[16,8,128]{2,1,0:T(8,128)S(1)}, u32[]{:S(2)}, u32[]{:S(2)}) %all-to-all-start.2) | async-done | bytes 65568 | tf_op jit(solution)/shard_map/all_to_all | solution.py:308
  112.3 2.1 %mix.1 = bf16[8,2,4,32,128]{4,3,2,1,0:T(8,128)(2,1)} custom-call(f32[256,128]{1,0:T(8,128)} %get-tuple-element.10.within_ref, bf16[256,128]{1,0:T(8,128)(2,1)} %get-tuple-element.11.carry_q_ref, f32[128,128]{1,0:T(8,128)} %bitcast.24, bf16[256,128]{1,0:T(8,128)(2,1)} %gate_ref.1, bf16[1,128]{1,0:T(2,128)(2,1)} %bitcast.31), custom_call_target="tpu_custom_call" | custom-call | flops 8388608 | bytes 1048576 | tf_op jit(solution)/shard_map/mix/pallas_call | solution.py:151
  114.4 8.6 %all-to-all-start.3 = ((bf16[16,4,32,128]{3,2,1,0:T(8,128)(2,1)}), bf16[16,4,32,128]{3,2,1,0:T(8,128)(2,1)S(1)}, u32[]{:S(2)}, u32[]{:S(2)}) async-start(bf16[16,4,32,128]{3,2,1,0:T(8,128)(2,1)} %bitcast.23), calls=%async_computation.3 | async-start | bytes 1048576 | tf_op jit(solution)/shard_map/all_to_all | solution.py:308
  123.1 9.4 %all-to-all-done.3 = bf16[16,4,32,128]{3,2,1,0:T(8,128)(2,1)S(1)} async-done(((bf16[16,4,32,128]{3,2,1,0:T(8,128)(2,1)}), bf16[16,4,32,128]{3,2,1,0:T(8,128)(2,1)S(1)}, u32[]{:S(2)}, u32[]{:S(2)}) %all-to-all-start.3) | async-done | bytes 524320 | tf_op jit(solution)/shard_map/all_to_all | solution.py:308
  132.5 3.2 %group_rows.1 = (bf16[256,2048]{1,0:T(8,128)(2,1)S(1)}, f32[32,2048]{1,0:T(8,128)S(1)}) custom-call(s32[3]{0:T(128)S(1)} %pad_add_fusion.here_ref, bf16[2,8,4,32,128]{4,3,2,1,0:T(8,128)(2,1)S(1)} %bitcast.20, bf16[512,2048]{1,0:T(8,128)(2,1)S(1)} %constant_dynamic-update-slice_fusion.near_w_ref, bf16[512,2048]{1,0:T(8,128)(2,1)} %collective-permute-done.3.far_w_ref, ...), custom_call_target="tpu_custom_call" | custom-call | flops 1073741824 | bytes 8388608 | tf_op jit(solution)/shard_map/group_rows/pallas_call | solution.py:208
  135.7 1.0 copy-done
  136.7 8.1 %feed_forward.1 = bf16[256,2048]{1,0:T(8,128)(2,1)} custom-call(bf16[256,2048]{1,0:T(8,128)(2,1)} %copy-done, bf16[16,2,2,3,32,704]{5,4,3,2,1,0:T(8,128)(2,1)} %bitcast.21), custom_call_target="tpu_custom_call" | custom-call | flops 2214592512 | bytes 8388608 | tf_op jit(solution)/shard_map/feed_forward/pallas_call | solution.py:273
  144.8 18.0 %all_to_all.25 = bf16[8,32,2048]{2,1,0:T(8,128)(2,1)S(1)} all-to-all(bf16[8,32,2048]{2,1,0:T(8,128)(2,1)} %bitcast.22), channel_id=1, replica_groups=mesh['zh'=4,'zl'=4,'y1'=2,'y0'=2,'x'=4,'c'=2] {'y0','x'}, dimensions={0} | all-to-all | bytes 2097152 | tf_op jit(solution)/shard_map/all_to_all | solution.py:308
  (28 shorter events, 2.5 us)
Async XLA Ops:
  6.5 24.9 %copy-start.1 = (bf16[128,2048]{1,0:T(8,128)(2,1)S(1)}, bf16[128,2048]{1,0:T(8,128)(2,1)}, u32[]{:S(2)}) copy-start(bf16[128,2048]{1,0:T(8,128)(2,1)} %param.19) | copy-start | bytes 1572868
  6.5 130.1 %all-gather.3.cloned.1.call-start = ((), (), s32[]{:S(2)}) async-start(), calls=%async_computation.5 | async-start | bytes 9732096 | tf_op jit(solution)/shard_map/all_gather | solution.py:319
  7.5 9.4 %collective-permute-start.8 = (bf16[96,704]{1,0:T(8,128)(2,1)S(1)}, bf16[96,704]{1,0:T(8,128)(2,1)S(1)}, u32[]{:S(2)}, u32[]{:S(2)}) collective-permute-start(bf16[96,704]{1,0:T(8,128)(2,1)S(1)} %pad_maximum_fusion.2), channel_id=1, source_target_pairs={{0,16},{1,24},{8,17},{9,25},{16,0},{17,8},{24,1},{25,9},{2,18},{3,... | collective-permute-start | bytes 405512 | tf_op jit(solution)/shard_map/ppermute | solution.py:299
  13.5 6.5 %collective-permute-start.9 = (bf16[96,704]{1,0:T(8,128)(2,1)S(1)}, bf16[96,704]{1,0:T(8,128)(2,1)S(1)}, u32[]{:S(2)}, u32[]{:S(2)}) collective-permute-start(bf16[96,704]{1,0:T(8,128)(2,1)S(1)} %pad_maximum_fusion.2), channel_id=1, source_target_pairs={{0,0},{1,8},{8,1},{9,9},{16,16},{17,24},{24,17},{25,25},{2,2},{3,1... | collective-permute-start | bytes 405512 | tf_op jit(solution)/shard_map/ppermute | solution.py:299
  20.8 41.4 %copy-start.3 = (bf16[32,2048]{1,0:T(8,128)(2,1)S(1)}, bf16[32,2048]{1,0:T(8,128)(2,1)}, u32[]{:S(2)}) copy-start(bf16[32,2048]{1,0:T(8,128)(2,1)} %param.12) | copy-start | bytes 393220
  20.8 14.0 %collective-permute-start = (bf16[128,2048]{1,0:T(8,128)(2,1)}, bf16[128,2048]{1,0:T(8,128)(2,1)S(1)}, u32[]{:S(2)}, u32[]{:S(2)}) collective-permute-start(bf16[128,2048]{1,0:T(8,128)(2,1)} %param.19), channel_id=1, source_target_pairs={{0,2},{2,4},{4,6},{6,0},{1,3},{3,5},{5,7},{7,1},{8,10},{10,12},{12... | collective-permute-start | bytes 1572872 | tf_op jit(solution)/shard_map/ppermute | solution.py:304
  24.0 24.3 %collective-permute-start.1 = (bf16[128,2048]{1,0:T(8,128)(2,1)}, bf16[128,2048]{1,0:T(8,128)(2,1)S(1)}, u32[]{:S(2)}, u32[]{:S(2)}) collective-permute-start(bf16[128,2048]{1,0:T(8,128)(2,1)} %param.19), channel_id=1, source_target_pairs={{0,4},{2,6},{4,0},{6,2},{1,5},{3,7},{5,1},{7,3},{8,12},{10,14},{12... | collective-permute-start | bytes 1572872 | tf_op jit(solution)/shard_map/ppermute | solution.py:304
  28.4 22.5 %collective-permute-start.2 = (bf16[128,2048]{1,0:T(8,128)(2,1)}, bf16[128,2048]{1,0:T(8,128)(2,1)S(1)}, u32[]{:S(2)}, u32[]{:S(2)}) collective-permute-start(bf16[128,2048]{1,0:T(8,128)(2,1)} %param.19), channel_id=1, source_target_pairs={{0,6},{2,0},{4,2},{6,4},{1,7},{3,1},{5,3},{7,5},{8,14},{10,8},{12,... | collective-permute-start | bytes 1572872 | tf_op jit(solution)/shard_map/ppermute | solution.py:304
  50.9 72.1 %copy-start.4 = (bf16[2048]{0:T(1024)(128)(2,1)S(1)}, bf16[2048]{0:T(1024)(128)(2,1)}, u32[]{:S(2)}) copy-start(bf16[2048]{0:T(1024)(128)(2,1)} %param.20) | copy-start | bytes 12292
  50.9 81.5 %collective-permute-start.3 = (bf16[512,2048]{1,0:T(8,128)(2,1)S(1)}, bf16[512,2048]{1,0:T(8,128)(2,1)}, u32[]{:S(2)}, u32[]{:S(2)}) collective-permute-start(bf16[512,2048]{1,0:T(8,128)(2,1)S(1)} %constant_dynamic-update-slice_fusion.near_w_ref), channel_id=1, source_target_pairs={{0,1},{1,0},{2,3},{3,2},{4,5},{5,4},{6,7},{7,6},{8,9},{9,8},{10,11... | collective-permute-start | bytes 6291464 | tf_op jit(solution)/shard_map/ppermute | solution.py:304
  56.2 16.5 %all-to-all-start = ((f32[16,16,128]{2,1,0:T(8,128)}), f32[16,16,128]{2,1,0:T(8,128)S(1)}, u32[]{:S(2)}, u32[]{:S(2)}) async-start(f32[16,16,128]{2,1,0:T(8,128)} %get-tuple-element.12), calls=%async_computation | async-start | bytes 262144 | tf_op jit(solution)/shard_map/all_to_all | solution.py:308
  62.2 42.2 %collective-permute-start.6 = (bf16[32,2048]{1,0:T(8,128)(2,1)S(1)}, bf16[32,2048]{1,0:T(8,128)(2,1)S(1)}, u32[]{:S(2)}, u32[]{:S(2)}) collective-permute-start(bf16[32,2048]{1,0:T(8,128)(2,1)S(1)} %copy-done.3), channel_id=1, source_target_pairs={{0,6},{2,0},{4,2},{6,4},{1,7},{3,1},{5,3},{7,5},{8,14},{10,8},{12,... | collective-permute-start | bytes 393224 | tf_op jit(solution)/shard_map/ppermute | solution.py:304
  66.5 37.9 %collective-permute-start.5 = (bf16[32,2048]{1,0:T(8,128)(2,1)S(1)}, bf16[32,2048]{1,0:T(8,128)(2,1)S(1)}, u32[]{:S(2)}, u32[]{:S(2)}) collective-permute-start(bf16[32,2048]{1,0:T(8,128)(2,1)S(1)} %copy-done.3), channel_id=1, source_target_pairs={{0,4},{2,6},{4,0},{6,2},{1,5},{3,7},{5,1},{7,3},{8,12},{10,14},{12... | collective-permute-start | bytes 393224 | tf_op jit(solution)/shard_map/ppermute | solution.py:304
  70.0 34.4 %collective-permute-start.4 = (bf16[32,2048]{1,0:T(8,128)(2,1)S(1)}, bf16[32,2048]{1,0:T(8,128)(2,1)S(1)}, u32[]{:S(2)}, u32[]{:S(2)}) collective-permute-start(bf16[32,2048]{1,0:T(8,128)(2,1)S(1)} %copy-done.3), channel_id=1, source_target_pairs={{0,2},{2,4},{4,6},{6,0},{1,3},{3,5},{5,7},{7,1},{8,10},{10,12},{12... | collective-permute-start | bytes 393224 | tf_op jit(solution)/shard_map/ppermute | solution.py:304
  73.4 24.1 %all-to-all-start.1 = ((f32[4,16,128]{2,1,0:T(8,128)}), f32[4,16,128]{2,1,0:T(8,128)S(1)}, u32[]{:S(2)}, u32[]{:S(2)}) async-start(f32[4,16,128]{2,1,0:T(8,128)} %joined_state.1), calls=%async_computation.1 | async-start | bytes 65536 | tf_op jit(solution)/shard_map/all_to_all | solution.py:308
  98.2 13.4 %all-to-all-start.2 = ((f32[16,8,128]{2,1,0:T(8,128)}), f32[16,8,128]{2,1,0:T(8,128)S(1)}, u32[]{:S(2)}, u32[]{:S(2)}) async-start(f32[16,8,128]{2,1,0:T(8,128)} %incoming_state.1), calls=%async_computation.2 | async-start | bytes 131072 | tf_op jit(solution)/shard_map/all_to_all | solution.py:308
  104.5 18.6 %collective-permute-start.7 = (bf16[4,32,2048]{2,1,0:T(8,128)(2,1)S(1)}, bf16[4,32,2048]{2,1,0:T(8,128)(2,1)}, u32[]{:S(2)}, u32[]{:S(2)}) collective-permute-start(bf16[4,32,2048]{2,1,0:T(8,128)(2,1)S(1)} %pad_maximum_fusion.near_s_ref), channel_id=1, source_target_pairs={{0,8},{8,0},{1,9},{9,1},{2,10},{10,2},{3,11},{11,3},{4,12},{12,4},... | collective-permute-start | bytes 1572872 | tf_op jit(solution)/shard_map/ppermute | solution.py:304
  111.6 0.6 copy-start.2
  114.4 18.1 %all-to-all-start.3 = ((bf16[16,4,32,128]{3,2,1,0:T(8,128)(2,1)}), bf16[16,4,32,128]{3,2,1,0:T(8,128)(2,1)S(1)}, u32[]{:S(2)}, u32[]{:S(2)}) async-start(bf16[16,4,32,128]{3,2,1,0:T(8,128)(2,1)} %bitcast.23), calls=%async_computation.3 | async-start | bytes 1048576 | tf_op jit(solution)/shard_map/all_to_all | solution.py:308
  135.7 1.0 copy-start
Sparse Core Ops, SparseCore 0:
  20.9 84.5 all-gather.2

commit v6 on v5

--- a/solution.py
+++ b/solution.py
@@ -159,7 +159,7 @@
 
 
 def rows_kernel(
-    here_ref, mixed_ref, near_w_ref, far_w_ref, near_s_ref, far_s_ref, gain_ref, normed_ref, own_ref, residual
+    here_ref, mixed_ref, near_w_ref, far_w_ref, near_s_ref, far_s_ref, gain_ref, normed_ref, own_ref, residual, normed, sems
 ):
     halves, _, blocks, lines, head_dim = mixed_ref.shape
     count, width = normed_ref.shape
@@ -195,11 +195,16 @@
         residual[:, span] = part
         squares += jnp.sum(part * part, axis=-1, keepdims=True)
     factor = lax.rsqrt(squares / width + EPS)
+    copies = []
     for n in range(4):
         span = slice(n * step, (n + 1) * step)
-        normed_ref[:, span] = (residual[:, span] * factor * gain_ref[:, span].astype(F32)).astype(BF16)
+        normed[:, span] = (residual[:, span] * factor * gain_ref[:, span].astype(F32)).astype(BF16)
+        copies.append(pltpu.make_async_copy(normed.at[:, span], normed_ref.at[:, span], sems.at[n]))
+        copies[n].start()
     first = pl.multiple_of((y0 * blocks + x) * lines, lines)
     own_ref[...] = residual[pl.ds(first, lines), :]
+    for copy in copies:
+        copy.wait()
 
 
 def group_rows(here, mixed, near_w, far_w, near_s, far_s, gain):
@@ -212,23 +217,26 @@
             jax.ShapeDtypeStruct((lines, width), F32),
         ),
         in_specs=[pl.BlockSpec(memory_space=pltpu.SMEM)] + vmem(6),
-        out_specs=vmem(2),
-        scratch_shapes=[pltpu.VMEM((count, width), F32)],
+        out_specs=[pl.BlockSpec(memory_space=pltpu.HBM)] + vmem(1),
+        scratch_shapes=[
+            pltpu.VMEM((count, width), F32),
+            pltpu.VMEM((count, width), BF16),
+            pltpu.SemaphoreType.DMA((4,)),
+        ],
         cost_estimate=kernel_cost(2 * count * width * 1024, 2**23),
         compiler_params=pltpu.CompilerParams(vmem_limit_bytes=20 * 2**20),
         name="group_rows",
     )(here, mixed, near_w, far_w, near_s, far_s, gain)
 
 
-CHUNKS = 4
-
-
-def ffn_kernel(rows_ref, weight_ref, out_ref, held, sems):
-    z, _, _, _, lines, hidden_width = weight_ref.shape
-    each = z // CHUNKS
-    depth = each * 4 * lines
+CHUNKS = (2, 1, 1)
+
+
+def ffn_kernel(rows_ref, weight_ref, out_ref, rows, held, rows_sem, sems):
+    z, _, _, kinds, lines, hidden_width = weight_ref.shape
 
     def copies(kind, n):
+        each = z // CHUNKS[kind]
         span = pl.ds(n * each, each)
         return [
             pltpu.make_async_copy(
@@ -240,31 +248,33 @@
             for y0 in range(2)
         ]
 
-    for n in range(CHUNKS):
-        for kind in (0, 1):
+    def arrived(kind, n):
+        each = z // CHUNKS[kind]
+        for copy in copies(kind, n):
+            copy.wait()
+        depth = each * 4 * lines
+        return held[kind, n * each : (n + 1) * each].reshape(depth, hidden_width), depth
+
+    fetch = pltpu.make_async_copy(rows_ref, rows, rows_sem)
+    fetch.start()
+    for kind in range(kinds):
+        for n in range(CHUNKS[kind]):
             for copy in copies(kind, n):
                 copy.start()
-    for n in range(CHUNKS):
-        for copy in copies(2, n):
-            copy.start()
-
-    def block(kind, n):
-        return held[kind, n * each : (n + 1) * each].reshape(depth, hidden_width)
-
-    gate_sum = up_sum = None
-    for n in range(CHUNKS):
-        for kind in (0, 1):
-            for copy in copies(kind, n):
-                copy.wait()
-        rows = rows_ref[:, n * depth : (n + 1) * depth]
-        gate_part, up_part = dot(rows, block(0, n)), dot(rows, block(1, n))
-        gate_sum = gate_part if gate_sum is None else gate_sum + gate_part
-        up_sum = up_part if up_sum is None else up_sum + up_part
+    fetch.wait()
+    sums = []
+    for kind in (0, 1):
+        total = None
+        for n in range(CHUNKS[kind]):
+            block, depth = arrived(kind, n)
+            part = dot(rows[:, n * depth : (n + 1) * depth], block)
+            total = part if total is None else total + part
+        sums.append(total)
+    gate_sum, up_sum = sums
     hidden = (gate_sum * jax.nn.sigmoid(gate_sum) * up_sum).astype(BF16)
-    for n in range(CHUNKS):
-        for copy in copies(2, n):
-            copy.wait()
-        out_ref[:, n * depth : (n + 1) * depth] = dot_nt(hidden, block(2, n)).astype(BF16)
+    for n in range(CHUNKS[2]):
+        block, depth = arrived(2, n)
+        out_ref[:, n * depth : (n + 1) * depth] = dot_nt(hidden, block).astype(BF16)
 
 
 def feed_forward(rows, weights):
@@ -273,17 +283,16 @@
     return pl.pallas_call(
         ffn_kernel,
         out_shape=jax.ShapeDtypeStruct((count, width), BF16),
-        in_specs=[
-            pl.BlockSpec(memory_space=pltpu.VMEM),
-            pl.BlockSpec(memory_space=pl.ANY),
-        ],
+        in_specs=[pl.BlockSpec(memory_space=pltpu.HBM)] * 2,
         out_specs=pl.BlockSpec(memory_space=pltpu.VMEM),
         scratch_shapes=[
+            pltpu.VMEM((count, width), BF16),
             pltpu.VMEM((kinds, z, y1, y0, lines, hidden_width), BF16),
-            pltpu.SemaphoreType.DMA((kinds, CHUNKS, 4)),
+            pltpu.SemaphoreType.DMA,
+            pltpu.SemaphoreType.DMA((kinds, max(CHUNKS), 4)),
         ],
         cost_estimate=kernel_cost(6 * count * width * hidden_width, 2**23, count * hidden_width),
-        compiler_params=pltpu.CompilerParams(vmem_limit_bytes=56 * 2**20),
+        compiler_params=pltpu.CompilerParams(vmem_limit_bytes=52 * 2**20),
         name="feed_forward",
     )(rows, weights)
 

time: 171 us -> 171 us (level)
  no operation moved by 1% of the time
where the time goes in v6:
time: 171 us; the launch traced here: 170 us
  starting transfers between devices  67.9 us (40%)
  waiting for transfers between devices  49.8 us (29%)
  blocking collectives  17.8 us (10%)
  Pallas kernels  16.5 us (10%)
  between operations  13.6 us (8%)
  other arithmetic  2.67 us (2%)
  local copies, waits for them, and re-layouts  1.79 us (1%)
    all_to_all x4, starting transfers between devices, exchange(): return lax.all_to_all(tiles, axes, split_axis=0, concat_axis=0, tiled=True)  32.9 us
    ppermute x8, starting transfers between devices, shifted(): lax.ppermute(value, axis, [(i, (i + by) % length) for i in range(length)])  27.1 us
    all_to_all x4, waiting for transfers between devices, exchange(): return lax.all_to_all(tiles, axes, split_axis=0, concat_axis=0, tiled=True)  25.9 us
    ppermute x8, waiting for transfers between devices, shifted(): lax.ppermute(value, axis, [(i, (i + by) % length) for i in range(length)])  19.3 us
    all_to_all x1, blocking collectives, exchange(): return lax.all_to_all(tiles, axes, split_axis=0, concat_axis=0, tiled=True)  17.8 us
    ppermute x2, starting transfers between devices, moved(): return lax.ppermute(value, axes, pairs)  7.94 us
    pallas_call x1, Pallas kernels, feed_forward(): pl.pallas_call(ffn_kernel, out_shape=jax.ShapeDtypeStruct((count, width),...  7.66 us
    ppermute x2, waiting for transfers between devices, moved(): return lax.ppermute(value, axes, pairs)  4.53 us
  transfers between devices with their start and end apart: 15, of which 9 were waited for; matrix products, arithmetic and copies ran while one was open for 0% of the time, Pallas kernels for 5%

profile of v6, /device:TPU:1, one launch (start us, length us, event | category | flops | bytes accessed | tf_op | source)
XLA Modules:
  0.0 170.0 jit_solution(120952059321960396)
XLA Ops:
  6.5 0.9 pad_maximum_fusion.2
  7.5 6.0 %collective-permute-start.8 = (bf16[96,704]{1,0:T(8,128)(2,1)S(1)}, bf16[96,704]{1,0:T(8,128)(2,1)S(1)}, u32[]{:S(2)}, u32[]{:S(2)}) collective-permute-start(bf16[96,704]{1,0:T(8,128)(2,1)S(1)} %pad_maximum_fusion.2), channel_id=1, source_target_pairs={{0,16},{1,24},{8,17},{9,25},{16,0},{17,8},{24,1},{25,9},{2,18},{3,... | collective-permute-start | bytes 405512 | tf_op jit(solution)/shard_map/ppermute | solution.py:308
  13.5 1.9 %collective-permute-start.9 = (bf16[96,704]{1,0:T(8,128)(2,1)S(1)}, bf16[96,704]{1,0:T(8,128)(2,1)S(1)}, u32[]{:S(2)}, u32[]{:S(2)}) collective-permute-start(bf16[96,704]{1,0:T(8,128)(2,1)S(1)} %pad_maximum_fusion.2), channel_id=1, source_target_pairs={{0,0},{1,8},{8,1},{9,9},{16,16},{17,24},{24,17},{25,25},{2,2},{3,1... | collective-permute-start | bytes 405512 | tf_op jit(solution)/shard_map/ppermute | solution.py:308
  15.4 1.4 collective-permute-done.8
  16.9 3.1 %collective-permute-done.9 = bf16[96,704]{1,0:T(8,128)(2,1)S(1)} collective-permute-done((bf16[96,704]{1,0:T(8,128)(2,1)S(1)}, bf16[96,704]{1,0:T(8,128)(2,1)S(1)}, u32[]{:S(2)}, u32[]{:S(2)}) %collective-permute-start.9) | collective-permute-done | bytes 135200 | tf_op jit(solution)/shard_map/ppermute | solution.py:308
  20.0 0.8 pad_maximum_fusion.1
  20.8 3.3 %collective-permute-start = (bf16[128,2048]{1,0:T(8,128)(2,1)}, bf16[128,2048]{1,0:T(8,128)(2,1)S(1)}, u32[]{:S(2)}, u32[]{:S(2)}) collective-permute-start(bf16[128,2048]{1,0:T(8,128)(2,1)} %param.19), channel_id=1, source_target_pairs={{0,2},{2,4},{4,6},{6,0},{1,3},{3,5},{5,7},{7,1},{8,10},{10,12},{12... | collective-permute-start | bytes 1572872 | tf_op jit(solution)/shard_map/ppermute | solution.py:313
  24.0 4.4 %collective-permute-start.1 = (bf16[128,2048]{1,0:T(8,128)(2,1)}, bf16[128,2048]{1,0:T(8,128)(2,1)S(1)}, u32[]{:S(2)}, u32[]{:S(2)}) collective-permute-start(bf16[128,2048]{1,0:T(8,128)(2,1)} %param.19), channel_id=1, source_target_pairs={{0,4},{2,6},{4,0},{6,2},{1,5},{3,7},{5,1},{7,3},{8,12},{10,14},{12... | collective-permute-start | bytes 1572872 | tf_op jit(solution)/shard_map/ppermute | solution.py:313
  28.4 3.1 %collective-permute-start.2 = (bf16[128,2048]{1,0:T(8,128)(2,1)}, bf16[128,2048]{1,0:T(8,128)(2,1)S(1)}, u32[]{:S(2)}, u32[]{:S(2)}) collective-permute-start(bf16[128,2048]{1,0:T(8,128)(2,1)} %param.19), channel_id=1, source_target_pairs={{0,6},{2,0},{4,2},{6,4},{1,7},{3,1},{5,3},{7,5},{8,14},{10,8},{12,... | collective-permute-start | bytes 1572872 | tf_op jit(solution)/shard_map/ppermute | solution.py:313
  31.5 3.3 %collective-permute-done = bf16[128,2048]{1,0:T(8,128)(2,1)S(1)} collective-permute-done((bf16[128,2048]{1,0:T(8,128)(2,1)}, bf16[128,2048]{1,0:T(8,128)(2,1)S(1)}, u32[]{:S(2)}, u32[]{:S(2)}) %collective-permute-start) | collective-permute-done | bytes 524320 | tf_op jit(solution)/shard_map/ppermute | solution.py:313
  34.9 13.5 %collective-permute-done.1 = bf16[128,2048]{1,0:T(8,128)(2,1)S(1)} collective-permute-done((bf16[128,2048]{1,0:T(8,128)(2,1)}, bf16[128,2048]{1,0:T(8,128)(2,1)S(1)}, u32[]{:S(2)}, u32[]{:S(2)}) %collective-permute-start.1) | collective-permute-done | bytes 524320 | tf_op jit(solution)/shard_map/ppermute | solution.py:313
  48.3 2.5 %collective-permute-done.2 = bf16[128,2048]{1,0:T(8,128)(2,1)S(1)} collective-permute-done((bf16[128,2048]{1,0:T(8,128)(2,1)}, bf16[128,2048]{1,0:T(8,128)(2,1)S(1)}, u32[]{:S(2)}, u32[]{:S(2)}) %collective-permute-start.2) | collective-permute-done | bytes 524320 | tf_op jit(solution)/shard_map/ppermute | solution.py:313
  50.9 3.4 %collective-permute-start.3 = (bf16[512,2048]{1,0:T(8,128)(2,1)S(1)}, bf16[512,2048]{1,0:T(8,128)(2,1)}, u32[]{:S(2)}, u32[]{:S(2)}) collective-permute-start(bf16[512,2048]{1,0:T(8,128)(2,1)S(1)} %constant_dynamic-update-slice_fusion.near_w_ref), channel_id=1, source_target_pairs={{0,1},{1,0},{2,3},{3,2},{4,5},{5,4},{6,7},{7,6},{8,9},{9,8},{10,11... | collective-permute-start | bytes 6291464 | tf_op jit(solution)/shard_map/ppermute | solution.py:313
  54.3 1.9 %retention.1 = (f32[256,128]{1,0:T(8,128)}, bf16[256,128]{1,0:T(8,128)(2,1)}, f32[16,16,128]{2,1,0:T(8,128)}) custom-call(bf16[256,128]{1,0:T(8,128)(2,1)} %q_ref.1, bf16[256,128]{1,0:T(8,128)(2,1)} %k_ref.1, bf16[256,128]{1,0:T(8,128)(2,1)} %v_ref.1, f32[1,256]{1,0:T(1,128)} %bitcast.30), custom_call_target="tpu_custom_call" | custom-call | flops 50331648 | bytes 1048576 | tf_op jit(solution)/shard_map/retention/pallas_call | solution.py:67
  56.2 5.9 %all-to-all-start = ((f32[16,16,128]{2,1,0:T(8,128)}), f32[16,16,128]{2,1,0:T(8,128)S(1)}, u32[]{:S(2)}, u32[]{:S(2)}) async-start(f32[16,16,128]{2,1,0:T(8,128)} %get-tuple-element.12), calls=%async_computation | async-start | bytes 262144 | tf_op jit(solution)/shard_map/all_to_all | solution.py:317
  62.2 4.3 %collective-permute-start.6 = (bf16[32,2048]{1,0:T(8,128)(2,1)S(1)}, bf16[32,2048]{1,0:T(8,128)(2,1)S(1)}, u32[]{:S(2)}, u32[]{:S(2)}) collective-permute-start(bf16[32,2048]{1,0:T(8,128)(2,1)S(1)} %copy-done.3), channel_id=1, source_target_pairs={{0,6},{2,0},{4,2},{6,4},{1,7},{3,1},{5,3},{7,5},{8,14},{10,8},{12,... | collective-permute-start | bytes 393224 | tf_op jit(solution)/shard_map/ppermute | solution.py:313
  66.5 3.6 %collective-permute-start.5 = (bf16[32,2048]{1,0:T(8,128)(2,1)S(1)}, bf16[32,2048]{1,0:T(8,128)(2,1)S(1)}, u32[]{:S(2)}, u32[]{:S(2)}) collective-permute-start(bf16[32,2048]{1,0:T(8,128)(2,1)S(1)} %copy-done.3), channel_id=1, source_target_pairs={{0,4},{2,6},{4,0},{6,2},{1,5},{3,7},{5,1},{7,3},{8,12},{10,14},{12... | collective-permute-start | bytes 393224 | tf_op jit(solution)/shard_map/ppermute | solution.py:313
  70.0 1.9 %collective-permute-start.4 = (bf16[32,2048]{1,0:T(8,128)(2,1)S(1)}, bf16[32,2048]{1,0:T(8,128)(2,1)S(1)}, u32[]{:S(2)}, u32[]{:S(2)}) collective-permute-start(bf16[32,2048]{1,0:T(8,128)(2,1)S(1)} %copy-done.3), channel_id=1, source_target_pairs={{0,2},{2,4},{4,6},{6,0},{1,3},{3,5},{5,7},{7,1},{8,10},{10,12},{12... | collective-permute-start | bytes 393224 | tf_op jit(solution)/shard_map/ppermute | solution.py:313
  72.0 0.8 all-to-all-done.states_ref
  73.4 12.2 %all-to-all-start.1 = ((f32[4,16,128]{2,1,0:T(8,128)}), f32[4,16,128]{2,1,0:T(8,128)S(1)}, u32[]{:S(2)}, u32[]{:S(2)}) async-start(f32[4,16,128]{2,1,0:T(8,128)} %joined_state.1), calls=%async_computation.1 | async-start | bytes 65536 | tf_op jit(solution)/shard_map/all_to_all | solution.py:317
  85.6 11.9 %all-to-all-done.1.joined_ref = f32[4,16,128]{2,1,0:T(8,128)S(1)} async-done(((f32[4,16,128]{2,1,0:T(8,128)}), f32[4,16,128]{2,1,0:T(8,128)S(1)}, u32[]{:S(2)}, u32[]{:S(2)}) %all-to-all-start.1) | async-done | bytes 32800 | tf_op jit(solution)/shard_map/all_to_all | solution.py:317
  97.5 0.7 incoming_state.1
  98.2 6.1 %all-to-all-start.2 = ((f32[16,8,128]{2,1,0:T(8,128)}), f32[16,8,128]{2,1,0:T(8,128)S(1)}, u32[]{:S(2)}, u32[]{:S(2)}) async-start(f32[16,8,128]{2,1,0:T(8,128)} %incoming_state.1), calls=%async_computation.2 | async-start | bytes 131072 | tf_op jit(solution)/shard_map/all_to_all | solution.py:317
  104.5 3.3 %collective-permute-start.7 = (bf16[4,32,2048]{2,1,0:T(8,128)(2,1)S(1)}, bf16[4,32,2048]{2,1,0:T(8,128)(2,1)}, u32[]{:S(2)}, u32[]{:S(2)}) collective-permute-start(bf16[4,32,2048]{2,1,0:T(8,128)(2,1)S(1)} %pad_maximum_fusion.near_s_ref), channel_id=1, source_target_pairs={{0,8},{8,0},{1,9},{9,1},{2,10},{10,2},{3,11},{11,3},{4,12},{12,4},... | collective-permute-start | bytes 1572872 | tf_op jit(solution)/shard_map/ppermute | solution.py:313
  107.8 3.9 %all-to-all-done.2 = f32[16,8,128]{2,1,0:T(8,128)S(1)} async-done(((f32[16,8,128]{2,1,0:T(8,128)}), f32[16,8,128]{2,1,0:T(8,128)S(1)}, u32[]{:S(2)}, u32[]{:S(2)}) %all-to-all-start.2) | async-done | bytes 65568 | tf_op jit(solution)/shard_map/all_to_all | solution.py:317
  112.3 2.1 %mix.1 = bf16[8,2,4,32,128]{4,3,2,1,0:T(8,128)(2,1)} custom-call(f32[256,128]{1,0:T(8,128)} %get-tuple-element.10.within_ref, bf16[256,128]{1,0:T(8,128)(2,1)} %get-tuple-element.11.carry_q_ref, f32[128,128]{1,0:T(8,128)} %bitcast.24, bf16[256,128]{1,0:T(8,128)(2,1)} %gate_ref.1, bf16[1,128]{1,0:T(2,128)(2,1)} %bitcast.31), custom_call_target="tpu_custom_call" | custom-call | flops 8388608 | bytes 1048576 | tf_op jit(solution)/shard_map/mix/pallas_call | solution.py:151
  114.4 8.6 %all-to-all-start.3 = ((bf16[16,4,32,128]{3,2,1,0:T(8,128)(2,1)}), bf16[16,4,32,128]{3,2,1,0:T(8,128)(2,1)S(1)}, u32[]{:S(2)}, u32[]{:S(2)}) async-start(bf16[16,4,32,128]{3,2,1,0:T(8,128)(2,1)} %bitcast.23), calls=%async_computation.3 | async-start | bytes 1048576 | tf_op jit(solution)/shard_map/all_to_all | solution.py:317
  123.1 9.4 %all-to-all-done.3 = bf16[16,4,32,128]{3,2,1,0:T(8,128)(2,1)S(1)} async-done(((bf16[16,4,32,128]{3,2,1,0:T(8,128)(2,1)}), bf16[16,4,32,128]{3,2,1,0:T(8,128)(2,1)S(1)}, u32[]{:S(2)}, u32[]{:S(2)}) %all-to-all-start.3) | async-done | bytes 524320 | tf_op jit(solution)/shard_map/all_to_all | solution.py:317
  132.5 3.4 %group_rows.1 = (bf16[256,2048]{1,0:T(8,128)(2,1)S(1)}, f32[32,2048]{1,0:T(8,128)S(1)}) custom-call(s32[3]{0:T(128)S(1)} %pad_add_fusion.here_ref, bf16[2,8,4,32,128]{4,3,2,1,0:T(8,128)(2,1)S(1)} %bitcast.21, bf16[512,2048]{1,0:T(8,128)(2,1)S(1)} %constant_dynamic-update-slice_fusion.near_w_ref, bf16[512,2048]{1,0:T(8,128)(2,1)} %collective-permute-done.3.far_w_ref, ...), custom_call_target="tpu_custom_call" | custom-call | flops 1073741824 | bytes 8388608 | tf_op jit(solution)/shard_map/group_rows/pallas_call | solution.py:213
  135.9 1.0 copy-done
  136.9 7.7 %feed_forward.1 = bf16[256,2048]{1,0:T(8,128)(2,1)S(1)} custom-call(bf16[256,2048]{1,0:T(8,128)(2,1)} %copy-done, bf16[16,2,2,3,32,704]{5,4,3,2,1,0:T(8,128)(2,1)} %bitcast.22), custom_call_target="tpu_custom_call" | custom-call | flops 2214592512 | bytes 8388608 | tf_op jit(solution)/shard_map/feed_forward/pallas_call | solution.py:283
  144.5 17.8 %all_to_all.25 = bf16[8,32,2048]{2,1,0:T(8,128)(2,1)S(1)} all-to-all(bf16[8,32,2048]{2,1,0:T(8,128)(2,1)S(1)} %bitcast.20), channel_id=1, replica_groups=mesh['zh'=4,'zl'=4,'y1'=2,'y0'=2,'x'=4,'c'=2] {'y0','x'}, dimensions={0} | all-to-all | bytes 2097152 | tf_op jit(solution)/shard_map/all_to_all | solution.py:317
  (28 shorter events, 2.5 us)
Async XLA Ops:
  6.5 24.9 %copy-start.1 = (bf16[128,2048]{1,0:T(8,128)(2,1)S(1)}, bf16[128,2048]{1,0:T(8,128)(2,1)}, u32[]{:S(2)}) copy-start(bf16[128,2048]{1,0:T(8,128)(2,1)} %param.19) | copy-start | bytes 1572868
  6.5 130.3 %all-gather.3.cloned.1.call-start = ((), (), s32[]{:S(2)}) async-start(), calls=%async_computation.5 | async-start | bytes 9732096 | tf_op jit(solution)/shard_map/all_gather | solution.py:328
  7.5 9.4 %collective-permute-start.8 = (bf16[96,704]{1,0:T(8,128)(2,1)S(1)}, bf16[96,704]{1,0:T(8,128)(2,1)S(1)}, u32[]{:S(2)}, u32[]{:S(2)}) collective-permute-start(bf16[96,704]{1,0:T(8,128)(2,1)S(1)} %pad_maximum_fusion.2), channel_id=1, source_target_pairs={{0,16},{1,24},{8,17},{9,25},{16,0},{17,8},{24,1},{25,9},{2,18},{3,... | collective-permute-start | bytes 405512 | tf_op jit(solution)/shard_map/ppermute | solution.py:308
  13.5 6.5 %collective-permute-start.9 = (bf16[96,704]{1,0:T(8,128)(2,1)S(1)}, bf16[96,704]{1,0:T(8,128)(2,1)S(1)}, u32[]{:S(2)}, u32[]{:S(2)}) collective-permute-start(bf16[96,704]{1,0:T(8,128)(2,1)S(1)} %pad_maximum_fusion.2), channel_id=1, source_target_pairs={{0,0},{1,8},{8,1},{9,9},{16,16},{17,24},{24,17},{25,25},{2,2},{3,1... | collective-permute-start | bytes 405512 | tf_op jit(solution)/shard_map/ppermute | solution.py:308
  20.8 41.4 %copy-start.3 = (bf16[32,2048]{1,0:T(8,128)(2,1)S(1)}, bf16[32,2048]{1,0:T(8,128)(2,1)}, u32[]{:S(2)}) copy-start(bf16[32,2048]{1,0:T(8,128)(2,1)} %param.12) | copy-start | bytes 393220
  20.8 14.0 %collective-permute-start = (bf16[128,2048]{1,0:T(8,128)(2,1)}, bf16[128,2048]{1,0:T(8,128)(2,1)S(1)}, u32[]{:S(2)}, u32[]{:S(2)}) collective-permute-start(bf16[128,2048]{1,0:T(8,128)(2,1)} %param.19), channel_id=1, source_target_pairs={{0,2},{2,4},{4,6},{6,0},{1,3},{3,5},{5,7},{7,1},{8,10},{10,12},{12... | collective-permute-start | bytes 1572872 | tf_op jit(solution)/shard_map/ppermute | solution.py:313
  24.0 24.3 %collective-permute-start.1 = (bf16[128,2048]{1,0:T(8,128)(2,1)}, bf16[128,2048]{1,0:T(8,128)(2,1)S(1)}, u32[]{:S(2)}, u32[]{:S(2)}) collective-permute-start(bf16[128,2048]{1,0:T(8,128)(2,1)} %param.19), channel_id=1, source_target_pairs={{0,4},{2,6},{4,0},{6,2},{1,5},{3,7},{5,1},{7,3},{8,12},{10,14},{12... | collective-permute-start | bytes 1572872 | tf_op jit(solution)/shard_map/ppermute | solution.py:313
  28.4 22.5 %collective-permute-start.2 = (bf16[128,2048]{1,0:T(8,128)(2,1)}, bf16[128,2048]{1,0:T(8,128)(2,1)S(1)}, u32[]{:S(2)}, u32[]{:S(2)}) collective-permute-start(bf16[128,2048]{1,0:T(8,128)(2,1)} %param.19), channel_id=1, source_target_pairs={{0,6},{2,0},{4,2},{6,4},{1,7},{3,1},{5,3},{7,5},{8,14},{10,8},{12,... | collective-permute-start | bytes 1572872 | tf_op jit(solution)/shard_map/ppermute | solution.py:313
  50.9 72.1 %copy-start.4 = (bf16[2048]{0:T(1024)(128)(2,1)S(1)}, bf16[2048]{0:T(1024)(128)(2,1)}, u32[]{:S(2)}) copy-start(bf16[2048]{0:T(1024)(128)(2,1)} %param.20) | copy-start | bytes 12292
  50.9 81.5 %collective-permute-start.3 = (bf16[512,2048]{1,0:T(8,128)(2,1)S(1)}, bf16[512,2048]{1,0:T(8,128)(2,1)}, u32[]{:S(2)}, u32[]{:S(2)}) collective-permute-start(bf16[512,2048]{1,0:T(8,128)(2,1)S(1)} %constant_dynamic-update-slice_fusion.near_w_ref), channel_id=1, source_target_pairs={{0,1},{1,0},{2,3},{3,2},{4,5},{5,4},{6,7},{7,6},{8,9},{9,8},{10,11... | collective-permute-start | bytes 6291464 | tf_op jit(solution)/shard_map/ppermute | solution.py:313
  56.2 16.5 %all-to-all-start = ((f32[16,16,128]{2,1,0:T(8,128)}), f32[16,16,128]{2,1,0:T(8,128)S(1)}, u32[]{:S(2)}, u32[]{:S(2)}) async-start(f32[16,16,128]{2,1,0:T(8,128)} %get-tuple-element.12), calls=%async_computation | async-start | bytes 262144 | tf_op jit(solution)/shard_map/all_to_all | solution.py:317
  62.2 42.2 %collective-permute-start.6 = (bf16[32,2048]{1,0:T(8,128)(2,1)S(1)}, bf16[32,2048]{1,0:T(8,128)(2,1)S(1)}, u32[]{:S(2)}, u32[]{:S(2)}) collective-permute-start(bf16[32,2048]{1,0:T(8,128)(2,1)S(1)} %copy-done.3), channel_id=1, source_target_pairs={{0,6},{2,0},{4,2},{6,4},{1,7},{3,1},{5,3},{7,5},{8,14},{10,8},{12,... | collective-permute-start | bytes 393224 | tf_op jit(solution)/shard_map/ppermute | solution.py:313
  66.5 37.9 %collective-permute-start.5 = (bf16[32,2048]{1,0:T(8,128)(2,1)S(1)}, bf16[32,2048]{1,0:T(8,128)(2,1)S(1)}, u32[]{:S(2)}, u32[]{:S(2)}) collective-permute-start(bf16[32,2048]{1,0:T(8,128)(2,1)S(1)} %copy-done.3), channel_id=1, source_target_pairs={{0,4},{2,6},{4,0},{6,2},{1,5},{3,7},{5,1},{7,3},{8,12},{10,14},{12... | collective-permute-start | bytes 393224 | tf_op jit(solution)/shard_map/ppermute | solution.py:313
  70.0 34.4 %collective-permute-start.4 = (bf16[32,2048]{1,0:T(8,128)(2,1)S(1)}, bf16[32,2048]{1,0:T(8,128)(2,1)S(1)}, u32[]{:S(2)}, u32[]{:S(2)}) collective-permute-start(bf16[32,2048]{1,0:T(8,128)(2,1)S(1)} %copy-done.3), channel_id=1, source_target_pairs={{0,2},{2,4},{4,6},{6,0},{1,3},{3,5},{5,7},{7,1},{8,10},{10,12},{12... | collective-permute-start | bytes 393224 | tf_op jit(solution)/shard_map/ppermute | solution.py:313
  73.4 24.1 %all-to-all-start.1 = ((f32[4,16,128]{2,1,0:T(8,128)}), f32[4,16,128]{2,1,0:T(8,128)S(1)}, u32[]{:S(2)}, u32[]{:S(2)}) async-start(f32[4,16,128]{2,1,0:T(8,128)} %joined_state.1), calls=%async_computation.1 | async-start | bytes 65536 | tf_op jit(solution)/shard_map/all_to_all | solution.py:317
  98.2 13.4 %all-to-all-start.2 = ((f32[16,8,128]{2,1,0:T(8,128)}), f32[16,8,128]{2,1,0:T(8,128)S(1)}, u32[]{:S(2)}, u32[]{:S(2)}) async-start(f32[16,8,128]{2,1,0:T(8,128)} %incoming_state.1), calls=%async_computation.2 | async-start | bytes 131072 | tf_op jit(solution)/shard_map/all_to_all | solution.py:317
  104.5 18.6 %collective-permute-start.7 = (bf16[4,32,2048]{2,1,0:T(8,128)(2,1)S(1)}, bf16[4,32,2048]{2,1,0:T(8,128)(2,1)}, u32[]{:S(2)}, u32[]{:S(2)}) collective-permute-start(bf16[4,32,2048]{2,1,0:T(8,128)(2,1)S(1)} %pad_maximum_fusion.near_s_ref), channel_id=1, source_target_pairs={{0,8},{8,0},{1,9},{9,1},{2,10},{10,2},{3,11},{11,3},{4,12},{12,4},... | collective-permute-start | bytes 1572872 | tf_op jit(solution)/shard_map/ppermute | solution.py:313
  111.6 0.6 copy-start.2
  114.4 18.1 %all-to-all-start.3 = ((bf16[16,4,32,128]{3,2,1,0:T(8,128)(2,1)}), bf16[16,4,32,128]{3,2,1,0:T(8,128)(2,1)S(1)}, u32[]{:S(2)}, u32[]{:S(2)}) async-start(bf16[16,4,32,128]{3,2,1,0:T(8,128)(2,1)} %bitcast.23), calls=%async_computation.3 | async-start | bytes 1048576 | tf_op jit(solution)/shard_map/all_to_all | solution.py:317
  135.9 1.0 copy-start
Sparse Core Ops, SparseCore 0:
  20.9 84.5 all-gather.2

commit v7 on v6

--- a/solution.py
+++ b/solution.py
@@ -12,8 +12,9 @@
 SP = Z + Y
 TP = ("x", "c")
 GROUP = ("y0", "x")
-SIZES = {"zh": 4, "zl": 4, "y1": 2, "y0": 2, "x": 4, "c": 2}
+SIZES = {"zh": 8, "zl": 2, "y1": 2, "y0": 2, "x": 4, "c": 2}
 EPS = 1e-6
+NEIGHBOURS = 8
 F32, BF16 = jnp.float32, jnp.bfloat16
 
 
@@ -63,13 +64,13 @@
 
 def retention(q, k, v, decay):
     rows, head_dim = q.shape
-    part = head_dim // 16
+    part = head_dim // NEIGHBOURS
     return pl.pallas_call(
         retention_kernel,
         out_shape=(
             jax.ShapeDtypeStruct((rows, head_dim), F32),
             jax.ShapeDtypeStruct((rows, head_dim), BF16),
-            jax.ShapeDtypeStruct((16, part + 8, head_dim), F32),
+            jax.ShapeDtypeStruct((NEIGHBOURS, part + 8, head_dim), F32),
         ),
         in_specs=vmem(4),
         out_specs=vmem(3),
@@ -84,7 +85,7 @@
     total = states_ref[0, part:, :]
     for n in range(1, states_ref.shape[0]):
         own = states_ref[n, part:, :]
-        state = jnp.exp(own) * state + states_ref[n, :part, :]
+        state = jnp.exp(own[:1]) * state + states_ref[n, :part, :]
         total = total + own
     for n in range(out_ref.shape[0]):
         out_ref[n, :part, :] = state
@@ -95,7 +96,7 @@
     _, lines, width = states.shape
     return pl.pallas_call(
         joined_kernel,
-        out_shape=jax.ShapeDtypeStruct((4, lines, width), F32),
+        out_shape=jax.ShapeDtypeStruct((SIZES["zh"], lines, width), F32),
         in_specs=vmem(1),
         out_specs=pl.BlockSpec(memory_space=pltpu.VMEM),
         cost_estimate=kernel_cost(2**18, 2**18, 2**10),
@@ -109,11 +110,11 @@
     here = here_ref[0]
     carried = jnp.zeros(out_ref.shape[1:], F32)
     for n in range(joined_ref.shape[0]):
-        after = jnp.exp(joined_ref[n, part:, :]) * carried + joined_ref[n, :part, :]
+        after = jnp.exp(joined_ref[n, part : part + 1, :]) * carried + joined_ref[n, :part, :]
         carried = jnp.where(n < here, after, carried)
     for n in range(out_ref.shape[0]):
         out_ref[n] = carried
-        carried = jnp.exp(states_ref[n, part:, :]) * carried + states_ref[n, :part, :]
+        carried = jnp.exp(states_ref[n, part : part + 1, :]) * carried + states_ref[n, :part, :]
 
 
 def incoming_state(here, joined, states):
@@ -230,6 +231,7 @@
 
 
 CHUNKS = (2, 1, 1)
+AHEAD = 2
 
 
 def ffn_kernel(rows_ref, weight_ref, out_ref, rows, held, rows_sem, sems):
@@ -248,19 +250,25 @@
             for y0 in range(2)
         ]
 
+    order = [(kind, n) for kind in range(kinds) for n in range(CHUNKS[kind])]
+
+    def start(at):
+        for place in order[at : at + 1]:
+            for copy in copies(*place):
+                copy.start()
+
     def arrived(kind, n):
         each = z // CHUNKS[kind]
         for copy in copies(kind, n):
             copy.wait()
+        start(order.index((kind, n)) + AHEAD)
         depth = each * 4 * lines
         return held[kind, n * each : (n + 1) * each].reshape(depth, hidden_width), depth
 
     fetch = pltpu.make_async_copy(rows_ref, rows, rows_sem)
     fetch.start()
-    for kind in range(kinds):
-        for n in range(CHUNKS[kind]):
-            for copy in copies(kind, n):
-                copy.start()
+    for at in range(AHEAD):
+        start(at)
     fetch.wait()
     sums = []
     for kind in (0, 1):

time: 171 us -> 162 us (0.947)
  waiting for transfers between devices: 49.8 us -> 40.2 us
  blocking collectives: 17.8 us -> 26.5 us
  starting transfers between devices: 67.9 us -> 60.8 us
    all_to_all x4 -> x3, waiting for transfers between devices: 25.9 us -> 16.4 us  [exchange(): return lax.all_to_all(tiles, axes, split_axis=0, concat_axis=0, tiled=True)]
    all_to_all x1 -> x2, blocking collectives: 17.8 us -> 26.5 us  [exchange(): return lax.all_to_all(tiles, axes, split_axis=0, concat_axis=0, tiled=True)]
    all_to_all x4 -> x3, starting transfers between devices: 32.9 us -> 26.2 us  [exchange(): return lax.all_to_all(tiles, axes, split_axis=0, concat_axis=0, tiled=True)]
  transfers between devices with their start and end apart: 15 -> 14, of which waited for: 9 -> 8; matrix products, arithmetic and copies ran while one was open for 0% -> 0% of each run, Pallas kernels for 5% -> 5%
where the time goes in v7:
time: 162 us; the launch traced here: 161 us
  starting transfers between devices  60.8 us (38%)
  waiting for transfers between devices  40.2 us (25%)
  blocking collectives  26.5 us (16%)
  Pallas kernels  15.2 us (9%)
  between operations  13.6 us (8%)
  other arithmetic  2.66 us (2%)
  local copies, waits for them, and re-layouts  1.77 us (1%)
    ppermute x8, starting transfers between devices, shifted(): lax.ppermute(value, axis, [(i, (i + by) % length) for i in range(length)])  26.7 us
    all_to_all x2, blocking collectives, exchange(): return lax.all_to_all(tiles, axes, split_axis=0, concat_axis=0, tiled=True)  26.5 us
    all_to_all x3, starting transfers between devices, exchange(): return lax.all_to_all(tiles, axes, split_axis=0, concat_axis=0, tiled=True)  26.2 us
    ppermute x8, waiting for transfers between devices, shifted(): lax.ppermute(value, axis, [(i, (i + by) % length) for i in range(length)])  19.3 us
    all_to_all x3, waiting for transfers between devices, exchange(): return lax.all_to_all(tiles, axes, split_axis=0, concat_axis=0, tiled=True)  16.4 us
    ppermute x2, starting transfers between devices, moved(): return lax.ppermute(value, axes, pairs)  7.94 us
    pallas_call x1, Pallas kernels, feed_forward(): pl.pallas_call(ffn_kernel, out_shape=jax.ShapeDtypeStruct((count, width),...  6.41 us
    ppermute x2, waiting for transfers between devices, moved(): return lax.ppermute(value, axes, pairs)  4.53 us
  transfers between devices with their start and end apart: 14, of which 8 were waited for; matrix products, arithmetic and copies ran while one was open for 0% of the time, Pallas kernels for 5%

profile of v7, /device:TPU:1, one launch (start us, length us, event | category | flops | bytes accessed | tf_op | source)
XLA Modules:
  0.0 160.7 jit_solution(11866464057771639423)
XLA Ops:
  6.5 0.9 pad_maximum_fusion.2
  7.5 6.0 %collective-permute-start.8 = (bf16[96,704]{1,0:T(8,128)(2,1)S(1)}, bf16[96,704]{1,0:T(8,128)(2,1)S(1)}, u32[]{:S(2)}, u32[]{:S(2)}) collective-permute-start(bf16[96,704]{1,0:T(8,128)(2,1)S(1)} %pad_maximum_fusion.2), channel_id=1, source_target_pairs={{0,16},{1,24},{8,17},{9,25},{16,0},{17,8},{24,1},{25,9},{2,18},{3,... | collective-permute-start | bytes 405512 | tf_op jit(solution)/shard_map/ppermute | solution.py:316
  13.5 1.9 %collective-permute-start.9 = (bf16[96,704]{1,0:T(8,128)(2,1)S(1)}, bf16[96,704]{1,0:T(8,128)(2,1)S(1)}, u32[]{:S(2)}, u32[]{:S(2)}) collective-permute-start(bf16[96,704]{1,0:T(8,128)(2,1)S(1)} %pad_maximum_fusion.2), channel_id=1, source_target_pairs={{0,0},{1,8},{8,1},{9,9},{16,16},{17,24},{24,17},{25,25},{2,2},{3,1... | collective-permute-start | bytes 405512 | tf_op jit(solution)/shard_map/ppermute | solution.py:316
  15.4 1.4 collective-permute-done.8
  16.9 3.1 %collective-permute-done.9 = bf16[96,704]{1,0:T(8,128)(2,1)S(1)} collective-permute-done((bf16[96,704]{1,0:T(8,128)(2,1)S(1)}, bf16[96,704]{1,0:T(8,128)(2,1)S(1)}, u32[]{:S(2)}, u32[]{:S(2)}) %collective-permute-start.9) | collective-permute-done | bytes 135200 | tf_op jit(solution)/shard_map/ppermute | solution.py:316
  20.0 0.7 pad_maximum_fusion.1
  20.8 3.1 %collective-permute-start = (bf16[128,2048]{1,0:T(8,128)(2,1)}, bf16[128,2048]{1,0:T(8,128)(2,1)S(1)}, u32[]{:S(2)}, u32[]{:S(2)}) collective-permute-start(bf16[128,2048]{1,0:T(8,128)(2,1)} %param.19), channel_id=1, source_target_pairs={{0,2},{2,4},{4,6},{6,0},{1,3},{3,5},{5,7},{7,1},{8,10},{10,12},{12... | collective-permute-start | bytes 1572872 | tf_op jit(solution)/shard_map/ppermute | solution.py:321
  23.9 4.4 %collective-permute-start.1 = (bf16[128,2048]{1,0:T(8,128)(2,1)}, bf16[128,2048]{1,0:T(8,128)(2,1)S(1)}, u32[]{:S(2)}, u32[]{:S(2)}) collective-permute-start(bf16[128,2048]{1,0:T(8,128)(2,1)} %param.19), channel_id=1, source_target_pairs={{0,4},{2,6},{4,0},{6,2},{1,5},{3,7},{5,1},{7,3},{8,12},{10,14},{12... | collective-permute-start | bytes 1572872 | tf_op jit(solution)/shard_map/ppermute | solution.py:321
  28.3 3.1 %collective-permute-start.2 = (bf16[128,2048]{1,0:T(8,128)(2,1)}, bf16[128,2048]{1,0:T(8,128)(2,1)S(1)}, u32[]{:S(2)}, u32[]{:S(2)}) collective-permute-start(bf16[128,2048]{1,0:T(8,128)(2,1)} %param.19), channel_id=1, source_target_pairs={{0,6},{2,0},{4,2},{6,4},{1,7},{3,1},{5,3},{7,5},{8,14},{10,8},{12,... | collective-permute-start | bytes 1572872 | tf_op jit(solution)/shard_map/ppermute | solution.py:321
  31.4 3.3 %collective-permute-done = bf16[128,2048]{1,0:T(8,128)(2,1)S(1)} collective-permute-done((bf16[128,2048]{1,0:T(8,128)(2,1)}, bf16[128,2048]{1,0:T(8,128)(2,1)S(1)}, u32[]{:S(2)}, u32[]{:S(2)}) %collective-permute-start) | collective-permute-done | bytes 524320 | tf_op jit(solution)/shard_map/ppermute | solution.py:321
  34.7 13.5 %collective-permute-done.1 = bf16[128,2048]{1,0:T(8,128)(2,1)S(1)} collective-permute-done((bf16[128,2048]{1,0:T(8,128)(2,1)}, bf16[128,2048]{1,0:T(8,128)(2,1)S(1)}, u32[]{:S(2)}, u32[]{:S(2)}) %collective-permute-start.1) | collective-permute-done | bytes 524320 | tf_op jit(solution)/shard_map/ppermute | solution.py:321
  48.2 2.5 %collective-permute-done.2 = bf16[128,2048]{1,0:T(8,128)(2,1)S(1)} collective-permute-done((bf16[128,2048]{1,0:T(8,128)(2,1)}, bf16[128,2048]{1,0:T(8,128)(2,1)S(1)}, u32[]{:S(2)}, u32[]{:S(2)}) %collective-permute-start.2) | collective-permute-done | bytes 524320 | tf_op jit(solution)/shard_map/ppermute | solution.py:321
  50.8 3.4 %collective-permute-start.3 = (bf16[512,2048]{1,0:T(8,128)(2,1)S(1)}, bf16[512,2048]{1,0:T(8,128)(2,1)}, u32[]{:S(2)}, u32[]{:S(2)}) collective-permute-start(bf16[512,2048]{1,0:T(8,128)(2,1)S(1)} %constant_dynamic-update-slice_fusion.near_w_ref), channel_id=1, source_target_pairs={{0,1},{1,0},{2,3},{3,2},{4,5},{5,4},{6,7},{7,6},{8,9},{9,8},{10,11... | collective-permute-start | bytes 6291464 | tf_op jit(solution)/shard_map/ppermute | solution.py:321
  54.2 1.9 %retention.1 = (f32[256,128]{1,0:T(8,128)}, bf16[256,128]{1,0:T(8,128)(2,1)}, f32[8,24,128]{2,1,0:T(8,128)}) custom-call(bf16[256,128]{1,0:T(8,128)(2,1)} %q_ref.1, bf16[256,128]{1,0:T(8,128)(2,1)} %k_ref.1, bf16[256,128]{1,0:T(8,128)(2,1)} %v_ref.1, f32[1,256]{1,0:T(1,128)} %bitcast.30), custom_call_target="tpu_custom_call" | custom-call | flops 50331648 | bytes 1048576 | tf_op jit(solution)/shard_map/retention/pallas_call | solution.py:68
  56.1 8.6 %all_to_all.25.states_ref = f32[8,24,128]{2,1,0:T(8,128)S(1)} all-to-all(f32[8,24,128]{2,1,0:T(8,128)} %get-tuple-element.12), channel_id=1, replica_groups=mesh['zh'=8,'zl'=2,'y1'=2,'y0'=2,'x'=4,'c'=2] {'zl','y1','y0'}, dimensions={0} | all-to-all | bytes 196608 | tf_op jit(solution)/shard_map/all_to_all | solution.py:325
  65.4 14.3 %all-to-all-start.1 = ((f32[8,24,128]{2,1,0:T(8,128)}), f32[8,24,128]{2,1,0:T(8,128)S(1)}, u32[]{:S(2)}, u32[]{:S(2)}) async-start(f32[8,24,128]{2,1,0:T(8,128)} %joined_state.1), calls=%async_computation.1 | async-start | bytes 196608 | tf_op jit(solution)/shard_map/all_to_all | solution.py:325
  79.7 4.3 %collective-permute-start.6 = (bf16[32,2048]{1,0:T(8,128)(2,1)S(1)}, bf16[32,2048]{1,0:T(8,128)(2,1)S(1)}, u32[]{:S(2)}, u32[]{:S(2)}) collective-permute-start(bf16[32,2048]{1,0:T(8,128)(2,1)S(1)} %copy-done.3), channel_id=1, source_target_pairs={{0,6},{2,0},{4,2},{6,4},{1,7},{3,1},{5,3},{7,5},{8,14},{10,8},{12,... | collective-permute-start | bytes 393224 | tf_op jit(solution)/shard_map/ppermute | solution.py:321
  84.0 3.3 %collective-permute-start.5 = (bf16[32,2048]{1,0:T(8,128)(2,1)S(1)}, bf16[32,2048]{1,0:T(8,128)(2,1)S(1)}, u32[]{:S(2)}, u32[]{:S(2)}) collective-permute-start(bf16[32,2048]{1,0:T(8,128)(2,1)S(1)} %copy-done.3), channel_id=1, source_target_pairs={{0,4},{2,6},{4,0},{6,2},{1,5},{3,7},{5,1},{7,3},{8,12},{10,14},{12... | collective-permute-start | bytes 393224 | tf_op jit(solution)/shard_map/ppermute | solution.py:321
  87.3 1.9 %collective-permute-start.4 = (bf16[32,2048]{1,0:T(8,128)(2,1)S(1)}, bf16[32,2048]{1,0:T(8,128)(2,1)S(1)}, u32[]{:S(2)}, u32[]{:S(2)}) collective-permute-start(bf16[32,2048]{1,0:T(8,128)(2,1)S(1)} %copy-done.3), channel_id=1, source_target_pairs={{0,2},{2,4},{4,6},{6,0},{1,3},{3,5},{5,7},{7,1},{8,10},{10,12},{12... | collective-permute-start | bytes 393224 | tf_op jit(solution)/shard_map/ppermute | solution.py:321
  89.2 5.2 %all-to-all-done.1.joined_ref = f32[8,24,128]{2,1,0:T(8,128)S(1)} async-done(((f32[8,24,128]{2,1,0:T(8,128)}), f32[8,24,128]{2,1,0:T(8,128)S(1)}, u32[]{:S(2)}, u32[]{:S(2)}) %all-to-all-start.1) | async-done | bytes 98336 | tf_op jit(solution)/shard_map/all_to_all | solution.py:325
  94.4 0.7 incoming_state.1
  95.1 3.4 %all-to-all-start.2 = ((f32[8,16,128]{2,1,0:T(8,128)}), f32[8,16,128]{2,1,0:T(8,128)S(1)}, u32[]{:S(2)}, u32[]{:S(2)}) async-start(f32[8,16,128]{2,1,0:T(8,128)} %incoming_state.1), calls=%async_computation.2 | async-start | bytes 131072 | tf_op jit(solution)/shard_map/all_to_all | solution.py:325
  98.6 3.3 %collective-permute-start.7 = (bf16[4,32,2048]{2,1,0:T(8,128)(2,1)S(1)}, bf16[4,32,2048]{2,1,0:T(8,128)(2,1)}, u32[]{:S(2)}, u32[]{:S(2)}) collective-permute-start(bf16[4,32,2048]{2,1,0:T(8,128)(2,1)S(1)} %pad_maximum_fusion.near_s_ref), channel_id=1, source_target_pairs={{0,8},{8,0},{1,9},{9,1},{2,10},{10,2},{3,11},{11,3},{4,12},{12,4},... | collective-permute-start | bytes 1572872 | tf_op jit(solution)/shard_map/ppermute | solution.py:321
  101.9 1.8 %all-to-all-done.2 = f32[8,16,128]{2,1,0:T(8,128)S(1)} async-done(((f32[8,16,128]{2,1,0:T(8,128)}), f32[8,16,128]{2,1,0:T(8,128)S(1)}, u32[]{:S(2)}, u32[]{:S(2)}) %all-to-all-start.2) | async-done | bytes 65568 | tf_op jit(solution)/shard_map/all_to_all | solution.py:325
  104.3 2.1 %mix.1 = bf16[8,2,4,32,128]{4,3,2,1,0:T(8,128)(2,1)} custom-call(f32[256,128]{1,0:T(8,128)} %get-tuple-element.10.within_ref, bf16[256,128]{1,0:T(8,128)(2,1)} %get-tuple-element.11.carry_q_ref, f32[128,128]{1,0:T(8,128)} %bitcast.24, bf16[256,128]{1,0:T(8,128)(2,1)} %gate_ref.1, bf16[1,128]{1,0:T(2,128)(2,1)} %bitcast.31), custom_call_target="tpu_custom_call" | custom-call | flops 8388608 | bytes 1048576 | tf_op jit(solution)/shard_map/mix/pallas_call | solution.py:152
  106.4 8.5 %all-to-all-start.3 = ((bf16[16,4,32,128]{3,2,1,0:T(8,128)(2,1)}), bf16[16,4,32,128]{3,2,1,0:T(8,128)(2,1)S(1)}, u32[]{:S(2)}, u32[]{:S(2)}) async-start(bf16[16,4,32,128]{3,2,1,0:T(8,128)(2,1)} %bitcast.23), calls=%async_computation.3 | async-start | bytes 1048576 | tf_op jit(solution)/shard_map/all_to_all | solution.py:325
  115.0 9.4 %all-to-all-done.3 = bf16[16,4,32,128]{3,2,1,0:T(8,128)(2,1)S(1)} async-done(((bf16[16,4,32,128]{3,2,1,0:T(8,128)(2,1)}), bf16[16,4,32,128]{3,2,1,0:T(8,128)(2,1)S(1)}, u32[]{:S(2)}, u32[]{:S(2)}) %all-to-all-start.3) | async-done | bytes 524320 | tf_op jit(solution)/shard_map/all_to_all | solution.py:325
  124.4 3.4 %group_rows.1 = (bf16[256,2048]{1,0:T(8,128)(2,1)S(1)}, f32[32,2048]{1,0:T(8,128)S(1)}) custom-call(s32[3]{0:T(128)S(1)} %pad_add_fusion.here_ref, bf16[2,8,4,32,128]{4,3,2,1,0:T(8,128)(2,1)S(1)} %bitcast.21, bf16[512,2048]{1,0:T(8,128)(2,1)S(1)} %constant_dynamic-update-slice_fusion.near_w_ref, bf16[512,2048]{1,0:T(8,128)(2,1)} %collective-permute-done.3.far_w_ref, ...), custom_call_target="tpu_custom_call" | custom-call | flops 1073741824 | bytes 8388608 | tf_op jit(solution)/shard_map/group_rows/pallas_call | solution.py:214
  127.8 1.0 copy-done
  128.7 6.4 %feed_forward.1 = bf16[256,2048]{1,0:T(8,128)(2,1)S(1)} custom-call(bf16[256,2048]{1,0:T(8,128)(2,1)} %copy-done, bf16[16,2,2,3,32,704]{5,4,3,2,1,0:T(8,128)(2,1)} %bitcast.22), custom_call_target="tpu_custom_call" | custom-call | flops 2214592512 | bytes 8388608 | tf_op jit(solution)/shard_map/feed_forward/pallas_call | solution.py:291
  135.2 17.8 %all_to_all.26 = bf16[8,32,2048]{2,1,0:T(8,128)(2,1)S(1)} all-to-all(bf16[8,32,2048]{2,1,0:T(8,128)(2,1)S(1)} %bitcast.20), channel_id=1, replica_groups=mesh['zh'=8,'zl'=2,'y1'=2,'y0'=2,'x'=4,'c'=2] {'y0','x'}, dimensions={0} | all-to-all | bytes 2097152 | tf_op jit(solution)/shard_map/all_to_all | solution.py:325
  153.1 0.7 add_convert_fusion
  (27 shorter events, 1.8 us)
Async XLA Ops:
  6.5 24.8 %copy-start.1 = (bf16[128,2048]{1,0:T(8,128)(2,1)S(1)}, bf16[128,2048]{1,0:T(8,128)(2,1)}, u32[]{:S(2)}) copy-start(bf16[128,2048]{1,0:T(8,128)(2,1)} %param.19) | copy-start | bytes 1572868
  6.5 122.2 %all-gather.3.cloned.1.call-start = ((), (), s32[]{:S(2)}) async-start(), calls=%async_computation.5 | async-start | bytes 9732096 | tf_op jit(solution)/shard_map/all_gather | solution.py:336
  7.5 9.4 %collective-permute-start.8 = (bf16[96,704]{1,0:T(8,128)(2,1)S(1)}, bf16[96,704]{1,0:T(8,128)(2,1)S(1)}, u32[]{:S(2)}, u32[]{:S(2)}) collective-permute-start(bf16[96,704]{1,0:T(8,128)(2,1)S(1)} %pad_maximum_fusion.2), channel_id=1, source_target_pairs={{0,16},{1,24},{8,17},{9,25},{16,0},{17,8},{24,1},{25,9},{2,18},{3,... | collective-permute-start | bytes 405512 | tf_op jit(solution)/shard_map/ppermute | solution.py:316
  13.5 6.5 %collective-permute-start.9 = (bf16[96,704]{1,0:T(8,128)(2,1)S(1)}, bf16[96,704]{1,0:T(8,128)(2,1)S(1)}, u32[]{:S(2)}, u32[]{:S(2)}) collective-permute-start(bf16[96,704]{1,0:T(8,128)(2,1)S(1)} %pad_maximum_fusion.2), channel_id=1, source_target_pairs={{0,0},{1,8},{8,1},{9,9},{16,16},{17,24},{24,17},{25,25},{2,2},{3,1... | collective-permute-start | bytes 405512 | tf_op jit(solution)/shard_map/ppermute | solution.py:316
  20.8 13.9 %collective-permute-start = (bf16[128,2048]{1,0:T(8,128)(2,1)}, bf16[128,2048]{1,0:T(8,128)(2,1)S(1)}, u32[]{:S(2)}, u32[]{:S(2)}) collective-permute-start(bf16[128,2048]{1,0:T(8,128)(2,1)} %param.19), channel_id=1, source_target_pairs={{0,2},{2,4},{4,6},{6,0},{1,3},{3,5},{5,7},{7,1},{8,10},{10,12},{12... | collective-permute-start | bytes 1572872 | tf_op jit(solution)/shard_map/ppermute | solution.py:321
  23.9 24.3 %collective-permute-start.1 = (bf16[128,2048]{1,0:T(8,128)(2,1)}, bf16[128,2048]{1,0:T(8,128)(2,1)S(1)}, u32[]{:S(2)}, u32[]{:S(2)}) collective-permute-start(bf16[128,2048]{1,0:T(8,128)(2,1)} %param.19), channel_id=1, source_target_pairs={{0,4},{2,6},{4,0},{6,2},{1,5},{3,7},{5,1},{7,3},{8,12},{10,14},{12... | collective-permute-start | bytes 1572872 | tf_op jit(solution)/shard_map/ppermute | solution.py:321
  28.3 22.5 %collective-permute-start.2 = (bf16[128,2048]{1,0:T(8,128)(2,1)}, bf16[128,2048]{1,0:T(8,128)(2,1)S(1)}, u32[]{:S(2)}, u32[]{:S(2)}) collective-permute-start(bf16[128,2048]{1,0:T(8,128)(2,1)} %param.19), channel_id=1, source_target_pairs={{0,6},{2,0},{4,2},{6,4},{1,7},{3,1},{5,3},{7,5},{8,14},{10,8},{12,... | collective-permute-start | bytes 1572872 | tf_op jit(solution)/shard_map/ppermute | solution.py:321
  31.4 48.3 %copy-start.3 = (bf16[32,2048]{1,0:T(8,128)(2,1)S(1)}, bf16[32,2048]{1,0:T(8,128)(2,1)}, u32[]{:S(2)}) copy-start(bf16[32,2048]{1,0:T(8,128)(2,1)} %param.12) | copy-start | bytes 393220
  50.8 64.1 %copy-start.4 = (bf16[2048]{0:T(1024)(128)(2,1)S(1)}, bf16[2048]{0:T(1024)(128)(2,1)}, u32[]{:S(2)}) copy-start(bf16[2048]{0:T(1024)(128)(2,1)} %param.20) | copy-start | bytes 12292
  50.8 73.6 %collective-permute-start.3 = (bf16[512,2048]{1,0:T(8,128)(2,1)S(1)}, bf16[512,2048]{1,0:T(8,128)(2,1)}, u32[]{:S(2)}, u32[]{:S(2)}) collective-permute-start(bf16[512,2048]{1,0:T(8,128)(2,1)S(1)} %constant_dynamic-update-slice_fusion.near_w_ref), channel_id=1, source_target_pairs={{0,1},{1,0},{2,3},{3,2},{4,5},{5,4},{6,7},{7,6},{8,9},{9,8},{10,11... | collective-permute-start | bytes 6291464 | tf_op jit(solution)/shard_map/ppermute | solution.py:321
  65.4 29.1 %all-to-all-start.1 = ((f32[8,24,128]{2,1,0:T(8,128)}), f32[8,24,128]{2,1,0:T(8,128)S(1)}, u32[]{:S(2)}, u32[]{:S(2)}) async-start(f32[8,24,128]{2,1,0:T(8,128)} %joined_state.1), calls=%async_computation.1 | async-start | bytes 196608 | tf_op jit(solution)/shard_map/all_to_all | solution.py:325
  79.7 18.8 %collective-permute-start.6 = (bf16[32,2048]{1,0:T(8,128)(2,1)S(1)}, bf16[32,2048]{1,0:T(8,128)(2,1)S(1)}, u32[]{:S(2)}, u32[]{:S(2)}) collective-permute-start(bf16[32,2048]{1,0:T(8,128)(2,1)S(1)} %copy-done.3), channel_id=1, source_target_pairs={{0,6},{2,0},{4,2},{6,4},{1,7},{3,1},{5,3},{7,5},{8,14},{10,8},{12,... | collective-permute-start | bytes 393224 | tf_op jit(solution)/shard_map/ppermute | solution.py:321
  84.0 14.5 %collective-permute-start.5 = (bf16[32,2048]{1,0:T(8,128)(2,1)S(1)}, bf16[32,2048]{1,0:T(8,128)(2,1)S(1)}, u32[]{:S(2)}, u32[]{:S(2)}) collective-permute-start(bf16[32,2048]{1,0:T(8,128)(2,1)S(1)} %copy-done.3), channel_id=1, source_target_pairs={{0,4},{2,6},{4,0},{6,2},{1,5},{3,7},{5,1},{7,3},{8,12},{10,14},{12... | collective-permute-start | bytes 393224 | tf_op jit(solution)/shard_map/ppermute | solution.py:321
  87.3 11.2 %collective-permute-start.4 = (bf16[32,2048]{1,0:T(8,128)(2,1)S(1)}, bf16[32,2048]{1,0:T(8,128)(2,1)S(1)}, u32[]{:S(2)}, u32[]{:S(2)}) collective-permute-start(bf16[32,2048]{1,0:T(8,128)(2,1)S(1)} %copy-done.3), channel_id=1, source_target_pairs={{0,2},{2,4},{4,6},{6,0},{1,3},{3,5},{5,7},{7,1},{8,10},{10,12},{12... | collective-permute-start | bytes 393224 | tf_op jit(solution)/shard_map/ppermute | solution.py:321
  95.1 8.5 %all-to-all-start.2 = ((f32[8,16,128]{2,1,0:T(8,128)}), f32[8,16,128]{2,1,0:T(8,128)S(1)}, u32[]{:S(2)}, u32[]{:S(2)}) async-start(f32[8,16,128]{2,1,0:T(8,128)} %incoming_state.1), calls=%async_computation.2 | async-start | bytes 131072 | tf_op jit(solution)/shard_map/all_to_all | solution.py:325
  98.6 16.4 %collective-permute-start.7 = (bf16[4,32,2048]{2,1,0:T(8,128)(2,1)S(1)}, bf16[4,32,2048]{2,1,0:T(8,128)(2,1)}, u32[]{:S(2)}, u32[]{:S(2)}) collective-permute-start(bf16[4,32,2048]{2,1,0:T(8,128)(2,1)S(1)} %pad_maximum_fusion.near_s_ref), channel_id=1, source_target_pairs={{0,8},{8,0},{1,9},{9,1},{2,10},{10,2},{3,11},{11,3},{4,12},{12,4},... | collective-permute-start | bytes 1572872 | tf_op jit(solution)/shard_map/ppermute | solution.py:321
  103.6 0.6 copy-start.2
  106.4 18.0 %all-to-all-start.3 = ((bf16[16,4,32,128]{3,2,1,0:T(8,128)(2,1)}), bf16[16,4,32,128]{3,2,1,0:T(8,128)(2,1)S(1)}, u32[]{:S(2)}, u32[]{:S(2)}) async-start(bf16[16,4,32,128]{3,2,1,0:T(8,128)(2,1)} %bitcast.23), calls=%async_computation.3 | async-start | bytes 1048576 | tf_op jit(solution)/shard_map/all_to_all | solution.py:325
  127.7 1.0 copy-start
Sparse Core Ops, SparseCore 0:
  20.9 85.6 all-gather.2

commit v8 on v7

--- a/solution.py
+++ b/solution.py
@@ -87,16 +87,20 @@
         own = states_ref[n, part:, :]
         state = jnp.exp(own[:1]) * state + states_ref[n, :part, :]
         total = total + own
+    high = total.astype(BF16).astype(F32)
+    mid = (total - high).astype(BF16).astype(F32)
+    line = lax.broadcasted_iota(jnp.int32, total.shape, 0)
+    terms = jnp.where(line == 0, high, jnp.where(line == 1, mid, total - high - mid))
+    packed = jnp.concatenate([state, terms], axis=0).astype(BF16)
     for n in range(out_ref.shape[0]):
-        out_ref[n, :part, :] = state
-        out_ref[n, part:, :] = total
+        out_ref[n] = packed
 
 
 def joined_state(states):
     _, lines, width = states.shape
     return pl.pallas_call(
         joined_kernel,
-        out_shape=jax.ShapeDtypeStruct((SIZES["zh"], lines, width), F32),
+        out_shape=jax.ShapeDtypeStruct((SIZES["zh"], lines, width), BF16),
         in_specs=vmem(1),
         out_specs=pl.BlockSpec(memory_space=pltpu.VMEM),
         cost_estimate=kernel_cost(2**18, 2**18, 2**10),
@@ -110,7 +114,9 @@
     here = here_ref[0]
     carried = jnp.zeros(out_ref.shape[1:], F32)
     for n in range(joined_ref.shape[0]):
-        after = jnp.exp(joined_ref[n, part : part + 1, :]) * carried + joined_ref[n, :part, :]
+        other = joined_ref[n].astype(F32)
+        total = other[part : part + 1] + other[part + 1 : part + 2] + other[part + 2 : part + 3]
+        after = jnp.exp(total) * carried + other[:part]
         carried = jnp.where(n < here, after, carried)
     for n in range(out_ref.shape[0]):
         out_ref[n] = carried
@@ -354,13 +360,12 @@
     weights = gathered_weights(gate_weight, up_weight, down_weight)
     rows, width = queries.shape[0], stream.shape[1]
     head_dim = queries.shape[1]
-    sides = [shifted(out_weight, "x", 1), shifted(out_weight, "x", 3)]
-    across = shifted(out_weight, "x", 2)
+    found = [out_weight] + [shifted(out_weight, "x", r) for r in (1, 2, 3)]
     others = [shifted(stream, "x", r) for r in (1, 2, 3)]
-    near_w = jnp.concatenate([out_weight, sides[0], across, sides[1]], axis=0)
     near_s = jnp.stack([stream, *others])
+    far_s = shifted(near_s, "y0", 1)
+    near_w = jnp.concatenate(found, axis=0)
     far_w = shifted(near_w, "c", 1)
-    far_s = shifted(near_s, "y0", 1)
     within, carry_q, state = retention(
         queries, keys_in, values_in, log_decay.reshape(1, rows)
     )

time: 162 us -> 160 us (0.988)
  waiting for transfers between devices: 40.2 us -> 37.9 us
    all_to_all x3, waiting for transfers between devices: 16.4 us -> 14.1 us  [exchange(): return lax.all_to_all(tiles, axes, split_axis=0, concat_axis=0, tiled=True)]
  transfers between devices with their start and end apart: 14 -> 14, of which waited for: 8 -> 8; matrix products, arithmetic and copies ran while one was open for 0% -> 0% of each run, Pallas kernels for 5% -> 6%
where the time goes in v8:
time: 160 us; the launch traced here: 159 us
  starting transfers between devices  61.1 us (38%)
  waiting for transfers between devices  37.9 us (24%)
  blocking collectives  26.5 us (17%)
  Pallas kernels  15.2 us (10%)
  between operations  13.6 us (8%)
  other arithmetic  2.66 us (2%)
  local copies, waits for them, and re-layouts  1.77 us (1%)
    ppermute x8, starting transfers between devices, shifted(): lax.ppermute(value, axis, [(i, (i + by) % length) for i in range(length)])  26.7 us
    all_to_all x3, starting transfers between devices, exchange(): return lax.all_to_all(tiles, axes, split_axis=0, concat_axis=0, tiled=True)  26.5 us
    all_to_all x2, blocking collectives, exchange(): return lax.all_to_all(tiles, axes, split_axis=0, concat_axis=0, tiled=True)  26.5 us
    ppermute x8, waiting for transfers between devices, shifted(): lax.ppermute(value, axis, [(i, (i + by) % length) for i in range(length)])  19.3 us
    all_to_all x3, waiting for transfers between devices, exchange(): return lax.all_to_all(tiles, axes, split_axis=0, concat_axis=0, tiled=True)  14.1 us
    ppermute x2, starting transfers between devices, moved(): return lax.ppermute(value, axes, pairs)  7.94 us
    pallas_call x1, Pallas kernels, feed_forward(): pl.pallas_call(ffn_kernel, out_shape=jax.ShapeDtypeStruct((count, width),...  6.41 us
    ppermute x2, waiting for transfers between devices, moved(): return lax.ppermute(value, axes, pairs)  4.53 us
  transfers between devices with their start and end apart: 14, of which 8 were waited for; matrix products, arithmetic and copies ran while one was open for 0% of the time, Pallas kernels for 6%

profile of v8, /device:TPU:1, one launch (start us, length us, event | category | flops | bytes accessed | tf_op | source)
XLA Modules:
  0.0 158.7 jit_solution(3629355365253736415)
XLA Ops:
  6.5 0.9 pad_maximum_fusion.2
  7.5 6.0 %collective-permute-start.8 = (bf16[96,704]{1,0:T(8,128)(2,1)S(1)}, bf16[96,704]{1,0:T(8,128)(2,1)S(1)}, u32[]{:S(2)}, u32[]{:S(2)}) collective-permute-start(bf16[96,704]{1,0:T(8,128)(2,1)S(1)} %pad_maximum_fusion.2), channel_id=1, source_target_pairs={{0,16},{1,24},{8,17},{9,25},{16,0},{17,8},{24,1},{25,9},{2,18},{3,... | collective-permute-start | bytes 405512 | tf_op jit(solution)/shard_map/ppermute | solution.py:322
  13.5 1.9 %collective-permute-start.9 = (bf16[96,704]{1,0:T(8,128)(2,1)S(1)}, bf16[96,704]{1,0:T(8,128)(2,1)S(1)}, u32[]{:S(2)}, u32[]{:S(2)}) collective-permute-start(bf16[96,704]{1,0:T(8,128)(2,1)S(1)} %pad_maximum_fusion.2), channel_id=1, source_target_pairs={{0,0},{1,8},{8,1},{9,9},{16,16},{17,24},{24,17},{25,25},{2,2},{3,1... | collective-permute-start | bytes 405512 | tf_op jit(solution)/shard_map/ppermute | solution.py:322
  15.4 1.4 collective-permute-done.8
  16.9 3.1 %collective-permute-done.9 = bf16[96,704]{1,0:T(8,128)(2,1)S(1)} collective-permute-done((bf16[96,704]{1,0:T(8,128)(2,1)S(1)}, bf16[96,704]{1,0:T(8,128)(2,1)S(1)}, u32[]{:S(2)}, u32[]{:S(2)}) %collective-permute-start.9) | collective-permute-done | bytes 135200 | tf_op jit(solution)/shard_map/ppermute | solution.py:322
  20.0 0.7 pad_maximum_fusion.1
  20.8 3.1 %collective-permute-start = (bf16[128,2048]{1,0:T(8,128)(2,1)}, bf16[128,2048]{1,0:T(8,128)(2,1)S(1)}, u32[]{:S(2)}, u32[]{:S(2)}) collective-permute-start(bf16[128,2048]{1,0:T(8,128)(2,1)} %param.19), channel_id=1, source_target_pairs={{0,2},{2,4},{4,6},{6,0},{1,3},{3,5},{5,7},{7,1},{8,10},{10,12},{12... | collective-permute-start | bytes 1572872 | tf_op jit(solution)/shard_map/ppermute | solution.py:327
  23.9 4.4 %collective-permute-start.1 = (bf16[128,2048]{1,0:T(8,128)(2,1)}, bf16[128,2048]{1,0:T(8,128)(2,1)S(1)}, u32[]{:S(2)}, u32[]{:S(2)}) collective-permute-start(bf16[128,2048]{1,0:T(8,128)(2,1)} %param.19), channel_id=1, source_target_pairs={{0,4},{2,6},{4,0},{6,2},{1,5},{3,7},{5,1},{7,3},{8,12},{10,14},{12... | collective-permute-start | bytes 1572872 | tf_op jit(solution)/shard_map/ppermute | solution.py:327
  28.3 3.1 %collective-permute-start.2 = (bf16[128,2048]{1,0:T(8,128)(2,1)}, bf16[128,2048]{1,0:T(8,128)(2,1)S(1)}, u32[]{:S(2)}, u32[]{:S(2)}) collective-permute-start(bf16[128,2048]{1,0:T(8,128)(2,1)} %param.19), channel_id=1, source_target_pairs={{0,6},{2,0},{4,2},{6,4},{1,7},{3,1},{5,3},{7,5},{8,14},{10,8},{12,... | collective-permute-start | bytes 1572872 | tf_op jit(solution)/shard_map/ppermute | solution.py:327
  31.4 3.3 %collective-permute-done = bf16[128,2048]{1,0:T(8,128)(2,1)S(1)} collective-permute-done((bf16[128,2048]{1,0:T(8,128)(2,1)}, bf16[128,2048]{1,0:T(8,128)(2,1)S(1)}, u32[]{:S(2)}, u32[]{:S(2)}) %collective-permute-start) | collective-permute-done | bytes 524320 | tf_op jit(solution)/shard_map/ppermute | solution.py:327
  34.7 13.5 %collective-permute-done.1 = bf16[128,2048]{1,0:T(8,128)(2,1)S(1)} collective-permute-done((bf16[128,2048]{1,0:T(8,128)(2,1)}, bf16[128,2048]{1,0:T(8,128)(2,1)S(1)}, u32[]{:S(2)}, u32[]{:S(2)}) %collective-permute-start.1) | collective-permute-done | bytes 524320 | tf_op jit(solution)/shard_map/ppermute | solution.py:327
  48.2 2.5 %collective-permute-done.2 = bf16[128,2048]{1,0:T(8,128)(2,1)S(1)} collective-permute-done((bf16[128,2048]{1,0:T(8,128)(2,1)}, bf16[128,2048]{1,0:T(8,128)(2,1)S(1)}, u32[]{:S(2)}, u32[]{:S(2)}) %collective-permute-start.2) | collective-permute-done | bytes 524320 | tf_op jit(solution)/shard_map/ppermute | solution.py:327
  50.8 3.4 %collective-permute-start.3 = (bf16[512,2048]{1,0:T(8,128)(2,1)S(1)}, bf16[512,2048]{1,0:T(8,128)(2,1)}, u32[]{:S(2)}, u32[]{:S(2)}) collective-permute-start(bf16[512,2048]{1,0:T(8,128)(2,1)S(1)} %constant_dynamic-update-slice_fusion.near_w_ref), channel_id=1, source_target_pairs={{0,1},{1,0},{2,3},{3,2},{4,5},{5,4},{6,7},{7,6},{8,9},{9,8},{10,11... | collective-permute-start | bytes 6291464 | tf_op jit(solution)/shard_map/ppermute | solution.py:327
  54.2 1.9 %retention.1 = (f32[256,128]{1,0:T(8,128)}, bf16[256,128]{1,0:T(8,128)(2,1)}, f32[8,24,128]{2,1,0:T(8,128)}) custom-call(bf16[256,128]{1,0:T(8,128)(2,1)} %q_ref.1, bf16[256,128]{1,0:T(8,128)(2,1)} %k_ref.1, bf16[256,128]{1,0:T(8,128)(2,1)} %v_ref.1, f32[1,256]{1,0:T(1,128)} %bitcast.30), custom_call_target="tpu_custom_call" | custom-call | flops 50331648 | bytes 1048576 | tf_op jit(solution)/shard_map/retention/pallas_call | solution.py:68
  56.1 8.6 %all_to_all.25.states_ref = f32[8,24,128]{2,1,0:T(8,128)S(1)} all-to-all(f32[8,24,128]{2,1,0:T(8,128)} %get-tuple-element.12), channel_id=1, replica_groups=mesh['zh'=8,'zl'=2,'y1'=2,'y0'=2,'x'=4,'c'=2] {'zl','y1','y0'}, dimensions={0} | all-to-all | bytes 196608 | tf_op jit(solution)/shard_map/all_to_all | solution.py:331
  65.3 14.3 %all-to-all-start.1 = ((bf16[8,24,128]{2,1,0:T(8,128)(2,1)}), bf16[8,24,128]{2,1,0:T(8,128)(2,1)S(1)}, u32[]{:S(2)}, u32[]{:S(2)}) async-start(bf16[8,24,128]{2,1,0:T(8,128)(2,1)} %joined_state.1), calls=%async_computation.1 | async-start | bytes 98304 | tf_op jit(solution)/shard_map/all_to_all | solution.py:331
  79.7 4.3 %collective-permute-start.6 = (bf16[32,2048]{1,0:T(8,128)(2,1)S(1)}, bf16[32,2048]{1,0:T(8,128)(2,1)S(1)}, u32[]{:S(2)}, u32[]{:S(2)}) collective-permute-start(bf16[32,2048]{1,0:T(8,128)(2,1)S(1)} %copy-done.3), channel_id=1, source_target_pairs={{0,6},{2,0},{4,2},{6,4},{1,7},{3,1},{5,3},{7,5},{8,14},{10,8},{12,... | collective-permute-start | bytes 393224 | tf_op jit(solution)/shard_map/ppermute | solution.py:327
  84.0 3.3 %collective-permute-start.5 = (bf16[32,2048]{1,0:T(8,128)(2,1)S(1)}, bf16[32,2048]{1,0:T(8,128)(2,1)S(1)}, u32[]{:S(2)}, u32[]{:S(2)}) collective-permute-start(bf16[32,2048]{1,0:T(8,128)(2,1)S(1)} %copy-done.3), channel_id=1, source_target_pairs={{0,4},{2,6},{4,0},{6,2},{1,5},{3,7},{5,1},{7,3},{8,12},{10,14},{12... | collective-permute-start | bytes 393224 | tf_op jit(solution)/shard_map/ppermute | solution.py:327
  87.3 1.9 %collective-permute-start.4 = (bf16[32,2048]{1,0:T(8,128)(2,1)S(1)}, bf16[32,2048]{1,0:T(8,128)(2,1)S(1)}, u32[]{:S(2)}, u32[]{:S(2)}) collective-permute-start(bf16[32,2048]{1,0:T(8,128)(2,1)S(1)} %copy-done.3), channel_id=1, source_target_pairs={{0,2},{2,4},{4,6},{6,0},{1,3},{3,5},{5,7},{7,1},{8,10},{10,12},{12... | collective-permute-start | bytes 393224 | tf_op jit(solution)/shard_map/ppermute | solution.py:327
  89.2 2.8 %all-to-all-done.1.joined_ref = bf16[8,24,128]{2,1,0:T(8,128)(2,1)S(1)} async-done(((bf16[8,24,128]{2,1,0:T(8,128)(2,1)}), bf16[8,24,128]{2,1,0:T(8,128)(2,1)S(1)}, u32[]{:S(2)}, u32[]{:S(2)}) %all-to-all-start.1) | async-done | bytes 49184 | tf_op jit(solution)/shard_map/all_to_all | solution.py:331
  92.1 0.7 incoming_state.1
  92.7 3.3 %all-to-all-start.2 = ((f32[8,16,128]{2,1,0:T(8,128)}), f32[8,16,128]{2,1,0:T(8,128)S(1)}, u32[]{:S(2)}, u32[]{:S(2)}) async-start(f32[8,16,128]{2,1,0:T(8,128)} %incoming_state.1), calls=%async_computation.2 | async-start | bytes 131072 | tf_op jit(solution)/shard_map/all_to_all | solution.py:331
  96.2 3.3 %collective-permute-start.7 = (bf16[4,32,2048]{2,1,0:T(8,128)(2,1)S(1)}, bf16[4,32,2048]{2,1,0:T(8,128)(2,1)}, u32[]{:S(2)}, u32[]{:S(2)}) collective-permute-start(bf16[4,32,2048]{2,1,0:T(8,128)(2,1)S(1)} %pad_maximum_fusion.near_s_ref), channel_id=1, source_target_pairs={{0,8},{8,0},{1,9},{9,1},{2,10},{10,2},{3,11},{11,3},{4,12},{12,4},... | collective-permute-start | bytes 1572872 | tf_op jit(solution)/shard_map/ppermute | solution.py:327
  99.5 1.8 %all-to-all-done.2 = f32[8,16,128]{2,1,0:T(8,128)S(1)} async-done(((f32[8,16,128]{2,1,0:T(8,128)}), f32[8,16,128]{2,1,0:T(8,128)S(1)}, u32[]{:S(2)}, u32[]{:S(2)}) %all-to-all-start.2) | async-done | bytes 65568 | tf_op jit(solution)/shard_map/all_to_all | solution.py:331
  101.9 2.1 %mix.1 = bf16[8,2,4,32,128]{4,3,2,1,0:T(8,128)(2,1)} custom-call(f32[256,128]{1,0:T(8,128)} %get-tuple-element.10.within_ref, bf16[256,128]{1,0:T(8,128)(2,1)} %get-tuple-element.11.carry_q_ref, f32[128,128]{1,0:T(8,128)} %bitcast.24, bf16[256,128]{1,0:T(8,128)(2,1)} %gate_ref.1, bf16[1,128]{1,0:T(2,128)(2,1)} %bitcast.31), custom_call_target="tpu_custom_call" | custom-call | flops 8388608 | bytes 1048576 | tf_op jit(solution)/shard_map/mix/pallas_call | solution.py:158
  104.1 8.8 %all-to-all-start.3 = ((bf16[16,4,32,128]{3,2,1,0:T(8,128)(2,1)}), bf16[16,4,32,128]{3,2,1,0:T(8,128)(2,1)S(1)}, u32[]{:S(2)}, u32[]{:S(2)}) async-start(bf16[16,4,32,128]{3,2,1,0:T(8,128)(2,1)} %bitcast.23), calls=%async_computation.3 | async-start | bytes 1048576 | tf_op jit(solution)/shard_map/all_to_all | solution.py:331
  113.0 9.4 %all-to-all-done.3 = bf16[16,4,32,128]{3,2,1,0:T(8,128)(2,1)S(1)} async-done(((bf16[16,4,32,128]{3,2,1,0:T(8,128)(2,1)}), bf16[16,4,32,128]{3,2,1,0:T(8,128)(2,1)S(1)}, u32[]{:S(2)}, u32[]{:S(2)}) %all-to-all-start.3) | async-done | bytes 524320 | tf_op jit(solution)/shard_map/all_to_all | solution.py:331
  122.4 3.4 %group_rows.1 = (bf16[256,2048]{1,0:T(8,128)(2,1)S(1)}, f32[32,2048]{1,0:T(8,128)S(1)}) custom-call(s32[3]{0:T(128)S(1)} %pad_add_fusion.here_ref, bf16[2,8,4,32,128]{4,3,2,1,0:T(8,128)(2,1)S(1)} %bitcast.21, bf16[512,2048]{1,0:T(8,128)(2,1)S(1)} %constant_dynamic-update-slice_fusion.near_w_ref, bf16[512,2048]{1,0:T(8,128)(2,1)} %collective-permute-done.3.far_w_ref, ...), custom_call_target="tpu_custom_call" | custom-call | flops 1073741824 | bytes 8388608 | tf_op jit(solution)/shard_map/group_rows/pallas_call | solution.py:220
  125.8 1.0 copy-done
  126.8 6.4 %feed_forward.1 = bf16[256,2048]{1,0:T(8,128)(2,1)S(1)} custom-call(bf16[256,2048]{1,0:T(8,128)(2,1)} %copy-done, bf16[16,2,2,3,32,704]{5,4,3,2,1,0:T(8,128)(2,1)} %bitcast.22), custom_call_target="tpu_custom_call" | custom-call | flops 2214592512 | bytes 8388608 | tf_op jit(solution)/shard_map/feed_forward/pallas_call | solution.py:297
  133.2 17.8 %all_to_all.26 = bf16[8,32,2048]{2,1,0:T(8,128)(2,1)S(1)} all-to-all(bf16[8,32,2048]{2,1,0:T(8,128)(2,1)S(1)} %bitcast.20), channel_id=1, replica_groups=mesh['zh'=8,'zl'=2,'y1'=2,'y0'=2,'x'=4,'c'=2] {'y0','x'}, dimensions={0} | all-to-all | bytes 2097152 | tf_op jit(solution)/shard_map/all_to_all | solution.py:331
  151.2 0.7 add_convert_fusion
  (27 shorter events, 1.8 us)
Async XLA Ops:
  6.5 24.8 %copy-start.1 = (bf16[128,2048]{1,0:T(8,128)(2,1)S(1)}, bf16[128,2048]{1,0:T(8,128)(2,1)}, u32[]{:S(2)}) copy-start(bf16[128,2048]{1,0:T(8,128)(2,1)} %param.19) | copy-start | bytes 1572868
  6.5 120.2 %all-gather.3.cloned.1.call-start = ((), (), s32[]{:S(2)}) async-start(), calls=%async_computation.5 | async-start | bytes 9732096 | tf_op jit(solution)/shard_map/all_gather | solution.py:342
  7.5 9.4 %collective-permute-start.8 = (bf16[96,704]{1,0:T(8,128)(2,1)S(1)}, bf16[96,704]{1,0:T(8,128)(2,1)S(1)}, u32[]{:S(2)}, u32[]{:S(2)}) collective-permute-start(bf16[96,704]{1,0:T(8,128)(2,1)S(1)} %pad_maximum_fusion.2), channel_id=1, source_target_pairs={{0,16},{1,24},{8,17},{9,25},{16,0},{17,8},{24,1},{25,9},{2,18},{3,... | collective-permute-start | bytes 405512 | tf_op jit(solution)/shard_map/ppermute | solution.py:322
  13.5 6.5 %collective-permute-start.9 = (bf16[96,704]{1,0:T(8,128)(2,1)S(1)}, bf16[96,704]{1,0:T(8,128)(2,1)S(1)}, u32[]{:S(2)}, u32[]{:S(2)}) collective-permute-start(bf16[96,704]{1,0:T(8,128)(2,1)S(1)} %pad_maximum_fusion.2), channel_id=1, source_target_pairs={{0,0},{1,8},{8,1},{9,9},{16,16},{17,24},{24,17},{25,25},{2,2},{3,1... | collective-permute-start | bytes 405512 | tf_op jit(solution)/shard_map/ppermute | solution.py:322
  20.8 13.9 %collective-permute-start = (bf16[128,2048]{1,0:T(8,128)(2,1)}, bf16[128,2048]{1,0:T(8,128)(2,1)S(1)}, u32[]{:S(2)}, u32[]{:S(2)}) collective-permute-start(bf16[128,2048]{1,0:T(8,128)(2,1)} %param.19), channel_id=1, source_target_pairs={{0,2},{2,4},{4,6},{6,0},{1,3},{3,5},{5,7},{7,1},{8,10},{10,12},{12... | collective-permute-start | bytes 1572872 | tf_op jit(solution)/shard_map/ppermute | solution.py:327
  23.9 24.3 %collective-permute-start.1 = (bf16[128,2048]{1,0:T(8,128)(2,1)}, bf16[128,2048]{1,0:T(8,128)(2,1)S(1)}, u32[]{:S(2)}, u32[]{:S(2)}) collective-permute-start(bf16[128,2048]{1,0:T(8,128)(2,1)} %param.19), channel_id=1, source_target_pairs={{0,4},{2,6},{4,0},{6,2},{1,5},{3,7},{5,1},{7,3},{8,12},{10,14},{12... | collective-permute-start | bytes 1572872 | tf_op jit(solution)/shard_map/ppermute | solution.py:327
  28.3 22.5 %collective-permute-start.2 = (bf16[128,2048]{1,0:T(8,128)(2,1)}, bf16[128,2048]{1,0:T(8,128)(2,1)S(1)}, u32[]{:S(2)}, u32[]{:S(2)}) collective-permute-start(bf16[128,2048]{1,0:T(8,128)(2,1)} %param.19), channel_id=1, source_target_pairs={{0,6},{2,0},{4,2},{6,4},{1,7},{3,1},{5,3},{7,5},{8,14},{10,8},{12,... | collective-permute-start | bytes 1572872 | tf_op jit(solution)/shard_map/ppermute | solution.py:327
  31.4 48.3 %copy-start.3 = (bf16[32,2048]{1,0:T(8,128)(2,1)S(1)}, bf16[32,2048]{1,0:T(8,128)(2,1)}, u32[]{:S(2)}) copy-start(bf16[32,2048]{1,0:T(8,128)(2,1)} %param.12) | copy-start | bytes 393220
  50.8 62.1 %copy-start.4 = (bf16[2048]{0:T(1024)(128)(2,1)S(1)}, bf16[2048]{0:T(1024)(128)(2,1)}, u32[]{:S(2)}) copy-start(bf16[2048]{0:T(1024)(128)(2,1)} %param.20) | copy-start | bytes 12292
  50.8 71.6 %collective-permute-start.3 = (bf16[512,2048]{1,0:T(8,128)(2,1)S(1)}, bf16[512,2048]{1,0:T(8,128)(2,1)}, u32[]{:S(2)}, u32[]{:S(2)}) collective-permute-start(bf16[512,2048]{1,0:T(8,128)(2,1)S(1)} %constant_dynamic-update-slice_fusion.near_w_ref), channel_id=1, source_target_pairs={{0,1},{1,0},{2,3},{3,2},{4,5},{5,4},{6,7},{7,6},{8,9},{9,8},{10,11... | collective-permute-start | bytes 6291464 | tf_op jit(solution)/shard_map/ppermute | solution.py:327
  65.3 26.7 %all-to-all-start.1 = ((bf16[8,24,128]{2,1,0:T(8,128)(2,1)}), bf16[8,24,128]{2,1,0:T(8,128)(2,1)S(1)}, u32[]{:S(2)}, u32[]{:S(2)}) async-start(bf16[8,24,128]{2,1,0:T(8,128)(2,1)} %joined_state.1), calls=%async_computation.1 | async-start | bytes 98304 | tf_op jit(solution)/shard_map/all_to_all | solution.py:331
  79.7 16.4 %collective-permute-start.6 = (bf16[32,2048]{1,0:T(8,128)(2,1)S(1)}, bf16[32,2048]{1,0:T(8,128)(2,1)S(1)}, u32[]{:S(2)}, u32[]{:S(2)}) collective-permute-start(bf16[32,2048]{1,0:T(8,128)(2,1)S(1)} %copy-done.3), channel_id=1, source_target_pairs={{0,6},{2,0},{4,2},{6,4},{1,7},{3,1},{5,3},{7,5},{8,14},{10,8},{12,... | collective-permute-start | bytes 393224 | tf_op jit(solution)/shard_map/ppermute | solution.py:327
  84.0 12.1 %collective-permute-start.5 = (bf16[32,2048]{1,0:T(8,128)(2,1)S(1)}, bf16[32,2048]{1,0:T(8,128)(2,1)S(1)}, u32[]{:S(2)}, u32[]{:S(2)}) collective-permute-start(bf16[32,2048]{1,0:T(8,128)(2,1)S(1)} %copy-done.3), channel_id=1, source_target_pairs={{0,4},{2,6},{4,0},{6,2},{1,5},{3,7},{5,1},{7,3},{8,12},{10,14},{12... | collective-permute-start | bytes 393224 | tf_op jit(solution)/shard_map/ppermute | solution.py:327
  87.3 8.8 %collective-permute-start.4 = (bf16[32,2048]{1,0:T(8,128)(2,1)S(1)}, bf16[32,2048]{1,0:T(8,128)(2,1)S(1)}, u32[]{:S(2)}, u32[]{:S(2)}) collective-permute-start(bf16[32,2048]{1,0:T(8,128)(2,1)S(1)} %copy-done.3), channel_id=1, source_target_pairs={{0,2},{2,4},{4,6},{6,0},{1,3},{3,5},{5,7},{7,1},{8,10},{10,12},{12... | collective-permute-start | bytes 393224 | tf_op jit(solution)/shard_map/ppermute | solution.py:327
  92.7 8.6 %all-to-all-start.2 = ((f32[8,16,128]{2,1,0:T(8,128)}), f32[8,16,128]{2,1,0:T(8,128)S(1)}, u32[]{:S(2)}, u32[]{:S(2)}) async-start(f32[8,16,128]{2,1,0:T(8,128)} %incoming_state.1), calls=%async_computation.2 | async-start | bytes 131072 | tf_op jit(solution)/shard_map/all_to_all | solution.py:331
  96.2 16.8 %collective-permute-start.7 = (bf16[4,32,2048]{2,1,0:T(8,128)(2,1)S(1)}, bf16[4,32,2048]{2,1,0:T(8,128)(2,1)}, u32[]{:S(2)}, u32[]{:S(2)}) collective-permute-start(bf16[4,32,2048]{2,1,0:T(8,128)(2,1)S(1)} %pad_maximum_fusion.near_s_ref), channel_id=1, source_target_pairs={{0,8},{8,0},{1,9},{9,1},{2,10},{10,2},{3,11},{11,3},{4,12},{12,4},... | collective-permute-start | bytes 1572872 | tf_op jit(solution)/shard_map/ppermute | solution.py:327
  101.3 0.6 copy-start.2
  104.1 18.3 %all-to-all-start.3 = ((bf16[16,4,32,128]{3,2,1,0:T(8,128)(2,1)}), bf16[16,4,32,128]{3,2,1,0:T(8,128)(2,1)S(1)}, u32[]{:S(2)}, u32[]{:S(2)}) async-start(bf16[16,4,32,128]{3,2,1,0:T(8,128)(2,1)} %bitcast.23), calls=%async_computation.3 | async-start | bytes 1048576 | tf_op jit(solution)/shard_map/all_to_all | solution.py:331
  125.8 1.0 copy-start
Sparse Core Ops, SparseCore 0:
  20.9 83.6 all-gather.2

commit v9 on v8

--- a/solution.py
+++ b/solution.py
@@ -272,8 +272,9 @@
         return held[kind, n * each : (n + 1) * each].reshape(depth, hidden_width), depth
 
     fetch = pltpu.make_async_copy(rows_ref, rows, rows_sem)
+    start(0)
     fetch.start()
-    for at in range(AHEAD):
+    for at in range(1, AHEAD):
         start(at)
     fetch.wait()
     sums = []
@@ -383,8 +384,11 @@
         here, mixed.reshape(2, 8, *mixed.shape[1:]), near_w, far_w, near_s, far_s, norm_gain.reshape(1, -1)
     )
     down_terms = feed_forward(normed, weights)
-    mixer_out = exchange(down_terms.reshape(8, rows // 8, width), GROUP).astype(F32).sum(axis=0)
-    return (residual + mixer_out).astype(BF16)
+    terms = exchange(down_terms.reshape(8, rows // 8, width), GROUP)
+    result = residual
+    for n in range(8):
+        result = result + terms[n].astype(F32)
+    return result.astype(BF16)
 
 
 def solution(mesh):

time: 160 us -> 160 us (level)
  no operation moved by 1% of the time
where the time goes in v9:
time: 160 us; the launch traced here: 159 us
  starting transfers between devices  61.1 us (38%)
  waiting for transfers between devices  37.9 us (24%)
  blocking collectives  26.5 us (17%)
  Pallas kernels  15.2 us (10%)
  between operations  13.6 us (8%)
  other arithmetic  2.66 us (2%)
  local copies, waits for them, and re-layouts  1.79 us (1%)
    ppermute x8, starting transfers between devices, shifted(): lax.ppermute(value, axis, [(i, (i + by) % length) for i in range(length)])  26.7 us
    all_to_all x3, starting transfers between devices, exchange(): return lax.all_to_all(tiles, axes, split_axis=0, concat_axis=0, tiled=True)  26.5 us
    all_to_all x2, blocking collectives, exchange(): return lax.all_to_all(tiles, axes, split_axis=0, concat_axis=0, tiled=True)  26.5 us
    ppermute x8, waiting for transfers between devices, shifted(): lax.ppermute(value, axis, [(i, (i + by) % length) for i in range(length)])  19.3 us
    all_to_all x3, waiting for transfers between devices, exchange(): return lax.all_to_all(tiles, axes, split_axis=0, concat_axis=0, tiled=True)  14 us
    ppermute x2, starting transfers between devices, moved(): return lax.ppermute(value, axes, pairs)  7.94 us
    pallas_call x1, Pallas kernels, feed_forward(): pl.pallas_call(ffn_kernel, out_shape=jax.ShapeDtypeStruct((count, width),...  6.41 us
    ppermute x2, waiting for transfers between devices, moved(): return lax.ppermute(value, axes, pairs)  4.53 us
  transfers between devices with their start and end apart: 14, of which 8 were waited for; matrix products, arithmetic and copies ran while one was open for 0% of the time, Pallas kernels for 6%

profile of v9, /device:TPU:1, one launch (start us, length us, event | category | flops | bytes accessed | tf_op | source)
XLA Modules:
  0.0 158.7 jit_solution(2608452056810969009)
XLA Ops:
  6.5 0.9 pad_maximum_fusion.2
  7.5 6.0 %collective-permute-start.8 = (bf16[96,704]{1,0:T(8,128)(2,1)S(1)}, bf16[96,704]{1,0:T(8,128)(2,1)S(1)}, u32[]{:S(2)}, u32[]{:S(2)}) collective-permute-start(bf16[96,704]{1,0:T(8,128)(2,1)S(1)} %pad_maximum_fusion.2), channel_id=1, source_target_pairs={{0,16},{1,24},{8,17},{9,25},{16,0},{17,8},{24,1},{25,9},{2,18},{3,... | collective-permute-start | bytes 405512 | tf_op jit(solution)/shard_map/ppermute | solution.py:323
  13.5 1.9 %collective-permute-start.9 = (bf16[96,704]{1,0:T(8,128)(2,1)S(1)}, bf16[96,704]{1,0:T(8,128)(2,1)S(1)}, u32[]{:S(2)}, u32[]{:S(2)}) collective-permute-start(bf16[96,704]{1,0:T(8,128)(2,1)S(1)} %pad_maximum_fusion.2), channel_id=1, source_target_pairs={{0,0},{1,8},{8,1},{9,9},{16,16},{17,24},{24,17},{25,25},{2,2},{3,1... | collective-permute-start | bytes 405512 | tf_op jit(solution)/shard_map/ppermute | solution.py:323
  15.4 1.4 collective-permute-done.8
  16.9 3.1 %collective-permute-done.9 = bf16[96,704]{1,0:T(8,128)(2,1)S(1)} collective-permute-done((bf16[96,704]{1,0:T(8,128)(2,1)S(1)}, bf16[96,704]{1,0:T(8,128)(2,1)S(1)}, u32[]{:S(2)}, u32[]{:S(2)}) %collective-permute-start.9) | collective-permute-done | bytes 135200 | tf_op jit(solution)/shard_map/ppermute | solution.py:323
  20.0 0.8 pad_maximum_fusion.1
  20.8 3.1 %collective-permute-start = (bf16[128,2048]{1,0:T(8,128)(2,1)}, bf16[128,2048]{1,0:T(8,128)(2,1)S(1)}, u32[]{:S(2)}, u32[]{:S(2)}) collective-permute-start(bf16[128,2048]{1,0:T(8,128)(2,1)} %param.19), channel_id=1, source_target_pairs={{0,2},{2,4},{4,6},{6,0},{1,3},{3,5},{5,7},{7,1},{8,10},{10,12},{12... | collective-permute-start | bytes 1572872 | tf_op jit(solution)/shard_map/ppermute | solution.py:328
  23.9 4.4 %collective-permute-start.1 = (bf16[128,2048]{1,0:T(8,128)(2,1)}, bf16[128,2048]{1,0:T(8,128)(2,1)S(1)}, u32[]{:S(2)}, u32[]{:S(2)}) collective-permute-start(bf16[128,2048]{1,0:T(8,128)(2,1)} %param.19), channel_id=1, source_target_pairs={{0,4},{2,6},{4,0},{6,2},{1,5},{3,7},{5,1},{7,3},{8,12},{10,14},{12... | collective-permute-start | bytes 1572872 | tf_op jit(solution)/shard_map/ppermute | solution.py:328
  28.3 3.1 %collective-permute-start.2 = (bf16[128,2048]{1,0:T(8,128)(2,1)}, bf16[128,2048]{1,0:T(8,128)(2,1)S(1)}, u32[]{:S(2)}, u32[]{:S(2)}) collective-permute-start(bf16[128,2048]{1,0:T(8,128)(2,1)} %param.19), channel_id=1, source_target_pairs={{0,6},{2,0},{4,2},{6,4},{1,7},{3,1},{5,3},{7,5},{8,14},{10,8},{12,... | collective-permute-start | bytes 1572872 | tf_op jit(solution)/shard_map/ppermute | solution.py:328
  31.4 3.3 %collective-permute-done = bf16[128,2048]{1,0:T(8,128)(2,1)S(1)} collective-permute-done((bf16[128,2048]{1,0:T(8,128)(2,1)}, bf16[128,2048]{1,0:T(8,128)(2,1)S(1)}, u32[]{:S(2)}, u32[]{:S(2)}) %collective-permute-start) | collective-permute-done | bytes 524320 | tf_op jit(solution)/shard_map/ppermute | solution.py:328
  34.7 13.5 %collective-permute-done.1 = bf16[128,2048]{1,0:T(8,128)(2,1)S(1)} collective-permute-done((bf16[128,2048]{1,0:T(8,128)(2,1)}, bf16[128,2048]{1,0:T(8,128)(2,1)S(1)}, u32[]{:S(2)}, u32[]{:S(2)}) %collective-permute-start.1) | collective-permute-done | bytes 524320 | tf_op jit(solution)/shard_map/ppermute | solution.py:328
  48.2 2.5 %collective-permute-done.2 = bf16[128,2048]{1,0:T(8,128)(2,1)S(1)} collective-permute-done((bf16[128,2048]{1,0:T(8,128)(2,1)}, bf16[128,2048]{1,0:T(8,128)(2,1)S(1)}, u32[]{:S(2)}, u32[]{:S(2)}) %collective-permute-start.2) | collective-permute-done | bytes 524320 | tf_op jit(solution)/shard_map/ppermute | solution.py:328
  50.8 3.4 %collective-permute-start.3 = (bf16[512,2048]{1,0:T(8,128)(2,1)S(1)}, bf16[512,2048]{1,0:T(8,128)(2,1)}, u32[]{:S(2)}, u32[]{:S(2)}) collective-permute-start(bf16[512,2048]{1,0:T(8,128)(2,1)S(1)} %constant_dynamic-update-slice_fusion.near_w_ref), channel_id=1, source_target_pairs={{0,1},{1,0},{2,3},{3,2},{4,5},{5,4},{6,7},{7,6},{8,9},{9,8},{10,11... | collective-permute-start | bytes 6291464 | tf_op jit(solution)/shard_map/ppermute | solution.py:328
  54.2 1.9 %retention.1 = (f32[256,128]{1,0:T(8,128)}, bf16[256,128]{1,0:T(8,128)(2,1)}, f32[8,24,128]{2,1,0:T(8,128)}) custom-call(bf16[256,128]{1,0:T(8,128)(2,1)} %q_ref.1, bf16[256,128]{1,0:T(8,128)(2,1)} %k_ref.1, bf16[256,128]{1,0:T(8,128)(2,1)} %v_ref.1, f32[1,256]{1,0:T(1,128)} %bitcast.70), custom_call_target="tpu_custom_call" | custom-call | flops 50331648 | bytes 1048576 | tf_op jit(solution)/shard_map/retention/pallas_call | solution.py:68
  56.1 8.6 %all_to_all.25.states_ref = f32[8,24,128]{2,1,0:T(8,128)S(1)} all-to-all(f32[8,24,128]{2,1,0:T(8,128)} %get-tuple-element.12), channel_id=1, replica_groups=mesh['zh'=8,'zl'=2,'y1'=2,'y0'=2,'x'=4,'c'=2] {'zl','y1','y0'}, dimensions={0} | all-to-all | bytes 196608 | tf_op jit(solution)/shard_map/all_to_all | solution.py:332
  65.3 14.3 %all-to-all-start.1 = ((bf16[8,24,128]{2,1,0:T(8,128)(2,1)}), bf16[8,24,128]{2,1,0:T(8,128)(2,1)S(1)}, u32[]{:S(2)}, u32[]{:S(2)}) async-start(bf16[8,24,128]{2,1,0:T(8,128)(2,1)} %joined_state.1), calls=%async_computation.1 | async-start | bytes 98304 | tf_op jit(solution)/shard_map/all_to_all | solution.py:332
  79.7 4.3 %collective-permute-start.6 = (bf16[32,2048]{1,0:T(8,128)(2,1)S(1)}, bf16[32,2048]{1,0:T(8,128)(2,1)S(1)}, u32[]{:S(2)}, u32[]{:S(2)}) collective-permute-start(bf16[32,2048]{1,0:T(8,128)(2,1)S(1)} %copy-done.3), channel_id=1, source_target_pairs={{0,6},{2,0},{4,2},{6,4},{1,7},{3,1},{5,3},{7,5},{8,14},{10,8},{12,... | collective-permute-start | bytes 393224 | tf_op jit(solution)/shard_map/ppermute | solution.py:328
  84.0 3.2 %collective-permute-start.5 = (bf16[32,2048]{1,0:T(8,128)(2,1)S(1)}, bf16[32,2048]{1,0:T(8,128)(2,1)S(1)}, u32[]{:S(2)}, u32[]{:S(2)}) collective-permute-start(bf16[32,2048]{1,0:T(8,128)(2,1)S(1)} %copy-done.3), channel_id=1, source_target_pairs={{0,4},{2,6},{4,0},{6,2},{1,5},{3,7},{5,1},{7,3},{8,12},{10,14},{12... | collective-permute-start | bytes 393224 | tf_op jit(solution)/shard_map/ppermute | solution.py:328
  87.3 1.9 %collective-permute-start.4 = (bf16[32,2048]{1,0:T(8,128)(2,1)S(1)}, bf16[32,2048]{1,0:T(8,128)(2,1)S(1)}, u32[]{:S(2)}, u32[]{:S(2)}) collective-permute-start(bf16[32,2048]{1,0:T(8,128)(2,1)S(1)} %copy-done.3), channel_id=1, source_target_pairs={{0,2},{2,4},{4,6},{6,0},{1,3},{3,5},{5,7},{7,1},{8,10},{10,12},{12... | collective-permute-start | bytes 393224 | tf_op jit(solution)/shard_map/ppermute | solution.py:328
  89.2 2.8 %all-to-all-done.1.joined_ref = bf16[8,24,128]{2,1,0:T(8,128)(2,1)S(1)} async-done(((bf16[8,24,128]{2,1,0:T(8,128)(2,1)}), bf16[8,24,128]{2,1,0:T(8,128)(2,1)S(1)}, u32[]{:S(2)}, u32[]{:S(2)}) %all-to-all-start.1) | async-done | bytes 49184 | tf_op jit(solution)/shard_map/all_to_all | solution.py:332
  92.1 0.7 incoming_state.1
  92.8 3.3 %all-to-all-start.2 = ((f32[8,16,128]{2,1,0:T(8,128)}), f32[8,16,128]{2,1,0:T(8,128)S(1)}, u32[]{:S(2)}, u32[]{:S(2)}) async-start(f32[8,16,128]{2,1,0:T(8,128)} %incoming_state.1), calls=%async_computation.2 | async-start | bytes 131072 | tf_op jit(solution)/shard_map/all_to_all | solution.py:332
  96.2 3.3 %collective-permute-start.7 = (bf16[4,32,2048]{2,1,0:T(8,128)(2,1)S(1)}, bf16[4,32,2048]{2,1,0:T(8,128)(2,1)}, u32[]{:S(2)}, u32[]{:S(2)}) collective-permute-start(bf16[4,32,2048]{2,1,0:T(8,128)(2,1)S(1)} %pad_maximum_fusion.near_s_ref), channel_id=1, source_target_pairs={{0,8},{8,0},{1,9},{9,1},{2,10},{10,2},{3,11},{11,3},{4,12},{12,4},... | collective-permute-start | bytes 1572872 | tf_op jit(solution)/shard_map/ppermute | solution.py:328
  99.5 1.8 %all-to-all-done.2 = f32[8,16,128]{2,1,0:T(8,128)S(1)} async-done(((f32[8,16,128]{2,1,0:T(8,128)}), f32[8,16,128]{2,1,0:T(8,128)S(1)}, u32[]{:S(2)}, u32[]{:S(2)}) %all-to-all-start.2) | async-done | bytes 65568 | tf_op jit(solution)/shard_map/all_to_all | solution.py:332
  101.9 2.1 %mix.1 = bf16[8,2,4,32,128]{4,3,2,1,0:T(8,128)(2,1)} custom-call(f32[256,128]{1,0:T(8,128)} %get-tuple-element.10.within_ref, bf16[256,128]{1,0:T(8,128)(2,1)} %get-tuple-element.11.carry_q_ref, f32[128,128]{1,0:T(8,128)} %bitcast.64, bf16[256,128]{1,0:T(8,128)(2,1)} %gate_ref.1, bf16[1,128]{1,0:T(2,128)(2,1)} %bitcast.71), custom_call_target="tpu_custom_call" | custom-call | flops 8388608 | bytes 1048576 | tf_op jit(solution)/shard_map/mix/pallas_call | solution.py:158
  104.1 8.8 %all-to-all-start.3 = ((bf16[16,4,32,128]{3,2,1,0:T(8,128)(2,1)}), bf16[16,4,32,128]{3,2,1,0:T(8,128)(2,1)S(1)}, u32[]{:S(2)}, u32[]{:S(2)}) async-start(bf16[16,4,32,128]{3,2,1,0:T(8,128)(2,1)} %bitcast.63), calls=%async_computation.3 | async-start | bytes 1048576 | tf_op jit(solution)/shard_map/all_to_all | solution.py:332
  113.0 9.4 %all-to-all-done.3 = bf16[16,4,32,128]{3,2,1,0:T(8,128)(2,1)S(1)} async-done(((bf16[16,4,32,128]{3,2,1,0:T(8,128)(2,1)}), bf16[16,4,32,128]{3,2,1,0:T(8,128)(2,1)S(1)}, u32[]{:S(2)}, u32[]{:S(2)}) %all-to-all-start.3) | async-done | bytes 524320 | tf_op jit(solution)/shard_map/all_to_all | solution.py:332
  122.4 3.4 %group_rows.1 = (bf16[256,2048]{1,0:T(8,128)(2,1)S(1)}, f32[32,2048]{1,0:T(8,128)S(1)}) custom-call(s32[3]{0:T(128)S(1)} %pad_add_fusion.here_ref, bf16[2,8,4,32,128]{4,3,2,1,0:T(8,128)(2,1)S(1)} %bitcast.61, bf16[512,2048]{1,0:T(8,128)(2,1)S(1)} %constant_dynamic-update-slice_fusion.near_w_ref, bf16[512,2048]{1,0:T(8,128)(2,1)} %collective-permute-done.3.far_w_ref, ...), custom_call_target="tpu_custom_call" | custom-call | flops 1073741824 | bytes 8388608 | tf_op jit(solution)/shard_map/group_rows/pallas_call | solution.py:220
  125.8 1.0 copy-done
  126.8 6.4 %feed_forward.1 = bf16[256,2048]{1,0:T(8,128)(2,1)S(1)} custom-call(bf16[256,2048]{1,0:T(8,128)(2,1)} %copy-done, bf16[16,2,2,3,32,704]{5,4,3,2,1,0:T(8,128)(2,1)} %bitcast.62), custom_call_target="tpu_custom_call" | custom-call | flops 2214592512 | bytes 8388608 | tf_op jit(solution)/shard_map/feed_forward/pallas_call | solution.py:298
  133.2 17.8 %all_to_all.26 = bf16[8,32,2048]{2,1,0:T(8,128)(2,1)S(1)} all-to-all(bf16[8,32,2048]{2,1,0:T(8,128)(2,1)S(1)} %bitcast.60), channel_id=1, replica_groups=mesh['zh'=8,'zl'=2,'y1'=2,'y0'=2,'x'=4,'c'=2] {'y0','x'}, dimensions={0} | all-to-all | bytes 2097152 | tf_op jit(solution)/shard_map/all_to_all | solution.py:332
  151.0 0.8 fusion
  (26 shorter events, 1.6 us)
Async XLA Ops:
  6.5 24.8 %copy-start.1 = (bf16[128,2048]{1,0:T(8,128)(2,1)S(1)}, bf16[128,2048]{1,0:T(8,128)(2,1)}, u32[]{:S(2)}) copy-start(bf16[128,2048]{1,0:T(8,128)(2,1)} %param.19) | copy-start | bytes 1572868
  6.5 120.3 %all-gather.3.cloned.1.call-start = ((), (), s32[]{:S(2)}) async-start(), calls=%async_computation.5 | async-start | bytes 9732096 | tf_op jit(solution)/shard_map/all_gather | solution.py:343
  7.5 9.4 %collective-permute-start.8 = (bf16[96,704]{1,0:T(8,128)(2,1)S(1)}, bf16[96,704]{1,0:T(8,128)(2,1)S(1)}, u32[]{:S(2)}, u32[]{:S(2)}) collective-permute-start(bf16[96,704]{1,0:T(8,128)(2,1)S(1)} %pad_maximum_fusion.2), channel_id=1, source_target_pairs={{0,16},{1,24},{8,17},{9,25},{16,0},{17,8},{24,1},{25,9},{2,18},{3,... | collective-permute-start | bytes 405512 | tf_op jit(solution)/shard_map/ppermute | solution.py:323
  13.5 6.5 %collective-permute-start.9 = (bf16[96,704]{1,0:T(8,128)(2,1)S(1)}, bf16[96,704]{1,0:T(8,128)(2,1)S(1)}, u32[]{:S(2)}, u32[]{:S(2)}) collective-permute-start(bf16[96,704]{1,0:T(8,128)(2,1)S(1)} %pad_maximum_fusion.2), channel_id=1, source_target_pairs={{0,0},{1,8},{8,1},{9,9},{16,16},{17,24},{24,17},{25,25},{2,2},{3,1... | collective-permute-start | bytes 405512 | tf_op jit(solution)/shard_map/ppermute | solution.py:323
  20.8 13.9 %collective-permute-start = (bf16[128,2048]{1,0:T(8,128)(2,1)}, bf16[128,2048]{1,0:T(8,128)(2,1)S(1)}, u32[]{:S(2)}, u32[]{:S(2)}) collective-permute-start(bf16[128,2048]{1,0:T(8,128)(2,1)} %param.19), channel_id=1, source_target_pairs={{0,2},{2,4},{4,6},{6,0},{1,3},{3,5},{5,7},{7,1},{8,10},{10,12},{12... | collective-permute-start | bytes 1572872 | tf_op jit(solution)/shard_map/ppermute | solution.py:328
  23.9 24.3 %collective-permute-start.1 = (bf16[128,2048]{1,0:T(8,128)(2,1)}, bf16[128,2048]{1,0:T(8,128)(2,1)S(1)}, u32[]{:S(2)}, u32[]{:S(2)}) collective-permute-start(bf16[128,2048]{1,0:T(8,128)(2,1)} %param.19), channel_id=1, source_target_pairs={{0,4},{2,6},{4,0},{6,2},{1,5},{3,7},{5,1},{7,3},{8,12},{10,14},{12... | collective-permute-start | bytes 1572872 | tf_op jit(solution)/shard_map/ppermute | solution.py:328
  28.3 22.5 %collective-permute-start.2 = (bf16[128,2048]{1,0:T(8,128)(2,1)}, bf16[128,2048]{1,0:T(8,128)(2,1)S(1)}, u32[]{:S(2)}, u32[]{:S(2)}) collective-permute-start(bf16[128,2048]{1,0:T(8,128)(2,1)} %param.19), channel_id=1, source_target_pairs={{0,6},{2,0},{4,2},{6,4},{1,7},{3,1},{5,3},{7,5},{8,14},{10,8},{12,... | collective-permute-start | bytes 1572872 | tf_op jit(solution)/shard_map/ppermute | solution.py:328
  31.4 48.3 %copy-start.3 = (bf16[32,2048]{1,0:T(8,128)(2,1)S(1)}, bf16[32,2048]{1,0:T(8,128)(2,1)}, u32[]{:S(2)}) copy-start(bf16[32,2048]{1,0:T(8,128)(2,1)} %param.12) | copy-start | bytes 393220
  50.8 62.1 %copy-start.4 = (bf16[2048]{0:T(1024)(128)(2,1)S(1)}, bf16[2048]{0:T(1024)(128)(2,1)}, u32[]{:S(2)}) copy-start(bf16[2048]{0:T(1024)(128)(2,1)} %param.20) | copy-start | bytes 12292
  50.8 71.6 %collective-permute-start.3 = (bf16[512,2048]{1,0:T(8,128)(2,1)S(1)}, bf16[512,2048]{1,0:T(8,128)(2,1)}, u32[]{:S(2)}, u32[]{:S(2)}) collective-permute-start(bf16[512,2048]{1,0:T(8,128)(2,1)S(1)} %constant_dynamic-update-slice_fusion.near_w_ref), channel_id=1, source_target_pairs={{0,1},{1,0},{2,3},{3,2},{4,5},{5,4},{6,7},{7,6},{8,9},{9,8},{10,11... | collective-permute-start | bytes 6291464 | tf_op jit(solution)/shard_map/ppermute | solution.py:328
  65.3 26.7 %all-to-all-start.1 = ((bf16[8,24,128]{2,1,0:T(8,128)(2,1)}), bf16[8,24,128]{2,1,0:T(8,128)(2,1)S(1)}, u32[]{:S(2)}, u32[]{:S(2)}) async-start(bf16[8,24,128]{2,1,0:T(8,128)(2,1)} %joined_state.1), calls=%async_computation.1 | async-start | bytes 98304 | tf_op jit(solution)/shard_map/all_to_all | solution.py:332
  79.7 16.4 %collective-permute-start.6 = (bf16[32,2048]{1,0:T(8,128)(2,1)S(1)}, bf16[32,2048]{1,0:T(8,128)(2,1)S(1)}, u32[]{:S(2)}, u32[]{:S(2)}) collective-permute-start(bf16[32,2048]{1,0:T(8,128)(2,1)S(1)} %copy-done.3), channel_id=1, source_target_pairs={{0,6},{2,0},{4,2},{6,4},{1,7},{3,1},{5,3},{7,5},{8,14},{10,8},{12,... | collective-permute-start | bytes 393224 | tf_op jit(solution)/shard_map/ppermute | solution.py:328
  84.0 12.1 %collective-permute-start.5 = (bf16[32,2048]{1,0:T(8,128)(2,1)S(1)}, bf16[32,2048]{1,0:T(8,128)(2,1)S(1)}, u32[]{:S(2)}, u32[]{:S(2)}) collective-permute-start(bf16[32,2048]{1,0:T(8,128)(2,1)S(1)} %copy-done.3), channel_id=1, source_target_pairs={{0,4},{2,6},{4,0},{6,2},{1,5},{3,7},{5,1},{7,3},{8,12},{10,14},{12... | collective-permute-start | bytes 393224 | tf_op jit(solution)/shard_map/ppermute | solution.py:328
  87.3 8.9 %collective-permute-start.4 = (bf16[32,2048]{1,0:T(8,128)(2,1)S(1)}, bf16[32,2048]{1,0:T(8,128)(2,1)S(1)}, u32[]{:S(2)}, u32[]{:S(2)}) collective-permute-start(bf16[32,2048]{1,0:T(8,128)(2,1)S(1)} %copy-done.3), channel_id=1, source_target_pairs={{0,2},{2,4},{4,6},{6,0},{1,3},{3,5},{5,7},{7,1},{8,10},{10,12},{12... | collective-permute-start | bytes 393224 | tf_op jit(solution)/shard_map/ppermute | solution.py:328
  92.8 8.5 %all-to-all-start.2 = ((f32[8,16,128]{2,1,0:T(8,128)}), f32[8,16,128]{2,1,0:T(8,128)S(1)}, u32[]{:S(2)}, u32[]{:S(2)}) async-start(f32[8,16,128]{2,1,0:T(8,128)} %incoming_state.1), calls=%async_computation.2 | async-start | bytes 131072 | tf_op jit(solution)/shard_map/all_to_all | solution.py:332
  96.2 16.8 %collective-permute-start.7 = (bf16[4,32,2048]{2,1,0:T(8,128)(2,1)S(1)}, bf16[4,32,2048]{2,1,0:T(8,128)(2,1)}, u32[]{:S(2)}, u32[]{:S(2)}) collective-permute-start(bf16[4,32,2048]{2,1,0:T(8,128)(2,1)S(1)} %pad_maximum_fusion.near_s_ref), channel_id=1, source_target_pairs={{0,8},{8,0},{1,9},{9,1},{2,10},{10,2},{3,11},{11,3},{4,12},{12,4},... | collective-permute-start | bytes 1572872 | tf_op jit(solution)/shard_map/ppermute | solution.py:328
  101.3 0.6 copy-start.2
  104.1 18.3 %all-to-all-start.3 = ((bf16[16,4,32,128]{3,2,1,0:T(8,128)(2,1)}), bf16[16,4,32,128]{3,2,1,0:T(8,128)(2,1)S(1)}, u32[]{:S(2)}, u32[]{:S(2)}) async-start(bf16[16,4,32,128]{3,2,1,0:T(8,128)(2,1)} %bitcast.63), calls=%async_computation.3 | async-start | bytes 1048576 | tf_op jit(solution)/shard_map/all_to_all | solution.py:332
  125.8 1.0 copy-start
Sparse Core Ops, SparseCore 0:
  20.9 83.6 all-gather.2

commit v10 on v9

--- a/solution.py
+++ b/solution.py
@@ -240,7 +240,7 @@
 AHEAD = 2
 
 
-def ffn_kernel(rows_ref, weight_ref, out_ref, rows, held, rows_sem, sems):
+def ffn_kernel(y1_ref, rows_ref, weight_ref, out_ref, rows, held, rows_sem, sems):
     z, _, _, kinds, lines, hidden_width = weight_ref.shape
 
     def copies(kind, n):
@@ -248,7 +248,7 @@
         span = pl.ds(n * each, each)
         return [
             pltpu.make_async_copy(
-                weight_ref.at[span, y0, y1, kind],
+                weight_ref.at[span, y0, jnp.where(y1_ref[0] == y1, 0, 1), kind],
                 held.at[kind, span, y1, y0],
                 sems.at[kind, n, 2 * y1 + y0],
             )
@@ -292,13 +292,13 @@
         out_ref[:, n * depth : (n + 1) * depth] = dot_nt(hidden, block).astype(BF16)
 
 
-def feed_forward(rows, weights):
+def feed_forward(here, rows, weights):
     count, width = rows.shape
     z, y0, y1, kinds, lines, hidden_width = weights.shape
     return pl.pallas_call(
         ffn_kernel,
         out_shape=jax.ShapeDtypeStruct((count, width), BF16),
-        in_specs=[pl.BlockSpec(memory_space=pltpu.HBM)] * 2,
+        in_specs=[pl.BlockSpec(memory_space=pltpu.SMEM)] + [pl.BlockSpec(memory_space=pltpu.HBM)] * 2,
         out_specs=pl.BlockSpec(memory_space=pltpu.VMEM),
         scratch_shapes=[
             pltpu.VMEM((count, width), BF16),
@@ -309,7 +309,7 @@
         cost_estimate=kernel_cost(6 * count * width * hidden_width, 2**23, count * hidden_width),
         compiler_params=pltpu.CompilerParams(vmem_limit_bytes=52 * 2**20),
         name="feed_forward",
-    )(rows, weights)
+    )(here, rows, weights)
 
 
 def moved(value, axes, place):
@@ -338,8 +338,7 @@
     axes = ("y1", "y0", "c")
     near = moved(mine, axes, lambda y1, y0, c: (y1, c, y0))
     far = moved(mine, axes, lambda y1, y0, c: (1 - y1, c, y0))
-    upper = lax.axis_index("y1") == 1
-    pair = jnp.stack([jnp.where(upper, far, near), jnp.where(upper, near, far)])
+    pair = jnp.concatenate([near, far], axis=0)
     whole = lax.all_gather(pair, Z + ("c",), axis=0)
     return whole.reshape(16, 2, 2, 3, lines // 3, width)
 
@@ -383,7 +382,8 @@
     normed, residual = group_rows(
         here, mixed.reshape(2, 8, *mixed.shape[1:]), near_w, far_w, near_s, far_s, norm_gain.reshape(1, -1)
     )
-    down_terms = feed_forward(normed, weights)
+    y1 = lax.axis_index("y1").astype(jnp.int32).reshape(1)
+    down_terms = feed_forward(y1, normed, weights)
     terms = exchange(down_terms.reshape(8, rows // 8, width), GROUP)
     result = residual
     for n in range(8):

time: 160 us -> 160 us (level)
  transfers between devices with their start and end apart: 14 -> 14, of which waited for: 8 -> 8; matrix products, arithmetic and copies ran while one was open for 0% -> 1% of each run, Pallas kernels for 6% -> 6%
where the time goes in v10:
time: 160 us; the launch traced here: 159 us
  starting transfers between devices  61.1 us (38%)
  waiting for transfers between devices  36.8 us (23%)
  blocking collectives  26.5 us (17%)
  Pallas kernels  15.2 us (10%)
  between operations  13.6 us (8%)
  local copies, waits for them, and re-layouts  2.82 us (2%)
  other arithmetic  2.57 us (2%)
    ppermute x8, starting transfers between devices, shifted(): lax.ppermute(value, axis, [(i, (i + by) % length) for i in range(length)])  26.7 us
    all_to_all x3, starting transfers between devices, exchange(): return lax.all_to_all(tiles, axes, split_axis=0, concat_axis=0, tiled=True)  26.5 us
    all_to_all x2, blocking collectives, exchange(): return lax.all_to_all(tiles, axes, split_axis=0, concat_axis=0, tiled=True)  26.5 us
    ppermute x8, waiting for transfers between devices, shifted(): lax.ppermute(value, axis, [(i, (i + by) % length) for i in range(length)])  18.2 us
    all_to_all x3, waiting for transfers between devices, exchange(): return lax.all_to_all(tiles, axes, split_axis=0, concat_axis=0, tiled=True)  14.1 us
    ppermute x2, starting transfers between devices, moved(): return lax.ppermute(value, axes, pairs)  7.94 us
    pallas_call x1, Pallas kernels, feed_forward(): pl.pallas_call(ffn_kernel, out_shape=jax.ShapeDtypeStruct((count, width),...  6.41 us
    ppermute x2, waiting for transfers between devices, moved(): return lax.ppermute(value, axes, pairs)  4.53 us
  transfers between devices with their start and end apart: 14, of which 8 were waited for; matrix products, arithmetic and copies ran while one was open for 1% of the time, Pallas kernels for 6%

profile of v10, /device:TPU:1, one launch (start us, length us, event | category | flops | bytes accessed | tf_op | source)
XLA Modules:
  0.0 158.6 jit_solution(10258713948689721328)
XLA Ops:
  6.5 0.9 pad_maximum_fusion.2
  7.4 6.0 %collective-permute-start.9 = (bf16[96,704]{1,0:T(8,128)(2,1)S(1)}, bf16[96,704]{1,0:T(8,128)(2,1)S(1)}, u32[]{:S(2)}, u32[]{:S(2)}) collective-permute-start(bf16[96,704]{1,0:T(8,128)(2,1)S(1)} %pad_maximum_fusion.2), channel_id=1, source_target_pairs={{0,16},{1,24},{8,17},{9,25},{16,0},{17,8},{24,1},{25,9},{2,18},{3,... | collective-permute-start | bytes 405512 | tf_op jit(solution)/shard_map/ppermute | solution.py:323
  13.4 1.9 %collective-permute-start.8 = (bf16[96,704]{1,0:T(8,128)(2,1)S(1)}, bf16[96,704]{1,0:T(8,128)(2,1)S(1)}, u32[]{:S(2)}, u32[]{:S(2)}) collective-permute-start(bf16[96,704]{1,0:T(8,128)(2,1)S(1)} %pad_maximum_fusion.2), channel_id=1, source_target_pairs={{0,0},{1,8},{8,1},{9,9},{16,16},{17,24},{24,17},{25,25},{2,2},{3,1... | collective-permute-start | bytes 405512 | tf_op jit(solution)/shard_map/ppermute | solution.py:323
  15.4 1.5 collective-permute-done.9
  16.8 3.1 %collective-permute-done.8 = bf16[96,704]{1,0:T(8,128)(2,1)S(1)} collective-permute-done((bf16[96,704]{1,0:T(8,128)(2,1)S(1)}, bf16[96,704]{1,0:T(8,128)(2,1)S(1)}, u32[]{:S(2)}, u32[]{:S(2)}) %collective-permute-start.8) | collective-permute-done | bytes 135200 | tf_op jit(solution)/shard_map/ppermute | solution.py:323
  19.9 0.7 pad_maximum_fusion.1
  20.7 3.1 %collective-permute-start = (bf16[128,2048]{1,0:T(8,128)(2,1)}, bf16[128,2048]{1,0:T(8,128)(2,1)S(1)}, u32[]{:S(2)}, u32[]{:S(2)}) collective-permute-start(bf16[128,2048]{1,0:T(8,128)(2,1)} %param.19), channel_id=1, source_target_pairs={{0,2},{2,4},{4,6},{6,0},{1,3},{3,5},{5,7},{7,1},{8,10},{10,12},{12... | collective-permute-start | bytes 1572872 | tf_op jit(solution)/shard_map/ppermute | solution.py:328
  23.8 4.4 %collective-permute-start.1 = (bf16[128,2048]{1,0:T(8,128)(2,1)}, bf16[128,2048]{1,0:T(8,128)(2,1)S(1)}, u32[]{:S(2)}, u32[]{:S(2)}) collective-permute-start(bf16[128,2048]{1,0:T(8,128)(2,1)} %param.19), channel_id=1, source_target_pairs={{0,4},{2,6},{4,0},{6,2},{1,5},{3,7},{5,1},{7,3},{8,12},{10,14},{12... | collective-permute-start | bytes 1572872 | tf_op jit(solution)/shard_map/ppermute | solution.py:328
  28.2 3.1 %collective-permute-start.2 = (bf16[128,2048]{1,0:T(8,128)(2,1)}, bf16[128,2048]{1,0:T(8,128)(2,1)S(1)}, u32[]{:S(2)}, u32[]{:S(2)}) collective-permute-start(bf16[128,2048]{1,0:T(8,128)(2,1)} %param.19), channel_id=1, source_target_pairs={{0,6},{2,0},{4,2},{6,4},{1,7},{3,1},{5,3},{7,5},{8,14},{10,8},{12,... | collective-permute-start | bytes 1572872 | tf_op jit(solution)/shard_map/ppermute | solution.py:328
  31.2 1.1 constant_dynamic-update-slice_fusion.3
  32.3 2.2 %collective-permute-done = bf16[128,2048]{1,0:T(8,128)(2,1)S(1)} collective-permute-done((bf16[128,2048]{1,0:T(8,128)(2,1)}, bf16[128,2048]{1,0:T(8,128)(2,1)S(1)}, u32[]{:S(2)}, u32[]{:S(2)}) %collective-permute-start) | collective-permute-done | bytes 524320 | tf_op jit(solution)/shard_map/ppermute | solution.py:328
  34.6 13.5 %collective-permute-done.1 = bf16[128,2048]{1,0:T(8,128)(2,1)S(1)} collective-permute-done((bf16[128,2048]{1,0:T(8,128)(2,1)}, bf16[128,2048]{1,0:T(8,128)(2,1)S(1)}, u32[]{:S(2)}, u32[]{:S(2)}) %collective-permute-start.1) | collective-permute-done | bytes 524320 | tf_op jit(solution)/shard_map/ppermute | solution.py:328
  48.1 2.5 %collective-permute-done.2 = bf16[128,2048]{1,0:T(8,128)(2,1)S(1)} collective-permute-done((bf16[128,2048]{1,0:T(8,128)(2,1)}, bf16[128,2048]{1,0:T(8,128)(2,1)S(1)}, u32[]{:S(2)}, u32[]{:S(2)}) %collective-permute-start.2) | collective-permute-done | bytes 524320 | tf_op jit(solution)/shard_map/ppermute | solution.py:328
  50.7 3.4 %collective-permute-start.3 = (bf16[512,2048]{1,0:T(8,128)(2,1)S(1)}, bf16[512,2048]{1,0:T(8,128)(2,1)}, u32[]{:S(2)}, u32[]{:S(2)}) collective-permute-start(bf16[512,2048]{1,0:T(8,128)(2,1)S(1)} %constant_dynamic-update-slice_fusion.near_w_ref), channel_id=1, source_target_pairs={{0,1},{1,0},{2,3},{3,2},{4,5},{5,4},{6,7},{7,6},{8,9},{9,8},{10,11... | collective-permute-start | bytes 6291464 | tf_op jit(solution)/shard_map/ppermute | solution.py:328
  54.1 1.9 %retention.1 = (f32[256,128]{1,0:T(8,128)}, bf16[256,128]{1,0:T(8,128)(2,1)}, f32[8,24,128]{2,1,0:T(8,128)}) custom-call(bf16[256,128]{1,0:T(8,128)(2,1)} %q_ref.1, bf16[256,128]{1,0:T(8,128)(2,1)} %k_ref.1, bf16[256,128]{1,0:T(8,128)(2,1)} %v_ref.1, f32[1,256]{1,0:T(1,128)} %bitcast.67), custom_call_target="tpu_custom_call" | custom-call | flops 50331648 | bytes 1048576 | tf_op jit(solution)/shard_map/retention/pallas_call | solution.py:68
  56.0 8.6 %all_to_all.25.states_ref = f32[8,24,128]{2,1,0:T(8,128)S(1)} all-to-all(f32[8,24,128]{2,1,0:T(8,128)} %get-tuple-element.12), channel_id=1, replica_groups=mesh['zh'=8,'zl'=2,'y1'=2,'y0'=2,'x'=4,'c'=2] {'zl','y1','y0'}, dimensions={0} | all-to-all | bytes 196608 | tf_op jit(solution)/shard_map/all_to_all | solution.py:332
  65.3 14.3 %all-to-all-start.1 = ((bf16[8,24,128]{2,1,0:T(8,128)(2,1)}), bf16[8,24,128]{2,1,0:T(8,128)(2,1)S(1)}, u32[]{:S(2)}, u32[]{:S(2)}) async-start(bf16[8,24,128]{2,1,0:T(8,128)(2,1)} %joined_state.1), calls=%async_computation.1 | async-start | bytes 98304 | tf_op jit(solution)/shard_map/all_to_all | solution.py:332
  79.6 4.3 %collective-permute-start.6 = (bf16[32,2048]{1,0:T(8,128)(2,1)S(1)}, bf16[32,2048]{1,0:T(8,128)(2,1)S(1)}, u32[]{:S(2)}, u32[]{:S(2)}) collective-permute-start(bf16[32,2048]{1,0:T(8,128)(2,1)S(1)} %copy-done.2), channel_id=1, source_target_pairs={{0,6},{2,0},{4,2},{6,4},{1,7},{3,1},{5,3},{7,5},{8,14},{10,8},{12,... | collective-permute-start | bytes 393224 | tf_op jit(solution)/shard_map/ppermute | solution.py:328
  83.9 3.3 %collective-permute-start.5 = (bf16[32,2048]{1,0:T(8,128)(2,1)S(1)}, bf16[32,2048]{1,0:T(8,128)(2,1)S(1)}, u32[]{:S(2)}, u32[]{:S(2)}) collective-permute-start(bf16[32,2048]{1,0:T(8,128)(2,1)S(1)} %copy-done.2), channel_id=1, source_target_pairs={{0,4},{2,6},{4,0},{6,2},{1,5},{3,7},{5,1},{7,3},{8,12},{10,14},{12... | collective-permute-start | bytes 393224 | tf_op jit(solution)/shard_map/ppermute | solution.py:328
  87.2 1.9 %collective-permute-start.4 = (bf16[32,2048]{1,0:T(8,128)(2,1)S(1)}, bf16[32,2048]{1,0:T(8,128)(2,1)S(1)}, u32[]{:S(2)}, u32[]{:S(2)}) collective-permute-start(bf16[32,2048]{1,0:T(8,128)(2,1)S(1)} %copy-done.2), channel_id=1, source_target_pairs={{0,2},{2,4},{4,6},{6,0},{1,3},{3,5},{5,7},{7,1},{8,10},{10,12},{12... | collective-permute-start | bytes 393224 | tf_op jit(solution)/shard_map/ppermute | solution.py:328
  89.1 2.8 %all-to-all-done.1.joined_ref = bf16[8,24,128]{2,1,0:T(8,128)(2,1)S(1)} async-done(((bf16[8,24,128]{2,1,0:T(8,128)(2,1)}), bf16[8,24,128]{2,1,0:T(8,128)(2,1)S(1)}, u32[]{:S(2)}, u32[]{:S(2)}) %all-to-all-start.1) | async-done | bytes 49184 | tf_op jit(solution)/shard_map/all_to_all | solution.py:332
  92.6 3.3 %all-to-all-start.2 = ((f32[8,16,128]{2,1,0:T(8,128)}), f32[8,16,128]{2,1,0:T(8,128)S(1)}, u32[]{:S(2)}, u32[]{:S(2)}) async-start(f32[8,16,128]{2,1,0:T(8,128)} %incoming_state.1), calls=%async_computation.2 | async-start | bytes 131072 | tf_op jit(solution)/shard_map/all_to_all | solution.py:332
  96.1 3.3 %collective-permute-start.7 = (bf16[4,32,2048]{2,1,0:T(8,128)(2,1)S(1)}, bf16[4,32,2048]{2,1,0:T(8,128)(2,1)}, u32[]{:S(2)}, u32[]{:S(2)}) collective-permute-start(bf16[4,32,2048]{2,1,0:T(8,128)(2,1)S(1)} %pad_maximum_fusion.near_s_ref), channel_id=1, source_target_pairs={{0,8},{8,0},{1,9},{9,1},{2,10},{10,2},{3,11},{11,3},{4,12},{12,4},... | collective-permute-start | bytes 1572872 | tf_op jit(solution)/shard_map/ppermute | solution.py:328
  99.4 1.8 %all-to-all-done.2 = f32[8,16,128]{2,1,0:T(8,128)S(1)} async-done(((f32[8,16,128]{2,1,0:T(8,128)}), f32[8,16,128]{2,1,0:T(8,128)S(1)}, u32[]{:S(2)}, u32[]{:S(2)}) %all-to-all-start.2) | async-done | bytes 65568 | tf_op jit(solution)/shard_map/all_to_all | solution.py:332
  101.8 2.1 %mix.1 = bf16[8,2,4,32,128]{4,3,2,1,0:T(8,128)(2,1)} custom-call(f32[256,128]{1,0:T(8,128)} %get-tuple-element.10.within_ref, bf16[256,128]{1,0:T(8,128)(2,1)} %get-tuple-element.11.carry_q_ref, f32[128,128]{1,0:T(8,128)} %bitcast.61, bf16[256,128]{1,0:T(8,128)(2,1)} %gate_ref.1, bf16[1,128]{1,0:T(2,128)(2,1)} %bitcast.68), custom_call_target="tpu_custom_call" | custom-call | flops 8388608 | bytes 1048576 | tf_op jit(solution)/shard_map/mix/pallas_call | solution.py:158
  104.0 8.8 %all-to-all-start.3 = ((bf16[16,4,32,128]{3,2,1,0:T(8,128)(2,1)}), bf16[16,4,32,128]{3,2,1,0:T(8,128)(2,1)S(1)}, u32[]{:S(2)}, u32[]{:S(2)}) async-start(bf16[16,4,32,128]{3,2,1,0:T(8,128)(2,1)} %bitcast.60), calls=%async_computation.3 | async-start | bytes 1048576 | tf_op jit(solution)/shard_map/all_to_all | solution.py:332
  112.9 9.4 %all-to-all-done.3 = bf16[16,4,32,128]{3,2,1,0:T(8,128)(2,1)S(1)} async-done(((bf16[16,4,32,128]{3,2,1,0:T(8,128)(2,1)}), bf16[16,4,32,128]{3,2,1,0:T(8,128)(2,1)S(1)}, u32[]{:S(2)}, u32[]{:S(2)}) %all-to-all-start.3) | async-done | bytes 524320 | tf_op jit(solution)/shard_map/all_to_all | solution.py:332
  122.3 3.4 %group_rows.1 = (bf16[256,2048]{1,0:T(8,128)(2,1)S(1)}, f32[32,2048]{1,0:T(8,128)S(1)}) custom-call(s32[3]{0:T(128)S(1)} %pad_add_fusion.here_ref, bf16[2,8,4,32,128]{4,3,2,1,0:T(8,128)(2,1)S(1)} %bitcast.58, bf16[512,2048]{1,0:T(8,128)(2,1)S(1)} %constant_dynamic-update-slice_fusion.near_w_ref, bf16[512,2048]{1,0:T(8,128)(2,1)} %collective-permute-done.3.far_w_ref, ...), custom_call_target="tpu_custom_call" | custom-call | flops 1073741824 | bytes 8388608 | tf_op jit(solution)/shard_map/group_rows/pallas_call | solution.py:220
  125.7 1.0 copy-done
  126.7 6.4 %feed_forward.1 = bf16[256,2048]{1,0:T(8,128)(2,1)S(1)} custom-call(s32[1]{0:T(128)} %bitcast.13.y1_ref, bf16[256,2048]{1,0:T(8,128)(2,1)} %copy-done, bf16[16,2,2,3,32,704]{5,4,3,2,1,0:T(8,128)(2,1)} %bitcast.59), custom_call_target="tpu_custom_call" | custom-call | flops 2214592512 | bytes 8388608 | tf_op jit(solution)/shard_map/feed_forward/pallas_call | solution.py:298
  133.1 17.8 %all_to_all.26 = bf16[8,32,2048]{2,1,0:T(8,128)(2,1)S(1)} all-to-all(bf16[8,32,2048]{2,1,0:T(8,128)(2,1)S(1)} %bitcast.57), channel_id=1, replica_groups=mesh['zh'=8,'zl'=2,'y1'=2,'y0'=2,'x'=4,'c'=2] {'y0','x'}, dimensions={0} | all-to-all | bytes 2097152 | tf_op jit(solution)/shard_map/all_to_all | solution.py:332
  150.9 0.8 fusion
  (23 shorter events, 2.2 us)
Async XLA Ops:
  6.5 120.1 %all-gather.3.cloned.1.call-start = ((), (), s32[]{:S(2)}) async-start(), calls=%async_computation.5 | async-start | bytes 9732096 | tf_op jit(solution)/shard_map/all_gather | solution.py:342
  7.4 9.4 %collective-permute-start.9 = (bf16[96,704]{1,0:T(8,128)(2,1)S(1)}, bf16[96,704]{1,0:T(8,128)(2,1)S(1)}, u32[]{:S(2)}, u32[]{:S(2)}) collective-permute-start(bf16[96,704]{1,0:T(8,128)(2,1)S(1)} %pad_maximum_fusion.2), channel_id=1, source_target_pairs={{0,16},{1,24},{8,17},{9,25},{16,0},{17,8},{24,1},{25,9},{2,18},{3,... | collective-permute-start | bytes 405512 | tf_op jit(solution)/shard_map/ppermute | solution.py:323
  13.4 6.5 %collective-permute-start.8 = (bf16[96,704]{1,0:T(8,128)(2,1)S(1)}, bf16[96,704]{1,0:T(8,128)(2,1)S(1)}, u32[]{:S(2)}, u32[]{:S(2)}) collective-permute-start(bf16[96,704]{1,0:T(8,128)(2,1)S(1)} %pad_maximum_fusion.2), channel_id=1, source_target_pairs={{0,0},{1,8},{8,1},{9,9},{16,16},{17,24},{24,17},{25,25},{2,2},{3,1... | collective-permute-start | bytes 405512 | tf_op jit(solution)/shard_map/ppermute | solution.py:323
  20.7 13.9 %collective-permute-start = (bf16[128,2048]{1,0:T(8,128)(2,1)}, bf16[128,2048]{1,0:T(8,128)(2,1)S(1)}, u32[]{:S(2)}, u32[]{:S(2)}) collective-permute-start(bf16[128,2048]{1,0:T(8,128)(2,1)} %param.19), channel_id=1, source_target_pairs={{0,2},{2,4},{4,6},{6,0},{1,3},{3,5},{5,7},{7,1},{8,10},{10,12},{12... | collective-permute-start | bytes 1572872 | tf_op jit(solution)/shard_map/ppermute | solution.py:328
  23.8 24.3 %collective-permute-start.1 = (bf16[128,2048]{1,0:T(8,128)(2,1)}, bf16[128,2048]{1,0:T(8,128)(2,1)S(1)}, u32[]{:S(2)}, u32[]{:S(2)}) collective-permute-start(bf16[128,2048]{1,0:T(8,128)(2,1)} %param.19), channel_id=1, source_target_pairs={{0,4},{2,6},{4,0},{6,2},{1,5},{3,7},{5,1},{7,3},{8,12},{10,14},{12... | collective-permute-start | bytes 1572872 | tf_op jit(solution)/shard_map/ppermute | solution.py:328
  28.2 22.5 %collective-permute-start.2 = (bf16[128,2048]{1,0:T(8,128)(2,1)}, bf16[128,2048]{1,0:T(8,128)(2,1)S(1)}, u32[]{:S(2)}, u32[]{:S(2)}) collective-permute-start(bf16[128,2048]{1,0:T(8,128)(2,1)} %param.19), channel_id=1, source_target_pairs={{0,6},{2,0},{4,2},{6,4},{1,7},{3,1},{5,3},{7,5},{8,14},{10,8},{12,... | collective-permute-start | bytes 1572872 | tf_op jit(solution)/shard_map/ppermute | solution.py:328
  32.3 47.3 %copy-start.2 = (bf16[32,2048]{1,0:T(8,128)(2,1)S(1)}, bf16[32,2048]{1,0:T(8,128)(2,1)}, u32[]{:S(2)}) copy-start(bf16[32,2048]{1,0:T(8,128)(2,1)} %param.12) | copy-start | bytes 393220
  50.7 62.1 %copy-start.3 = (bf16[2048]{0:T(1024)(128)(2,1)S(1)}, bf16[2048]{0:T(1024)(128)(2,1)}, u32[]{:S(2)}) copy-start(bf16[2048]{0:T(1024)(128)(2,1)} %param.20) | copy-start | bytes 12292
  50.7 71.6 %collective-permute-start.3 = (bf16[512,2048]{1,0:T(8,128)(2,1)S(1)}, bf16[512,2048]{1,0:T(8,128)(2,1)}, u32[]{:S(2)}, u32[]{:S(2)}) collective-permute-start(bf16[512,2048]{1,0:T(8,128)(2,1)S(1)} %constant_dynamic-update-slice_fusion.near_w_ref), channel_id=1, source_target_pairs={{0,1},{1,0},{2,3},{3,2},{4,5},{5,4},{6,7},{7,6},{8,9},{9,8},{10,11... | collective-permute-start | bytes 6291464 | tf_op jit(solution)/shard_map/ppermute | solution.py:328
  65.3 26.7 %all-to-all-start.1 = ((bf16[8,24,128]{2,1,0:T(8,128)(2,1)}), bf16[8,24,128]{2,1,0:T(8,128)(2,1)S(1)}, u32[]{:S(2)}, u32[]{:S(2)}) async-start(bf16[8,24,128]{2,1,0:T(8,128)(2,1)} %joined_state.1), calls=%async_computation.1 | async-start | bytes 98304 | tf_op jit(solution)/shard_map/all_to_all | solution.py:332
  79.6 16.4 %collective-permute-start.6 = (bf16[32,2048]{1,0:T(8,128)(2,1)S(1)}, bf16[32,2048]{1,0:T(8,128)(2,1)S(1)}, u32[]{:S(2)}, u32[]{:S(2)}) collective-permute-start(bf16[32,2048]{1,0:T(8,128)(2,1)S(1)} %copy-done.2), channel_id=1, source_target_pairs={{0,6},{2,0},{4,2},{6,4},{1,7},{3,1},{5,3},{7,5},{8,14},{10,8},{12,... | collective-permute-start | bytes 393224 | tf_op jit(solution)/shard_map/ppermute | solution.py:328
  83.9 12.1 %collective-permute-start.5 = (bf16[32,2048]{1,0:T(8,128)(2,1)S(1)}, bf16[32,2048]{1,0:T(8,128)(2,1)S(1)}, u32[]{:S(2)}, u32[]{:S(2)}) collective-permute-start(bf16[32,2048]{1,0:T(8,128)(2,1)S(1)} %copy-done.2), channel_id=1, source_target_pairs={{0,4},{2,6},{4,0},{6,2},{1,5},{3,7},{5,1},{7,3},{8,12},{10,14},{12... | collective-permute-start | bytes 393224 | tf_op jit(solution)/shard_map/ppermute | solution.py:328
  87.2 8.8 %collective-permute-start.4 = (bf16[32,2048]{1,0:T(8,128)(2,1)S(1)}, bf16[32,2048]{1,0:T(8,128)(2,1)S(1)}, u32[]{:S(2)}, u32[]{:S(2)}) collective-permute-start(bf16[32,2048]{1,0:T(8,128)(2,1)S(1)} %copy-done.2), channel_id=1, source_target_pairs={{0,2},{2,4},{4,6},{6,0},{1,3},{3,5},{5,7},{7,1},{8,10},{10,12},{12... | collective-permute-start | bytes 393224 | tf_op jit(solution)/shard_map/ppermute | solution.py:328
  92.6 8.6 %all-to-all-start.2 = ((f32[8,16,128]{2,1,0:T(8,128)}), f32[8,16,128]{2,1,0:T(8,128)S(1)}, u32[]{:S(2)}, u32[]{:S(2)}) async-start(f32[8,16,128]{2,1,0:T(8,128)} %incoming_state.1), calls=%async_computation.2 | async-start | bytes 131072 | tf_op jit(solution)/shard_map/all_to_all | solution.py:332
  96.1 16.8 %collective-permute-start.7 = (bf16[4,32,2048]{2,1,0:T(8,128)(2,1)S(1)}, bf16[4,32,2048]{2,1,0:T(8,128)(2,1)}, u32[]{:S(2)}, u32[]{:S(2)}) collective-permute-start(bf16[4,32,2048]{2,1,0:T(8,128)(2,1)S(1)} %pad_maximum_fusion.near_s_ref), channel_id=1, source_target_pairs={{0,8},{8,0},{1,9},{9,1},{2,10},{10,2},{3,11},{11,3},{4,12},{12,4},... | collective-permute-start | bytes 1572872 | tf_op jit(solution)/shard_map/ppermute | solution.py:328
  101.2 0.6 copy-start.1
  104.0 18.3 %all-to-all-start.3 = ((bf16[16,4,32,128]{3,2,1,0:T(8,128)(2,1)}), bf16[16,4,32,128]{3,2,1,0:T(8,128)(2,1)S(1)}, u32[]{:S(2)}, u32[]{:S(2)}) async-start(bf16[16,4,32,128]{3,2,1,0:T(8,128)(2,1)} %bitcast.60), calls=%async_computation.3 | async-start | bytes 1048576 | tf_op jit(solution)/shard_map/all_to_all | solution.py:332
  125.7 1.0 copy-start
Sparse Core Ops, SparseCore 0:
  20.8 83.6 all-gather.2
